TPU v7x, 128 devices: a whole 4x4x4 slice. The times are simulated.
128 devices in a mesh: sp: 64 (over z, y, x), tp: 2 (over core).
Axes of the slice: x: 4, y: 4, z: 4, core: 2. Of those that a mesh axis runs over, the one named last changes fastest.
Arguments:
- mixer_output: bfloat16 [8192, 2048], P('sp'), may hold values from -6 to 6
- layer_cotangent: bfloat16 [8192, 2048], P('sp'), may hold values from -16 to 16
- expert_choice: int32 [8192, 2], P('sp'), may hold values from 0 to 63, all different within a row; in each aligned block of 128 rows (0 to 127, 128 to 255, ...) at most 8 rows name the same one
- route_weight: float32 [8192, 2], P('sp'), may hold values from 0.1 to 0.9
- gate_pre: bfloat16 [64, 512, 1024], P('sp', None, 'tp'), may hold values from -15 to 15
- up_pre: bfloat16 [64, 512, 1024], P('sp', None, 'tp'), may hold values from -15 to 15
- w_gate: bfloat16 [64, 2048, 1024], P('sp', None, 'tp'), may hold values from -0.125 to 0.125
- w_up: bfloat16 [64, 2048, 1024], P('sp', None, 'tp'), may hold values from -0.125 to 0.125
- w_down: bfloat16 [64, 1024, 2048], P('sp', 'tp'), may hold values from -0.1875 to 0.1875
- w_out: bfloat16 [2048, 2048], P('tp'), may hold values from -0.125 to 0.125
- norm_gain: bfloat16 [2048], P('tp'), may hold values from 0.099609375 to 1.8984375
- scan_in: bfloat16 [8192, 2048], P('sp', 'tp'), may hold values from -6 to 6
- gate_in: bfloat16 [8192, 2048], P('sp', 'tp'), may hold values from -9 to 9
- b_proj: bfloat16 [8192, 1024], P('sp', 'tp'), may hold values from -1.796875 to 1.796875
- c_proj: bfloat16 [8192, 1024], P('sp', 'tp'), may hold values from -1.796875 to 1.796875
- log_decay: float32 [8192, 32], P('sp', 'tp'), may hold values from -3 to 0
- entry_state: float32 [64, 32, 64, 128], P('sp', 'tp'), may hold values from -24 to 24
Outputs:
- grad_w_gate: bfloat16 [64, 2048, 1024], P('sp', None, 'tp')
- grad_w_up: bfloat16 [64, 2048, 1024], P('sp', None, 'tp')
- grad_w_down: bfloat16 [64, 1024, 2048], P('sp', 'tp')
- grad_out_proj: float32 [2048, 2048], P('sp', 'tp')
- grad_scan_in: bfloat16 [8192, 2048], P('sp', 'tp')
- grad_gate_in: bfloat16 [8192, 2048], P('sp', 'tp')
- grad_b_proj: bfloat16 [8192, 1024], P('sp', 'tp')
- grad_c_proj: bfloat16 [8192, 1024], P('sp', 'tp')
- grad_log_decay: float32 [8192, 32], P('sp', 'tp')
Inputs may be any that keep to these rules, and one draw needn't show every extreme that they name: `expert_choice`: in the 128 rows of one device no expert is named more than 8 times, a bound that some blocks reach; the 2 entries of a row differ.
All inputs are finite; a program needn't handle non-finite values.
Results may differ from a plain program's by a relative error of at most 0.012.
Values may be sent and summed in bfloat16 or wider, within the bound.
A program may use at most 192 MiB of HBM per device.

v0:
```python
import jax
import jax.numpy as jnp
from jax import lax
from jax.sharding import Mesh
from jax.sharding import PartitionSpec as P

HEAD_DIM = 64
STATE = 128
SP = ("sp_0", "sp_1", "sp_2")


rms_epsilon = 1e-05
clamp_limit = 7.0
swish_alpha = 1.702


def sent_together(arrays, axis, split_dim, concat_dim, along):
    both = jnp.concatenate(arrays, axis=along)
    out, at, gathered = (
        lax.all_to_all(both, axis, split_axis=split_dim, concat_axis=concat_dim, tiled=True),
        0,
        [],
    )
    for a in arrays:
        gathered.append(lax.slice_in_dim(out, at, at + a.shape[along], axis=along))
        at += a.shape[along]
    return tuple(gathered)


def in_one_piece(arrays, axis, dim, along):
    both = jnp.concatenate(arrays, axis=along)
    out, at, gathered = (lax.all_gather(both, axis, axis=dim, tiled=True), 0, [])
    for a in arrays:
        gathered.append(lax.slice_in_dim(out, at, at + a.shape[along], axis=along))
        at += a.shape[along]
    return tuple(gathered)


def from_everyone(x, axis):
    size = lax.axis_size(axis)
    return lax.all_to_all(jnp.broadcast_to(x[None], (size, *x.shape)), axis, 0, 0, tiled=True)


def of_everyone(x, axis):
    return from_everyone(x, axis).astype(jnp.float32).sum(axis=0)


def summed_rows(running, axes):
    for axis in axes:
        running = lax.psum_scatter(running, axis, scatter_dimension=0, tiled=True)
    return running


def filled_with(x, identity):
    return jax.tree.map(
        lambda part, zero: jnp.zeros_like(part) + jnp.asarray(zero, part.dtype), x, identity
    )


def carried_in(x, axes, combine, identity):
    before = start = filled_with(x, identity)
    running = x
    for axis in reversed(axes):
        size, position = (lax.axis_size(axis), lax.axis_index(axis))
        pieces = jax.tree.map(lambda part: lax.all_gather(part, axis), running)
        inside, running = (start, start)
        for k in reversed(range(size)):
            passed = k > position
            running = combine(running, jax.tree.map(lambda part: part[k], pieces))
            inside = jax.tree.map(lambda new, old: jnp.where(passed, new, old), running, inside)
        before = combine(inside, before)
    return before


def slot_ranks(expert_ids, expert_count):
    targets = expert_ids.reshape(-1)
    one_hot = (targets[:, None] == jnp.arange(expert_count, dtype=jnp.int32)[None, :]).astype(
        jnp.int32
    )
    earlier = jnp.cumsum(one_hot, axis=0) - one_hot
    return (targets, jnp.sum(earlier * one_hot, axis=1))


def expert_side(hidden_rows, grad_rows, gate_value, up_value, gate_weight, up_weight, down_weight):
    act_grad = jnp.einsum("rd,fd->rf", grad_rows, down_weight, preferred_element_type=jnp.float32)
    gate_full = gate_value.astype(jnp.float32)
    up_full = up_value.astype(jnp.float32)
    gate_clip = jnp.minimum(gate_full, clamp_limit)
    up_clip = jnp.clip(up_full, -clamp_limit, clamp_limit)
    sigmoid_gate = jax.nn.sigmoid(swish_alpha * gate_clip)
    swish_gate = gate_clip * sigmoid_gate
    active = ((up_clip + 1.0) * swish_gate).astype(jnp.bfloat16)
    up_grad = jnp.where(
        (up_full > -clamp_limit) & (up_full < clamp_limit), act_grad * swish_gate, 0.0
    ).astype(jnp.bfloat16)
    slope = sigmoid_gate + swish_alpha * gate_clip * sigmoid_gate * (1.0 - sigmoid_gate)
    gate_grad = jnp.where(gate_full < clamp_limit, act_grad * (up_clip + 1.0) * slope, 0.0).astype(
        jnp.bfloat16
    )
    down_wgrad = jnp.einsum(
        "rf,rd->fd", active, grad_rows, preferred_element_type=jnp.float32
    ).astype(jnp.bfloat16)
    gate_wgrad = jnp.einsum(
        "rd,rf->df", hidden_rows, gate_grad, preferred_element_type=jnp.float32
    ).astype(jnp.bfloat16)
    up_wgrad = jnp.einsum(
        "rd,rf->df", hidden_rows, up_grad, preferred_element_type=jnp.float32
    ).astype(jnp.bfloat16)
    partial_rows = jnp.einsum(
        "rf,df->rd", gate_grad, gate_weight, preferred_element_type=jnp.float32
    )
    partial_rows = partial_rows + jnp.einsum(
        "rf,df->rd", up_grad, up_weight, preferred_element_type=jnp.float32
    )
    return (gate_wgrad, up_wgrad, down_wgrad, partial_rows)


def join_reverse(earlier, later):
    upper_decay, upper_state, upper_local, upper_grad = earlier
    lower_decay, lower_state, lower_local, lower_grad = later
    joined_decay = lower_decay * upper_decay
    joined_state = lower_state + lower_decay[:, None, None] * upper_state
    joined_local = upper_decay[:, None, None] * lower_local + upper_local
    joined_grad = lower_grad + upper_grad - jnp.sum(upper_state * lower_local, axis=(1, 2))
    return (joined_decay, joined_state, joined_local, joined_grad)


def body(
    mixer_output,
    layer_cotangent,
    expert_choice,
    route_weight,
    gate_pre,
    up_pre,
    w_gate,
    w_up,
    w_down,
    w_out,
    norm_gain,
    scan_in,
    gate_in,
    b_proj,
    c_proj,
    log_decay,
    entry_state,
):
    expert_count = lax.axis_size(SP)
    tokens_here = mixer_output.shape[0]
    model_width = mixer_output.shape[1]
    top_count = expert_choice.shape[1]
    capacity = gate_pre.shape[1] // expert_count
    targets, ranked = slot_ranks(expert_choice, expert_count)
    token_of = jnp.arange(tokens_here * top_count, dtype=jnp.int32) // top_count
    grad_rows = (
        route_weight.reshape(-1)[:, None] * layer_cotangent[token_of].astype(jnp.float32)
    ).astype(jnp.bfloat16)
    blank_slots = jnp.zeros((expert_count, capacity, model_width), jnp.bfloat16)
    send_hidden = blank_slots.at[targets, ranked].set(mixer_output[token_of])
    send_grads = blank_slots.at[targets, ranked].set(grad_rows)
    half_width = model_width // lax.axis_size("tp")
    half_start = lax.axis_index("tp") * half_width
    hidden_half = lax.dynamic_slice_in_dim(send_hidden, half_start, half_width, 2)
    grads_half = lax.dynamic_slice_in_dim(send_grads, half_start, half_width, 2)
    came_hidden, came_grads = sent_together((hidden_half, grads_half), SP, 0, 0, 1)
    recv_hidden, recv_grads = in_one_piece((came_hidden, came_grads), "tp", 2, 0)
    gate_wgrad, up_wgrad, down_wgrad, partial_rows = expert_side(
        recv_hidden.reshape(-1, model_width),
        recv_grads.reshape(-1, model_width),
        gate_pre[0],
        up_pre[0],
        w_gate[0],
        w_up[0],
        w_down[0],
    )
    summed = of_everyone(partial_rows.astype(jnp.bfloat16), "tp").astype(jnp.float32)
    returned = lax.all_to_all(
        summed.astype(jnp.bfloat16).reshape(expert_count, capacity, -1),
        SP,
        split_axis=0,
        concat_axis=0,
        tiled=True,
    )
    columns = returned.shape[2]
    moe_terms = (
        returned[targets, ranked]
        .astype(jnp.float32)
        .reshape(tokens_here, top_count, columns)
        .sum(axis=1)
    )
    grad_hidden = (layer_cotangent.astype(jnp.float32) + moe_terms).astype(jnp.bfloat16)
    head_count = log_decay.shape[1]
    group_count = b_proj.shape[1] // STATE
    per_group = head_count // group_count
    scan_heads = scan_in.reshape(tokens_here, head_count, HEAD_DIM)
    b_groups = b_proj.reshape(tokens_here, group_count, STATE)
    c_groups = c_proj.reshape(tokens_here, group_count, STATE)
    x_float = scan_heads.astype(jnp.float32)
    b_float = b_groups.astype(jnp.float32)
    c_float = c_groups.astype(jnp.float32)
    cumulative = jnp.cumsum(log_decay, axis=0)
    growth = jnp.exp(cumulative)
    tail_decay = jnp.exp(cumulative[-1][None, :] - cumulative)
    token_locations = jnp.arange(tokens_here)
    causal = token_locations[:, None] >= token_locations[None, :]
    log_gaps = cumulative.T[:, :, None] - cumulative.T[:, None, :]
    decay_mat = jnp.exp(jnp.where(causal[None], log_gaps, -jnp.inf))
    inner_prod = jnp.einsum("tgn,sgn->gts", c_groups, b_groups, preferred_element_type=jnp.float32)
    mix_weights = (jnp.repeat(inner_prod, per_group, axis=0) * decay_mat).astype(jnp.bfloat16)
    state_groups = entry_state.reshape(group_count, per_group, HEAD_DIM, STATE)
    y_inner = jnp.einsum(
        "hts,shp->thp", mix_weights, scan_heads, preferred_element_type=jnp.float32
    )
    y_carry = jnp.einsum("tgn,grpn->tgrp", c_float, state_groups).reshape(
        tokens_here, head_count, HEAD_DIM
    )
    scan_out = y_inner + y_carry * growth[:, :, None]
    gate_float = gate_in.astype(jnp.float32)
    gate_sig = jax.nn.sigmoid(gate_float)
    gate_silu = gate_float * gate_sig
    gated = scan_out.reshape(tokens_here, -1) * gate_silu
    grouped = gated.reshape(tokens_here, group_count, -1)
    inv_rms = lax.rsqrt(jnp.mean(grouped * grouped, axis=-1, keepdims=True) + rms_epsilon)
    unit = grouped * inv_rms
    gain_groups = norm_gain.astype(jnp.float32).reshape(group_count, -1)
    mixed = (unit * gain_groups).reshape(tokens_here, -1).astype(jnp.bfloat16)
    grad_out_proj = summed_rows(
        jnp.einsum("td,ti->di", grad_hidden, mixed, preferred_element_type=jnp.float32), SP
    )
    grad_mixed = jnp.einsum("td,id->ti", grad_hidden, w_out, preferred_element_type=jnp.float32)
    grad_unit = grad_mixed.reshape(tokens_here, group_count, -1) * gain_groups
    grad_grouped = inv_rms * (grad_unit - unit * jnp.mean(grad_unit * unit, axis=-1, keepdims=True))
    grad_gated = grad_grouped.reshape(tokens_here, -1)
    grad_gate_in = (
        grad_gated
        * scan_out.reshape(tokens_here, -1)
        * gate_sig
        * (1.0 + gate_float * (1.0 - gate_sig))
    ).astype(jnp.bfloat16)
    grad_y = (grad_gated * gate_silu).reshape(tokens_here, head_count, HEAD_DIM)
    grad_y_b = grad_y.astype(jnp.bfloat16)
    grad_x_inner = jnp.einsum(
        "hts,thp->shp", mix_weights, grad_y_b, preferred_element_type=jnp.float32
    )
    grad_weights = (
        jnp.einsum("thp,shp->hts", grad_y_b, scan_heads, preferred_element_type=jnp.float32)
        * decay_mat
    )
    grad_weights = (
        grad_weights.reshape(group_count, per_group, tokens_here, tokens_here)
        .sum(axis=1)
        .astype(jnp.bfloat16)
    )
    grad_c_inner = jnp.einsum(
        "gts,sgn->tgn", grad_weights, b_groups, preferred_element_type=jnp.float32
    )
    grad_b_inner = jnp.einsum(
        "gts,tgn->sgn", grad_weights, c_groups, preferred_element_type=jnp.float32
    )
    grown_grads = (grad_y * growth[:, :, None]).reshape(
        tokens_here, group_count, per_group, HEAD_DIM
    )
    grad_c_carry = jnp.einsum("tgrp,grpn->tgn", grown_grads, state_groups)
    block_state = jnp.einsum("tgrp,tgn->grpn", grown_grads, c_float).reshape(
        head_count, HEAD_DIM, STATE
    )
    x_tail = (x_float * tail_decay[:, :, None]).reshape(
        tokens_here, group_count, per_group, HEAD_DIM
    )
    local_state = jnp.einsum("sgrp,sgn->grpn", x_tail, b_float).reshape(head_count, HEAD_DIM, STATE)
    local_grad = jnp.sum(
        jnp.sum(grad_y * scan_out, axis=2) - jnp.sum(x_float * grad_x_inner, axis=2), axis=0
    )
    identity = (
        jnp.ones((head_count,), jnp.float32),
        jnp.zeros((head_count, HEAD_DIM, STATE), jnp.float32),
        jnp.zeros((head_count, HEAD_DIM, STATE), jnp.float32),
        jnp.zeros((head_count,), jnp.float32),
    )
    scanned = carried_in(
        (jnp.exp(cumulative[-1]), block_state, local_state, local_grad), SP, join_reverse, identity
    )
    later_state = scanned[1]
    later_grad = scanned[3]
    later_groups = later_state.reshape(group_count, per_group, HEAD_DIM, STATE)
    grad_x_carry = jnp.einsum("sgn,grpn->sgrp", b_float, later_groups).reshape(
        tokens_here, head_count, HEAD_DIM
    )
    grad_x = grad_x_inner + grad_x_carry * tail_decay[:, :, None]
    grad_b_carry = jnp.einsum("sgrp,grpn->sgn", x_tail, later_groups)
    grad_a = jnp.sum(grad_y * scan_out, axis=2) - jnp.sum(x_float * grad_x, axis=2)
    grad_log_decay = jnp.flip(jnp.cumsum(jnp.flip(grad_a, 0), axis=0), 0) + later_grad[None, :]
    grad_scan_in = grad_x.reshape(tokens_here, -1).astype(jnp.bfloat16)
    grad_b_proj = (grad_b_inner + grad_b_carry).reshape(tokens_here, -1).astype(jnp.bfloat16)
    grad_c_proj = (grad_c_inner + grad_c_carry).reshape(tokens_here, -1).astype(jnp.bfloat16)
    return (
        gate_wgrad[None],
        up_wgrad[None],
        down_wgrad[None],
        grad_out_proj,
        grad_scan_in,
        grad_gate_in,
        grad_b_proj,
        grad_c_proj,
        grad_log_decay,
    )


def solution(mesh):
    split = Mesh(mesh.devices.reshape(4, 4, 4, mesh.shape["tp"]), ("sp_0", "sp_1", "sp_2", "tp"))
    return jax.shard_map(
        body,
        mesh=split,
        in_specs=(
            P(SP, None),
            P(SP, None),
            P(SP, None),
            P(SP, None),
            P(SP, None, "tp"),
            P(SP, None, "tp"),
            P(SP, None, "tp"),
            P(SP, None, "tp"),
            P(SP, "tp", None),
            P("tp", None),
            P("tp"),
            P(SP, "tp"),
            P(SP, "tp"),
            P(SP, "tp"),
            P(SP, "tp"),
            P(SP, "tp"),
            P(SP, "tp", None, None),
        ),
        out_specs=(
            P(SP, None, "tp"),
            P(SP, None, "tp"),
            P(SP, "tp", None),
            P(SP, "tp"),
            P(SP, "tp"),
            P(SP, "tp"),
            P(SP, "tp"),
            P(SP, "tp"),
            P(SP, "tp"),
        ),
        check_vma=False,
    )
```

profile of v0, /device:TPU:0, one launch (start us, length us, event | category | flops | bytes accessed | tf_op | source)
XLA Modules:
  0.0 497.3 jit_solution(16533501211170878534)
XLA Ops:
  11.3 2.3 gather_fusion.1
  13.6 2.3 gather_fusion
  16.1 2.4 multiply_convert_fusion
  18.5 1.6 broadcast_in_dim.29.clone
  20.1 46.1 %scatter_fusion.1 = bf16[64,8,2048]{2,1,0:T(8,128)(2,1)} fusion(bf16[64,8,2048]{2,1,0:T(8,128)(2,1)} %broadcast_in_dim.29.clone, s32[256]{0:T(256)S(1)} %bitcast.593, bf16[256,2048]{1,0:T(8,128)(2,1)} %multiply_convert_fusion), kind=kCustom, calls=%fused_computation.4 | custom fusion | bytes 3147776 | tf_op jit(solution)/shard_map/scatter | solution.py:159
  66.2 1.6 broadcast_in_dim.29.clone.1
  67.8 46.1 %scatter_fusion = bf16[64,8,2048]{2,1,0:T(8,128)(2,1)} fusion(bf16[64,8,2048]{2,1,0:T(8,128)(2,1)} %broadcast_in_dim.29.clone.1, s32[256]{0:T(256)S(1)} %bitcast.594, bf16[256,2048]{1,0:T(8,128)(2,1)} %gather_fusion), kind=kCustom, calls=%fused_computation.3 | custom fusion | bytes 3147776 | tf_op jit(solution)/shard_map/scatter | solution.py:158
  113.9 1.7 constant_dynamic-slice_fusion
  115.8 41.5 %all_to_all.15 = bf16[64,16,1024]{2,1,0:T(8,128)(2,1)S(1)} all-to-all(bf16[64,16,1024]{2,1,0:T(8,128)(2,1)S(1)} %pad_maximum_fusion), channel_id=1, replica_groups=mesh['sp_0'=4,'sp_1'=4,'sp_2'=4,'tp'=2] {'sp_0','sp_1','sp_2'}, dimensions={0} | all-to-all | bytes 4194304 | tf_op jit(solution)/shard_map/all_to_all | solution.py:20
  157.5 1.5 pad_maximum_fusion.1
  161.7 10.6 %all-gather.14.cloned.1.call-done = bf16[128,8,2048]{2,1,0:T(8,128)(2,1)} async-done(((bf16[128,8,1024]{2,1,0:T(8,128)(2,1)}), bf16[128,8,2048]{2,1,0:T(8,128)(2,1)}) %all-gather.14.cloned.1.call-update) | async-done | bytes 4194320 | tf_op jit(solution)/shard_map/all_gather | solution.py:32
  172.3 4.2 fusion.29
  176.6 1.7 fusion.4
  178.7 1.3 add_convert_fusion
  180.5 8.2 %all_to_all.16 = bf16[2,512,2048]{2,1,0:T(8,128)(2,1)} all-to-all(bf16[2,512,2048]{2,1,0:T(8,128)(2,1)S(1)} %broadcast_in_dim.34), channel_id=1, replica_groups=mesh['sp_0'=4,'sp_1'=4,'sp_2'=4,'tp'=2] {'tp'}, dimensions={0} | all-to-all | bytes 8388608 | tf_op jit(solution)/shard_map/all_to_all | solution.py:41
  188.7 5.1 %reduce_sum.266 = bf16[512,2048]{1,0:T(8,128)(2,1)} reduce(bf16[2,512,2048]{2,1,0:T(8,128)(2,1)} %all_to_all.16, bf16[]{:T(256)} %constant.26.clone.1), dimensions={0}, to_apply=%region_5.6 | reduce | flops 1048576 | bytes 6291458 | tf_op jit(solution)/shard_map/reduce_sum | solution.py:45
  193.7 10.5 %all-to-all-start.2 = ((bf16[64,8,2048]{2,1,0:T(8,128)(2,1)}), bf16[64,8,2048]{2,1,0:T(8,128)(2,1)S(1)}, u32[]{:S(2)}, u32[]{:S(2)}) async-start(bf16[64,8,2048]{2,1,0:T(8,128)(2,1)} %bitcast.600), calls=%async_computation.2 | async-start | bytes 4194304 | tf_op jit(solution)/shard_map/all_to_all | solution.py:176
  210.7 1.5 fusion.115
  212.2 1.3 fusion.13
  213.5 1.2 copy.123
  214.8 2.1 fusion.107
  216.8 2.1 reshape.481
  219.0 1.3 multiply_reduce_fusion.2
  221.8 21.7 %all-to-all-done.2 = bf16[64,8,2048]{2,1,0:T(8,128)(2,1)S(1)} async-done(((bf16[64,8,2048]{2,1,0:T(8,128)(2,1)}), bf16[64,8,2048]{2,1,0:T(8,128)(2,1)S(1)}, u32[]{:S(2)}, u32[]{:S(2)}) %all-to-all-start.2) | async-done | bytes 2097184 | tf_op jit(solution)/shard_map/all_to_all | solution.py:176
  243.5 5.2 %gather_fusion.2 = bf16[256,2048]{1,0:T(8,128)(2,1)} fusion(bf16[64,8,2048]{2,1,0:T(8,128)(2,1)S(1)} %all-to-all-done.2, s32[256]{0:T(256)S(1)} %bitcast.595), kind=kCustom, calls=%fused_computation.2 | custom fusion | bytes 2099200 | tf_op jit(solution)/shard_map/gather | solution.py:185
  248.7 3.6 reshape.487
  252.2 4.1 reduce_sum.267
  256.4 4.5 fusion.155
  260.9 2.1 reshape.482
  263.1 1.5 multiply_reduce_fusion.1
  265.0 1.2 fusion.50
  266.2 1.2 copy.124
  268.6 7.6 %all-gather.1 = f32[4,1,16]{2,1,0:T(1,128)S(1)} all-gather(f32[1,1,16]{2,1,0:T(1,128)S(1)} %copy-done.109), channel_id=1, replica_groups=mesh['sp_0'=4,'sp_1'=4,'sp_2'=4,'tp'=2] {'sp_2'}, dimensions={0}, use_global_device_ids=true | all-gather | bytes 320 | tf_op jit(solution)/shard_map/all_gather | solution.py:65
  277.2 1.2 slice_bitcast_fusion.24
  278.4 2.5 add_add_fusion.1
  281.0 14.6 %all-gather.16.cloned.1.call-done = f32[4,16,64,128]{3,2,1,0:T(8,128)} async-done(((f32[1,16,64,128]{3,2,1,0:T(8,128)}), f32[4,16,64,128]{3,2,1,0:T(8,128)}) %all-gather.16.cloned.1.call-update) | async-done | bytes 2097168 | tf_op jit(solution)/shard_map/all_gather | solution.py:65
  295.6 3.3 fusion.163
  298.9 5.6 %fusion.99 = f32[2048,1024]{1,0:T(8,128)} fusion(f32[1024]{0:T(1024)S(1)} %convert_element_type.135, f32[128,1024]{1,0:T(8,128)S(1)} %bitcast.607, f32[128,2048]{1,0:T(8,128)S(1)} %reduce_sum.267, bf16[128,2048]{1,0:T(8,128)(2,1)S(1)} %copy-done.2, f32[128,1024]{1,0:T(8,128)S(1)} %copy-done.10, bf16[128,1024]{1,0:T(8,128)(2,1)} %param.29), kind=kOutput, calls=%fused_computation.178 | convolution fusion | flops 538836992 | bytes 11276288 | tf_op jit(solution)/shard_map/td,ti->di/dot_general | solution.py:227
  305.2 9.8 %all-gather.2 = f32[4,1,16]{2,1,0:T(1,128)S(1)} all-gather(f32[1,1,16]{2,1,0:T(1,128)S(1)} %copy-done.114), channel_id=1, replica_groups=mesh['sp_0'=4,'sp_1'=4,'sp_2'=4,'tp'=2] {'sp_1'}, dimensions={0}, use_global_device_ids=true | all-gather | bytes 320 | tf_op jit(solution)/shard_map/all_gather | solution.py:65
  315.6 12.8 %all-gather.24.cloned.1.call-done = f32[4,16,64,128]{3,2,1,0:T(8,128)} async-done(((f32[1,16,64,128]{3,2,1,0:T(8,128)}), f32[4,16,64,128]{3,2,1,0:T(8,128)}) %all-gather.24.cloned.1.call-update) | async-done | bytes 2097168 | tf_op jit(solution)/shard_map/all_gather | solution.py:65
  328.4 2.5 add_add_fusion
  331.0 30.3 %all-gather.18.cloned.1.call-done = f32[4,16,64,128]{3,2,1,0:T(8,128)} async-done(((f32[1,16,64,128]{3,2,1,0:T(8,128)}), f32[4,16,64,128]{3,2,1,0:T(8,128)}) %all-gather.18.cloned.1.call-update) | async-done | bytes 2097168 | tf_op jit(solution)/shard_map/all_gather | solution.py:65
  361.4 3.3 fusion.164
  365.5 10.2 %all-gather.3 = f32[4,1,16]{2,1,0:T(1,128)S(1)} all-gather(f32[1,1,16]{2,1,0:T(1,128)S(1)} %get-tuple-element.124), channel_id=1, replica_groups=mesh['sp_0'=4,'sp_1'=4,'sp_2'=4,'tp'=2] {'sp_0'}, dimensions={0}, use_global_device_ids=true | all-gather | bytes 320 | tf_op jit(solution)/shard_map/all_gather | solution.py:65
  381.4 4.4 fusion.2
  385.9 1.6 reduce-scatter.4.cloned.1.call-done
  387.9 4.4 fusion.1
  392.3 2.9 fusion
  397.0 1.7 copy.138
  399.4 1.9 all-gather.26.cloned.1.call-done
  401.3 1.8 fusion.57
  403.2 2.8 fusion.86
  406.1 2.2 fusion.72
  408.4 25.0 %all-gather.20.cloned.1.call-done = f32[4,16,64,128]{3,2,1,0:T(8,128)} async-done(((f32[1,16,64,128]{3,2,1,0:T(8,128)}), f32[4,16,64,128]{3,2,1,0:T(8,128)}) %all-gather.20.cloned.1.call-update) | async-done | bytes 2097168 | tf_op jit(solution)/shard_map/all_gather | solution.py:65
  433.4 1.9 fusion.165
  435.7 1.3 multiply_add_fusion
  438.7 10.5 %all-reduce = f32[64]{0:T(128)S(1)} all-reduce(f32[64]{0:T(128)S(1)} %dynamic-update-slice), channel_id=2, replica_groups=mesh['sp_0'=4,'sp_1'=4,'sp_2'=4,'tp'=2] {'sp_2'}, use_global_device_ids=true, to_apply=%add | all-reduce | flops 64 | bytes 512
  449.4 9.8 %all-gather.4 = f32[4,1,16]{2,1,0:T(1,128)S(1)} all-gather(f32[1,1,16]{2,1,0:T(1,128)S(1)} %bitcast.636), channel_id=1, replica_groups=mesh['sp_0'=4,'sp_1'=4,'sp_2'=4,'tp'=2] {'sp_1'}, dimensions={0}, use_global_device_ids=true | all-gather | bytes 320 | tf_op jit(solution)/shard_map/all_gather | solution.py:65
  459.7 5.5 %reduce-scatter.6.cloned.1.call-done = f32[128,1024]{1,0:T(8,128)} async-done(((f32[512,1024]{1,0:T(8,128)}), f32[128,1024]{1,0:T(8,128)}) %reduce-scatter.6.cloned.1.call-update) | async-done | bytes 524304 | tf_op jit(solution)/shard_map/reduce_scatter | solution.py:50
  465.9 1.8 copy.136
  468.9 10.0 %all-gather.5 = f32[4,1,16]{2,1,0:T(1,128)S(1)} all-gather(f32[1,1,16]{2,1,0:T(1,128)S(1)} %bitcast.637), channel_id=1, replica_groups=mesh['sp_0'=4,'sp_1'=4,'sp_2'=4,'tp'=2] {'sp_0'}, dimensions={0}, use_global_device_ids=true | all-gather | bytes 320 | tf_op jit(solution)/shard_map/all_gather | solution.py:65
  478.9 1.8 fusion.56
  480.9 2.4 fusion.62
  484.1 5.3 %reduce-scatter.8.cloned.1.call-done = f32[32,1024]{1,0:T(8,128)} async-done(((f32[128,1024]{1,0:T(8,128)}), f32[32,1024]{1,0:T(8,128)}) %reduce-scatter.8.cloned.1.call-update) | async-done | bytes 131088 | tf_op jit(solution)/shard_map/reduce_scatter | solution.py:50
  (357 shorter events, 33.0 us)
Async XLA Ops:
  8.0 168.5 %copy-start = (bf16[1,2048,512]{2,1,0:T(8,128)(2,1)S(1)}, bf16[1,2048,512]{2,1,0:T(8,128)(2,1)}, u32[]{:S(2)}) copy-start(bf16[1,2048,512]{2,1,0:T(8,128)(2,1)} %param.23) | copy-start | bytes 6291460
  8.0 164.3 %all-gather.14.cloned.1.call-start = ((), (), s32[]{:S(2)}) async-start(), calls=%async_computation.6 | async-start | bytes 6291456 | tf_op jit(solution)/shard_map/all_gather | solution.py:32
  193.7 13.4 %copy-start.43 = (bf16[128,512]{1,0:T(8,128)(2,1)S(1)}, bf16[128,512]{1,0:T(8,128)(2,1)}, u32[]{:S(2)}) copy-start(bf16[128,512]{1,0:T(8,128)(2,1)} %param.31) | copy-start | bytes 393220
  193.7 49.7 %all-to-all-start.2 = ((bf16[64,8,2048]{2,1,0:T(8,128)(2,1)}), bf16[64,8,2048]{2,1,0:T(8,128)(2,1)S(1)}, u32[]{:S(2)}, u32[]{:S(2)}) async-start(bf16[64,8,2048]{2,1,0:T(8,128)(2,1)} %bitcast.600), calls=%async_computation.2 | async-start | bytes 4194304 | tf_op jit(solution)/shard_map/all_to_all | solution.py:176
  204.3 74.1 %all-gather.22.cloned.1.call-start = ((), (), s32[]{:S(2)}) async-start(), calls=%async_computation.13 | async-start | bytes 2621440 | tf_op jit(solution)/shard_map/all_gather | solution.py:65
  205.4 90.2 %all-gather.16.cloned.1.call-start = ((), (), s32[]{:S(2)}) async-start(), calls=%async_computation.10 | async-start | bytes 2621440 | tf_op jit(solution)/shard_map/all_gather | solution.py:65
  214.7 50.2 %copy-start.9 = (f32[128,1024]{1,0:T(8,128)}, f32[128,1024]{1,0:T(8,128)S(1)}, u32[]{:S(2)}) copy-start(f32[128,1024]{1,0:T(8,128)S(1)} %copy.123) | copy-start | bytes 1572868
  268.5 59.9 %all-gather.24.cloned.1.call-start = ((), (), s32[]{:S(2)}) async-start(), calls=%async_computation.14 | async-start | bytes 2621440 | tf_op jit(solution)/shard_map/all_gather | solution.py:65
  276.7 18.8 %copy-start.73 = (f32[16]{0:T(128)}, f32[16]{0:T(128)S(1)}, u32[]{:S(2)}) copy-start(f32[16]{0:T(128)S(1)} %get-tuple-element.77) | copy-start | bytes 196
  277.2 18.3 %copy-start.95 = (f32[16]{0:T(128)}, f32[16]{0:T(128)S(1)}, u32[]{:S(2)}) copy-start(f32[16]{0:T(128)S(1)} %get-tuple-element.125) | copy-start | bytes 196
  278.4 17.2 %copy-start.99 = (f32[16]{0:T(128)}, f32[16]{0:T(128)S(1)}, u32[]{:S(2)}) copy-start(f32[16]{0:T(128)S(1)} %get-tuple-element.127) | copy-start | bytes 196
  278.4 17.2 %copy-start.75 = (f32[16]{0:T(128)S(1)}, f32[16]{0:T(128)}, u32[]{:S(2)}) copy-start(f32[16]{0:T(128)} %get-tuple-element.126) | copy-start | bytes 196
  280.9 80.4 %all-gather.18.cloned.1.call-start = ((), (), s32[]{:S(2)}) async-start(), calls=%async_computation.11 | async-start | bytes 2621440 | tf_op jit(solution)/shard_map/all_gather | solution.py:65
  298.9 88.6 %reduce-scatter.4.cloned.1.call-start = ((), (), s32[]{:S(2)}) async-start(), calls=%async_computation.7 | async-start | bytes 10485760 | tf_op jit(solution)/shard_map/reduce_scatter | solution.py:50
  304.5 96.7 %all-gather.26.cloned.1.call-start = ((), (), s32[]{:S(2)}) async-start(), calls=%async_computation.15 | async-start | bytes 2621440 | tf_op jit(solution)/shard_map/all_gather | solution.py:65
  315.6 45.8 %copy-start.71 = (f32[16]{0:T(128)}, f32[16]{0:T(128)S(1)}, u32[]{:S(2)}) copy-start(f32[16]{0:T(128)S(1)} %get-tuple-element.75) | copy-start | bytes 196
  315.6 45.8 %copy-start.93 = (f32[16]{0:T(128)}, f32[16]{0:T(128)S(1)}, u32[]{:S(2)}) copy-start(f32[16]{0:T(128)S(1)} %get-tuple-element.114) | copy-start | bytes 196
  315.6 49.1 %copy-start.76 = (f32[16]{0:T(128)}, f32[16]{0:T(128)S(1)}, u32[]{:S(2)}) copy-start(f32[16]{0:T(128)S(1)} %get-tuple-element.115) | copy-start | bytes 196
  315.6 45.7 %copy-start.97 = (f32[16]{0:T(128)}, f32[16]{0:T(128)S(1)}, u32[]{:S(2)}) copy-start(f32[16]{0:T(128)S(1)} %get-tuple-element.116) | copy-start | bytes 196
  315.6 49.1 %copy-start.78 = (f32[16]{0:T(128)}, f32[16]{0:T(128)S(1)}, u32[]{:S(2)}) copy-start(f32[16]{0:T(128)S(1)} %get-tuple-element.117) | copy-start | bytes 196
  315.6 49.1 %copy-start.80 = (f32[16]{0:T(128)}, f32[16]{0:T(128)S(1)}, u32[]{:S(2)}) copy-start(f32[16]{0:T(128)S(1)} %get-tuple-element.118) | copy-start | bytes 196
  315.6 49.1 %copy-start.82 = (f32[16]{0:T(128)}, f32[16]{0:T(128)S(1)}, u32[]{:S(2)}) copy-start(f32[16]{0:T(128)S(1)} %get-tuple-element.119) | copy-start | bytes 196
  331.0 102.4 %all-gather.20.cloned.1.call-start = ((), (), s32[]{:S(2)}) async-start(), calls=%async_computation.12 | async-start | bytes 2621440 | tf_op jit(solution)/shard_map/all_gather | solution.py:65
  361.3 17.8 %copy-start.113 = (f32[16]{0:T(128)S(1)}, f32[16]{0:T(128)}, u32[]{:S(2)}) copy-start(f32[16]{0:T(128)} %get-tuple-element.133) | copy-start | bytes 196
  361.4 17.9 %copy-start.112 = (f32[16]{0:T(128)S(1)}, f32[16]{0:T(128)}, u32[]{:S(2)}) copy-start(f32[16]{0:T(128)} %get-tuple-element.131) | copy-start | bytes 196
  361.4 18.0 %copy-start.111 = (f32[16]{0:T(128)S(1)}, f32[16]{0:T(128)}, u32[]{:S(2)}) copy-start(f32[16]{0:T(128)} %get-tuple-element.132) | copy-start | bytes 196
  361.4 18.1 %copy-start.110 = (f32[16]{0:T(128)S(1)}, f32[16]{0:T(128)}, u32[]{:S(2)}) copy-start(f32[16]{0:T(128)} %get-tuple-element.134) | copy-start | bytes 196
  361.4 18.1 %copy-start.121 = (u32[128]{0:T(128)S(1)}, u32[128]{0:T(128)}, u32[]{:S(2)}) copy-start(u32[128]{0:T(128)} %constant.135) | copy-start | bytes 1540
  361.4 20.0 %copy-start.118 = (bf16[1,512,512]{2,1,0:T(8,128)(2,1)S(1)}, bf16[1,512,512]{2,1,0:T(8,128)(2,1)}, u32[]{:S(2)}) copy-start(bf16[1,512,512]{2,1,0:T(8,128)(2,1)} %param.21) | copy-start | bytes 1572868
  361.4 20.0 %copy-start.120 = (bf16[1,512,512]{2,1,0:T(8,128)(2,1)S(1)}, bf16[1,512,512]{2,1,0:T(8,128)(2,1)}, u32[]{:S(2)}) copy-start(bf16[1,512,512]{2,1,0:T(8,128)(2,1)} %param.22) | copy-start | bytes 1572868
  364.7 100.5 %reduce-scatter.6.cloned.1.call-start = ((), (), s32[]{:S(2)}) async-start(), calls=%async_computation.8 | async-start | bytes 2621440 | tf_op jit(solution)/shard_map/reduce_scatter | solution.py:50
  387.5 101.8 %reduce-scatter.8.cloned.1.call-start = ((), (), s32[]{:S(2)}) async-start(), calls=%async_computation.9 | async-start | bytes 655360 | tf_op jit(solution)/shard_map/reduce_scatter | solution.py:50
  406.0 43.3 %copy-start.84 = (f32[16]{0:T(128)}, f32[16]{0:T(128)S(1)}, u32[]{:S(2)}) copy-start(f32[16]{0:T(128)S(1)} %get-tuple-element.47) | copy-start | bytes 196
  406.0 43.3 %copy-start.86 = (f32[16]{0:T(128)}, f32[16]{0:T(128)S(1)}, u32[]{:S(2)}) copy-start(f32[16]{0:T(128)S(1)} %get-tuple-element.54) | copy-start | bytes 196
  406.0 43.3 %copy-start.88 = (f32[16]{0:T(128)}, f32[16]{0:T(128)S(1)}, u32[]{:S(2)}) copy-start(f32[16]{0:T(128)S(1)} %get-tuple-element.57) | copy-start | bytes 196
  408.3 27.0 %copy-start.19 = (f32[1,16,64,128]{3,2,1,0:T(8,128)S(1)}, f32[1,16,64,128]{3,2,1,0:T(8,128)}, u32[]{:S(2)}) copy-start(f32[1,16,64,128]{3,2,1,0:T(8,128)} %get-tuple-element.84) | copy-start | bytes 1572868
  408.3 27.0 %copy-start.20 = (f32[1,16,64,128]{3,2,1,0:T(8,128)S(1)}, f32[1,16,64,128]{3,2,1,0:T(8,128)}, u32[]{:S(2)}) copy-start(f32[1,16,64,128]{3,2,1,0:T(8,128)} %get-tuple-element.86) | copy-start | bytes 1572868
  408.3 27.0 %copy-start.21 = (f32[1,16,64,128]{3,2,1,0:T(8,128)S(1)}, f32[1,16,64,128]{3,2,1,0:T(8,128)}, u32[]{:S(2)}) copy-start(f32[1,16,64,128]{3,2,1,0:T(8,128)} %get-tuple-element.87) | copy-start | bytes 1572868
  408.3 27.0 %copy-start.53 = (f32[4,4]{1,0:T(4,128)S(1)}, f32[4,4]{1,0:T(4,128)}, u32[]{:S(2)}) copy-start(f32[4,4]{1,0:T(4,128)} %copy-done.52) | copy-start | bytes 196
  408.3 27.0 %copy-start.55 = (f32[4,4]{1,0:T(4,128)S(1)}, f32[4,4]{1,0:T(4,128)}, u32[]{:S(2)}) copy-start(f32[4,4]{1,0:T(4,128)} %copy-done.54) | copy-start | bytes 196
  408.3 27.0 %copy-start.57 = (f32[4,4]{1,0:T(4,128)S(1)}, f32[4,4]{1,0:T(4,128)}, u32[]{:S(2)}) copy-start(f32[4,4]{1,0:T(4,128)} %copy-done.56) | copy-start | bytes 196
  408.3 27.0 %copy-start.59 = (f32[4,4]{1,0:T(4,128)S(1)}, f32[4,4]{1,0:T(4,128)}, u32[]{:S(2)}) copy-start(f32[4,4]{1,0:T(4,128)} %copy-done.58) | copy-start | bytes 196
  408.3 27.0 %copy-start.61 = (f32[4,4]{1,0:T(4,128)S(1)}, f32[4,4]{1,0:T(4,128)}, u32[]{:S(2)}) copy-start(f32[4,4]{1,0:T(4,128)} %get-tuple-element.78) | copy-start | bytes 196
  408.4 27.0 %copy-start.62 = (f32[4,4]{1,0:T(4,128)S(1)}, f32[4,4]{1,0:T(4,128)}, u32[]{:S(2)}) copy-start(f32[4,4]{1,0:T(4,128)} %get-tuple-element.79) | copy-start | bytes 196
  408.4 27.0 %copy-start.63 = (f32[4,4]{1,0:T(4,128)S(1)}, f32[4,4]{1,0:T(4,128)}, u32[]{:S(2)}) copy-start(f32[4,4]{1,0:T(4,128)} %get-tuple-element.136) | copy-start | bytes 196
  408.4 27.0 %copy-start.64 = (f32[4,4]{1,0:T(4,128)S(1)}, f32[4,4]{1,0:T(4,128)}, u32[]{:S(2)}) copy-start(f32[4,4]{1,0:T(4,128)} %get-tuple-element.137) | copy-start | bytes 196
  408.4 27.0 %copy-start.65 = (f32[4,4]{1,0:T(4,128)S(1)}, f32[4,4]{1,0:T(4,128)}, u32[]{:S(2)}) copy-start(f32[4,4]{1,0:T(4,128)} %mul.797) | copy-start | bytes 196
  408.4 27.0 %copy-start.66 = (f32[4,4]{1,0:T(4,128)S(1)}, f32[4,4]{1,0:T(4,128)}, u32[]{:S(2)}) copy-start(f32[4,4]{1,0:T(4,128)} %mul.794) | copy-start | bytes 196
  408.4 27.0 %copy-start.67 = (f32[4,4]{1,0:T(4,128)S(1)}, f32[4,4]{1,0:T(4,128)}, u32[]{:S(2)}) copy-start(f32[4,4]{1,0:T(4,128)} %mul.792) | copy-start | bytes 196
  408.4 27.0 %copy-start.68 = (f32[4,4]{1,0:T(4,128)S(1)}, f32[4,4]{1,0:T(4,128)}, u32[]{:S(2)}) copy-start(f32[4,4]{1,0:T(4,128)} %mul.790) | copy-start | bytes 196
  437.0 22.5 %copy-start.32 = (bf16[128,4,128]{0,2,1:T(8,128)(2,1)S(1)}, bf16[128,4,128]{0,2,1:T(8,128)(2,1)}, u32[]{:S(2)}) copy-start(bf16[128,4,128]{0,2,1:T(8,128)(2,1)} %copy-done.31) | copy-start | bytes 393220
  437.3 22.2 %copy-start.39 = (bf16[4,128,128]{2,1,0:T(8,128)(2,1)S(1)}, bf16[4,128,128]{2,1,0:T(8,128)(2,1)}, u32[]{:S(2)}) copy-start(bf16[4,128,128]{2,1,0:T(8,128)(2,1)} %copy-done.38) | copy-start | bytes 393220
  437.3 27.9 %copy-start.90 = (f32[16]{0:T(128)S(1)}, f32[16]{0:T(128)}, u32[]{:S(2)}) copy-start(f32[16]{0:T(128)} %get-tuple-element.45) | copy-start | bytes 196
  437.3 27.9 %copy-start.91 = (f32[16]{0:T(128)S(1)}, f32[16]{0:T(128)}, u32[]{:S(2)}) copy-start(f32[16]{0:T(128)} %get-tuple-element.53) | copy-start | bytes 196
  438.4 40.5 %copy-start.6 = (f32[4,16,64,128]{3,2,1,0:T(8,128)S(1)}, f32[4,16,64,128]{3,2,1,0:T(8,128)}, u32[]{:S(2)}) copy-start(f32[4,16,64,128]{3,2,1,0:T(8,128)} %all-gather.20.cloned.1.call-done) | copy-start | bytes 6291460
  438.4 40.5 %copy-start.101 = (f32[16]{0:T(128)S(1)}, f32[16]{0:T(128)}, u32[]{:S(2)}) copy-start(f32[16]{0:T(128)} %get-tuple-element.112) | copy-start | bytes 196
  438.4 40.5 %copy-start.102 = (f32[16]{0:T(128)S(1)}, f32[16]{0:T(128)}, u32[]{:S(2)}) copy-start(f32[16]{0:T(128)} %get-tuple-element.113) | copy-start | bytes 196
  438.4 40.5 %copy-start.115 = (f32[16]{0:T(128)S(1)}, f32[16]{0:T(128)}, u32[]{:S(2)}) copy-start(f32[16]{0:T(128)} %get-tuple-element.111) | copy-start | bytes 196
  467.7 13.0 %copy-start.27 = (f32[16,64,128]{2,1,0:T(8,128)S(1)}, f32[16,64,128]{2,1,0:T(8,128)}, u32[]{:S(2)}) copy-start(f32[16,64,128]{2,1,0:T(8,128)} %get-tuple-element.72) | copy-start | bytes 1572868
  467.7 13.0 %copy-start.72 = (f32[16]{0:T(128)S(1)}, f32[16]{0:T(128)}, u32[]{:S(2)}) copy-start(f32[16]{0:T(128)} %copy-done.71) | copy-start | bytes 196
  467.7 13.1 %copy-start.94 = (f32[16]{0:T(128)S(1)}, f32[16]{0:T(128)}, u32[]{:S(2)}) copy-start(f32[16]{0:T(128)} %copy-done.93) | copy-start | bytes 196
  467.7 13.1 %copy-start.98 = (f32[16]{0:T(128)S(1)}, f32[16]{0:T(128)}, u32[]{:S(2)}) copy-start(f32[16]{0:T(128)} %copy-done.97) | copy-start | bytes 196
  467.7 13.1 %copy-start.103 = (f32[16]{0:T(128)S(1)}, f32[16]{0:T(128)}, u32[]{:S(2)}) copy-start(f32[16]{0:T(128)} %get-tuple-element.74) | copy-start | bytes 196
  467.7 13.1 %copy-start.105 = (f32[16]{0:T(128)S(1)}, f32[16]{0:T(128)}, u32[]{:S(2)}) copy-start(f32[16]{0:T(128)} %get-tuple-element.110) | copy-start | bytes 196
  (71 other events, 209.7 us)
Sparse Core Ops, SparseCore 0:
  159.1 13.1 all-gather.13
  304.7 82.8 reduce-scatter.3
Sparse Core Ops, SparseCore 1:
  206.4 40.5 all-gather.21
  268.6 26.9 all-gather.15
  297.7 30.7 all-gather.23
  330.7 30.6 all-gather.17
  363.0 38.2 all-gather.25
  402.9 30.4 all-gather.19
  435.7 29.5 reduce-scatter.5
  468.0 21.3 reduce-scatter.7
where the time goes:
time: 506 us; the launch traced here: 497 us
  local copies, waits for them, and re-layouts  140 us (28%)
  waiting for transfers between devices  129 us (25%)
  blocking collectives  108 us (21%)
  other arithmetic  52.7 us (10%)
  matrix products  37.4 us (7%)
  between operations  18.3 us (4%)
  starting transfers between devices  11.5 us (2%)
    all_gather x6, waiting for transfers between devices, carried_in(): pieces = jax.tree.map(lambda part: lax.all_gather(part, axis), running)  84.5 us
    all_gather x5, blocking collectives, carried_in(): pieces = jax.tree.map(lambda part: lax.all_gather(part, axis), running)  47.5 us
    scatter x1, local copies, waits for them, and re-layouts, body(): send_hidden = blank_slots.at[targets, ranked].set(mixer_output[token_of])  46.1 us
    scatter x1, local copies, waits for them, and re-layouts, body(): send_grads = blank_slots.at[targets, ranked].set(grad_rows)  46.1 us
    all_to_all x1, blocking collectives, sent_together(): lax.all_to_all(both, axis, split_axis=split_dim, concat_axis=concat_dim,...  41.5 us
    all_to_all x1, waiting for transfers between devices, body(): lax.all_to_all(summed.astype(jnp.bfloat16).reshape(expert_count, capacity...  21.7 us
    reduce_scatter x3, waiting for transfers between devices, summed_rows(): running = lax.psum_scatter(running, axis, scatter_dimension=0, tiled=True)  12.5 us
    unnamed x261, local copies, waits for them, and re-layouts  12.4 us
  transfers between devices with their start and end apart: 11, of which 10 were waited for; matrix products, arithmetic and copies ran while one was open for 21% of the time, Pallas kernels for 0%

commit v1 on v0

v1 whole, which is shorter than its diff:
```python
import jax
import jax.numpy as jnp
from jax import lax
from jax.sharding import Mesh
from jax.sharding import PartitionSpec as P

HEAD_DIM = 64
STATE = 128
SP = ("sp_0", "sp_1", "sp_2")


rms_epsilon = 1e-05
clamp_limit = 7.0
swish_alpha = 1.702


def expert_side(hidden_rows, grad_rows, gate_value, up_value, gate_weight, up_weight, down_weight):
    act_grad = jnp.einsum("rd,fd->rf", grad_rows, down_weight, preferred_element_type=jnp.float32)
    gate_full = gate_value.astype(jnp.float32)
    up_full = up_value.astype(jnp.float32)
    gate_clip = jnp.minimum(gate_full, clamp_limit)
    up_clip = jnp.clip(up_full, -clamp_limit, clamp_limit)
    sigmoid_gate = jax.nn.sigmoid(swish_alpha * gate_clip)
    swish_gate = gate_clip * sigmoid_gate
    active = ((up_clip + 1.0) * swish_gate).astype(jnp.bfloat16)
    up_grad = jnp.where(
        (up_full > -clamp_limit) & (up_full < clamp_limit), act_grad * swish_gate, 0.0
    ).astype(jnp.bfloat16)
    slope = sigmoid_gate + swish_alpha * gate_clip * sigmoid_gate * (1.0 - sigmoid_gate)
    gate_grad = jnp.where(gate_full < clamp_limit, act_grad * (up_clip + 1.0) * slope, 0.0).astype(
        jnp.bfloat16
    )
    down_wgrad = jnp.einsum(
        "rf,rd->fd", active, grad_rows, preferred_element_type=jnp.float32
    ).astype(jnp.bfloat16)
    gate_wgrad = jnp.einsum(
        "rd,rf->df", hidden_rows, gate_grad, preferred_element_type=jnp.float32
    ).astype(jnp.bfloat16)
    up_wgrad = jnp.einsum(
        "rd,rf->df", hidden_rows, up_grad, preferred_element_type=jnp.float32
    ).astype(jnp.bfloat16)
    partial_rows = jnp.einsum(
        "rf,df->rd", gate_grad, gate_weight, preferred_element_type=jnp.float32
    )
    partial_rows = partial_rows + jnp.einsum(
        "rf,df->rd", up_grad, up_weight, preferred_element_type=jnp.float32
    )
    return (gate_wgrad, up_wgrad, down_wgrad, partial_rows)


def slot_rows(expert_choice, expert_count, capacity):
    choice = expert_choice.T
    tokens = choice.shape[1]
    experts = lax.broadcasted_iota(jnp.int32, (expert_count, tokens), 0)
    hots = [(experts == choice[k][None, :]) for k in range(choice.shape[0])]
    named = sum(h.astype(jnp.bfloat16) for h in hots)
    before = (
        lax.broadcasted_iota(jnp.int32, (tokens, tokens), 0)
        < lax.broadcasted_iota(jnp.int32, (tokens, tokens), 1)
    ).astype(jnp.bfloat16)
    earlier = jnp.dot(named, before, preferred_element_type=jnp.float32)
    places = lax.broadcasted_iota(jnp.int32, (expert_count * capacity, tokens), 0)
    out = []
    for k, hot in enumerate(hots):
        rank = jnp.sum(jnp.where(hot, earlier, 0.0), axis=0).astype(jnp.int32)
        slot = choice[k] * capacity + rank
        out.append((places == slot[None, :]).astype(jnp.bfloat16))
    return out


def body(
    mixer_output,
    layer_cotangent,
    expert_choice,
    route_weight,
    gate_pre,
    up_pre,
    w_gate,
    w_up,
    w_down,
    w_out,
    norm_gain,
    scan_in,
    gate_in,
    b_proj,
    c_proj,
    log_decay,
    entry_state,
):
    f32, bf16 = jnp.float32, jnp.bfloat16
    expert_count = lax.axis_size(SP)
    sp = lax.axis_index(SP)
    tokens_here, model_width = mixer_output.shape
    capacity = gate_pre.shape[1] // expert_count
    half_width = model_width // lax.axis_size("tp")
    half_start = lax.axis_index("tp") * half_width
    mixer_half = lax.dynamic_slice_in_dim(mixer_output, half_start, half_width, 1)
    cotangent_half = lax.dynamic_slice_in_dim(layer_cotangent, half_start, half_width, 1)
    hot0, hot1 = slot_rows(expert_choice, expert_count, capacity)
    hot_any = hot0 + hot1
    cot_f = cotangent_half.astype(f32)
    rows0 = (route_weight[:, 0:1] * cot_f).astype(bf16)
    rows1 = (route_weight[:, 1:2] * cot_f).astype(bf16)
    send_grads = jnp.dot(
        jnp.concatenate([hot0, hot1], axis=1),
        jnp.concatenate([rows0, rows1], axis=0),
        preferred_element_type=f32,
    ).astype(bf16)
    send_hidden = jnp.dot(hot_any, mixer_half, preferred_element_type=f32).astype(bf16)

    def exchanged(rows):
        return lax.all_to_all(
            rows.reshape(expert_count, capacity, -1), SP, 0, 0, tiled=True
        ).reshape(expert_count * capacity, -1)

    both = jnp.concatenate(
        [
            send_grads.reshape(expert_count, capacity, -1),
            send_hidden.reshape(expert_count, capacity, -1),
        ],
        axis=1,
    )
    came = lax.all_to_all(both, SP, 0, 0, tiled=True)
    came = jnp.concatenate(
        [
            came[:, :capacity].reshape(-1, half_width),
            came[:, capacity:].reshape(-1, half_width),
        ],
        axis=0,
    )
    came = lax.all_gather(came, "tp", axis=1, tiled=True)
    recv_grads, recv_hidden = jnp.split(came, 2, axis=0)
    gate_wgrad, up_wgrad, down_wgrad, partial_rows = expert_side(
        recv_hidden, recv_grads, gate_pre[0], up_pre[0], w_gate[0], w_up[0], w_down[0]
    )
    pieces = partial_rows.astype(bf16).reshape(-1, 2, half_width)
    pieces = lax.all_to_all(pieces.transpose(1, 0, 2), "tp", 0, 0, tiled=True)
    summed = (pieces[0].astype(f32) + pieces[1].astype(f32)).astype(bf16)
    returned = exchanged(summed)
    moe_half = lax.dot_general(
        hot_any, returned, (((0,), (0,)), ((), ())), preferred_element_type=f32
    )
    hidden_half = (cot_f + moe_half).astype(bf16)
    grad_hidden = lax.all_gather(hidden_half, "tp", axis=1, tiled=True)

    head_count = log_decay.shape[1]
    group_count = b_proj.shape[1] // STATE
    per_group = head_count // group_count
    scan_heads = scan_in.reshape(tokens_here, head_count, HEAD_DIM)
    b_groups = b_proj.reshape(tokens_here, group_count, STATE)
    c_groups = c_proj.reshape(tokens_here, group_count, STATE)
    x_float = scan_heads.astype(f32)
    b_float = b_groups.astype(f32)
    c_float = c_groups.astype(f32)
    cumulative = jnp.cumsum(log_decay, axis=0)
    growth = jnp.exp(cumulative)
    tail_decay = jnp.exp(cumulative[-1][None, :] - cumulative)
    token_locations = jnp.arange(tokens_here)
    causal = token_locations[:, None] >= token_locations[None, :]
    log_gaps = cumulative.T[:, :, None] - cumulative.T[:, None, :]
    decay_mat = jnp.exp(jnp.where(causal[None], log_gaps, -jnp.inf))
    inner_prod = jnp.einsum("tgn,sgn->gts", c_groups, b_groups, preferred_element_type=f32)
    mix_weights = (jnp.repeat(inner_prod, per_group, axis=0) * decay_mat).astype(bf16)
    state_groups = entry_state.reshape(group_count, per_group, HEAD_DIM, STATE)
    y_inner = jnp.einsum("hts,shp->thp", mix_weights, scan_heads, preferred_element_type=f32)
    y_carry = jnp.einsum("tgn,grpn->tgrp", c_float, state_groups).reshape(
        tokens_here, head_count, HEAD_DIM
    )
    scan_out = y_inner + y_carry * growth[:, :, None]
    gate_float = gate_in.astype(f32)
    gate_sig = jax.nn.sigmoid(gate_float)
    gate_silu = gate_float * gate_sig
    gated = scan_out.reshape(tokens_here, -1) * gate_silu
    grouped = gated.reshape(tokens_here, group_count, -1)
    inv_rms = lax.rsqrt(jnp.mean(grouped * grouped, axis=-1, keepdims=True) + rms_epsilon)
    unit = grouped * inv_rms
    gain_groups = norm_gain.astype(f32).reshape(group_count, -1)
    mixed = (unit * gain_groups).reshape(tokens_here, -1).astype(bf16)
    mixed_line = lax.all_gather(mixed, SP[0], axis=0, tiled=True)

    columns_line = lax.all_to_all(grad_hidden, SP[0], 1, 0, tiled=True)
    outer = lax.dot_general(
        columns_line, mixed_line, (((0,), (0,)), ((), ())), preferred_element_type=f32
    )
    outer = lax.psum_scatter(outer, SP[1], scatter_dimension=0, tiled=True)
    grad_out_proj = lax.psum_scatter(outer, SP[2], scatter_dimension=0, tiled=True)

    grad_mixed = jnp.einsum("td,id->ti", grad_hidden, w_out, preferred_element_type=f32)
    grad_unit = grad_mixed.reshape(tokens_here, group_count, -1) * gain_groups
    grad_grouped = inv_rms * (grad_unit - unit * jnp.mean(grad_unit * unit, axis=-1, keepdims=True))
    grad_gated = grad_grouped.reshape(tokens_here, -1)
    grad_gate_in = (
        grad_gated
        * scan_out.reshape(tokens_here, -1)
        * gate_sig
        * (1.0 + gate_float * (1.0 - gate_sig))
    ).astype(bf16)
    grad_y = (grad_gated * gate_silu).reshape(tokens_here, head_count, HEAD_DIM)
    grad_y_b = grad_y.astype(bf16)
    grown_grads = (grad_y * growth[:, :, None]).reshape(
        tokens_here, group_count, per_group, HEAD_DIM
    )
    block_state = jnp.einsum("tgrp,tgn->grpn", grown_grads, c_float).reshape(
        expert_count, -1, STATE
    )
    rows = block_state.shape[1]
    each = expert_count // head_count
    last = jnp.repeat(cumulative[-1], each)
    sent = jnp.concatenate(
        [block_state, jnp.broadcast_to(last[:, None, None], (expert_count, 8, STATE))], axis=1
    )
    came_state = lax.all_to_all(sent, SP, 0, 0, tiled=True)
    states, lasts = came_state[:, :rows], came_state[:, rows, 0]
    through = jnp.cumsum(lasts)
    upto = jnp.concatenate([jnp.zeros((1,), f32), through[:-1]])
    blocks = jnp.arange(expert_count)
    gaps = upto[None, :] - through[:, None]
    carry = jnp.exp(jnp.where(blocks[None, :] > blocks[:, None], gaps, -jnp.inf))
    later_all = jnp.dot(
        carry, states.reshape(expert_count, -1), precision=lax.Precision.HIGHEST
    ).reshape(expert_count, rows, STATE)
    later_state = lax.all_to_all(later_all, SP, 0, 0, tiled=True)

    grad_x_inner = jnp.einsum("hts,thp->shp", mix_weights, grad_y_b, preferred_element_type=f32)
    grad_weights = (
        jnp.einsum("thp,shp->hts", grad_y_b, scan_heads, preferred_element_type=f32) * decay_mat
    )
    grad_weights = (
        grad_weights.reshape(group_count, per_group, tokens_here, tokens_here)
        .sum(axis=1)
        .astype(bf16)
    )
    grad_c_inner = jnp.einsum("gts,sgn->tgn", grad_weights, b_groups, preferred_element_type=f32)
    grad_b_inner = jnp.einsum("gts,tgn->sgn", grad_weights, c_groups, preferred_element_type=f32)
    grad_c_carry = jnp.einsum("tgrp,grpn->tgn", grown_grads, state_groups)
    x_tail = (x_float * tail_decay[:, :, None]).reshape(
        tokens_here, group_count, per_group, HEAD_DIM
    )
    later_groups = later_state.reshape(group_count, per_group, HEAD_DIM, STATE)
    grad_x_carry = jnp.einsum("sgn,grpn->sgrp", b_float, later_groups).reshape(
        tokens_here, head_count, HEAD_DIM
    )
    grad_x = grad_x_inner + grad_x_carry * tail_decay[:, :, None]
    grad_b_carry = jnp.einsum("sgrp,grpn->sgn", x_tail, later_groups)
    grad_a = jnp.sum(grad_y * scan_out, axis=2) - jnp.sum(x_float * grad_x, axis=2)
    suffix = jnp.flip(jnp.cumsum(jnp.flip(grad_a, 0), axis=0), 0)
    totals = lax.all_gather(suffix[0], SP)
    later_grad = jnp.sum(jnp.where(blocks[:, None] > sp, totals, 0.0), axis=0)
    grad_log_decay = suffix + later_grad[None, :]
    grad_scan_in = grad_x.reshape(tokens_here, -1).astype(bf16)
    grad_b_proj = (grad_b_inner + grad_b_carry).reshape(tokens_here, -1).astype(bf16)
    grad_c_proj = (grad_c_inner + grad_c_carry).reshape(tokens_here, -1).astype(bf16)
    return (
        gate_wgrad[None],
        up_wgrad[None],
        down_wgrad[None],
        grad_out_proj,
        grad_scan_in,
        grad_gate_in,
        grad_b_proj,
        grad_c_proj,
        grad_log_decay,
    )


def solution(mesh):
    split = Mesh(mesh.devices.reshape(4, 4, 4, mesh.shape["tp"]), ("sp_0", "sp_1", "sp_2", "tp"))
    return jax.shard_map(
        body,
        mesh=split,
        in_specs=(
            P(SP, None),
            P(SP, None),
            P(SP, None),
            P(SP, None),
            P(SP, None, "tp"),
            P(SP, None, "tp"),
            P(SP, None, "tp"),
            P(SP, None, "tp"),
            P(SP, "tp", None),
            P("tp", None),
            P("tp"),
            P(SP, "tp"),
            P(SP, "tp"),
            P(SP, "tp"),
            P(SP, "tp"),
            P(SP, "tp"),
            P(SP, "tp", None, None),
        ),
        out_specs=(
            P(SP, None, "tp"),
            P(SP, None, "tp"),
            P(SP, "tp", None),
            P(SP, "tp"),
            P(SP, "tp"),
            P(SP, "tp"),
            P(SP, "tp"),
            P(SP, "tp"),
            P(SP, "tp"),
        ),
        check_vma=False,
    )
```

time: 506 us -> 393 us (0.78); the launches traced: 497 us -> 392 us
  blocking collectives: 108 us -> 237 us
  local copies, waits for them, and re-layouts: 140 us -> 16.3 us
  waiting for transfers between devices: 129 us -> 45.7 us
  other arithmetic: 52.7 us -> 14.2 us
  starting transfers between devices: 11.5 us -> 25.1 us
    all_gather x5 -> x2, blocking collectives: 47.5 us -> 174 us  [the longest x1 171 us: body(): totals = lax.all_gather(suffix[0], SP)]
    scatter x2 -> x0, local copies, waits for them, and re-layouts: 92.2 us -> none  [the longest x1 46.1 us: body(): send_hidden = blank_slots.at[targets, ranked].set(mixer_output[token_of])]
    all_gather x7 -> x2, waiting for transfers between devices: 95.1 us -> 13.1 us  [the longest x1 7.05 us: body(): came = lax.all_gather(came, 'tp', axis=1, tiled=True)]
    reduce_sum x9 -> x1, other arithmetic: 20.4 us -> 0.75 us  [body(): later_grad = jnp.sum(jnp.where(blocks[:, None] > sp, totals, 0.0), axis=0)]
    all_to_all x1 -> x3, starting transfers between devices: 10.5 us -> 24.9 us  [the longest x1 10.7 us: exchanged(): lax.all_to_all(rows.reshape(expert_count, capacity, -1), SP, 0, 0, tiled=...]
    all_to_all x2 -> x3, blocking collectives: 49.6 us -> 62.9 us  [the longest x1 41.3 us: body(): came = lax.all_to_all(both, SP, 0, 0, tiled=True)]
    reduce_scatter x3 -> x2, waiting for transfers between devices: 12.5 us -> 0.01 us  [the longest x1 0.01 us: body(): outer = lax.psum_scatter(outer, SP[1], scatter_dimension=0, tiled=True)]
    all_to_all x1 -> x3, waiting for transfers between devices: 21.7 us -> 32.5 us  [the longest x1 15.7 us: exchanged(): lax.all_to_all(rows.reshape(expert_count, capacity, -1), SP, 0, 0, tiled=...]
  transfers between devices with their start and end apart: 11 -> 7, of which waited for: 10 -> 5; matrix products, arithmetic and copies ran while one was open for 21% -> 10% of each run, Pallas kernels for 0% -> 0%
where the time goes in v1:
time: 393 us; the launch traced here: 392 us
  blocking collectives  237 us (60%)
  waiting for transfers between devices  45.7 us (12%)
  matrix products  39.9 us (10%)
  starting transfers between devices  25.1 us (6%)
  local copies, waits for them, and re-layouts  16.3 us (4%)
  between operations  14.5 us (4%)
  other arithmetic  14.2 us (4%)
    all_gather x1, blocking collectives, body(): totals = lax.all_gather(suffix[0], SP)  171 us
    all_to_all x1, blocking collectives, body(): came = lax.all_to_all(both, SP, 0, 0, tiled=True)  41.3 us
    all_to_all x1, blocking collectives, body(): columns_line = lax.all_to_all(grad_hidden, SP[0], 1, 0, tiled=True)  16.2 us
    all_to_all x1, waiting for transfers between devices, exchanged(): lax.all_to_all(rows.reshape(expert_count, capacity, -1), SP, 0, 0, tiled=...  15.7 us
    all_to_all x1, starting transfers between devices, exchanged(): lax.all_to_all(rows.reshape(expert_count, capacity, -1), SP, 0, 0, tiled=...  10.7 us
    all_to_all x1, waiting for transfers between devices, body(): later_state = lax.all_to_all(later_all, SP, 0, 0, tiled=True)  8.53 us
    all_to_all x1, waiting for transfers between devices, body(): came_state = lax.all_to_all(sent, SP, 0, 0, tiled=True)  8.28 us
    unnamed x109, local copies, waits for them, and re-layouts  8.06 us
  transfers between devices with their start and end apart: 7, of which 5 were waited for; matrix products, arithmetic and copies ran while one was open for 10% of the time, Pallas kernels for 0%

profile of v1, /device:TPU:0, one launch (start us, length us, event | category | flops | bytes accessed | tf_op | source)
XLA Modules:
  0.0 392.4 jit_solution(3006423140785712156)
XLA Ops:
  7.2 0.8 slice_bitcast_fusion.7
  8.1 0.8 slice_bitcast_fusion.4
  9.0 0.8 fusion.107
  9.8 1.4 fusion.12
  11.2 1.1 fusion.44
  12.3 0.4 fusion.13
  13.1 41.3 %all_to_all.44 = bf16[64,16,1024]{2,1,0:T(8,128)(2,1)S(1)} all-to-all(bf16[64,16,1024]{2,1,0:T(8,128)(2,1)S(1)} %pad_maximum_fusion), channel_id=1, replica_groups=mesh['sp_0'=4,'sp_1'=4,'sp_2'=4,'tp'=2] {'sp_0','sp_1','sp_2'}, dimensions={0} | all-to-all | bytes 4194304 | tf_op jit(solution)/shard_map/all_to_all | solution.py:123
  54.5 1.5 pad_maximum_fusion.1
  56.1 0.6 copy-done.39
  56.7 0.6 mul.218
  57.3 0.6 convert_element_type.185
  58.2 0.6 slice_reduce_fusion.1
  58.8 0.6 subtract_exponential_fusion
  59.9 0.5 copy-done.8
  61.3 1.0 fusion.82
  62.3 7.1 %all-gather.4.cloned.1.call-done = bf16[1024,2048]{1,0:T(8,128)(2,1)} async-done(((bf16[1024,1024]{1,0:T(8,128)(2,1)}), bf16[1024,2048]{1,0:T(8,128)(2,1)}) %all-gather.4.cloned.1.call-update) | async-done | bytes 4194320 | tf_op jit(solution)/shard_map/all_gather | solution.py:131
  69.4 4.1 %select_convert_fusion = (bf16[512,512]{1,0:T(8,128)(2,1)S(1)}, f32[512,512]{1,0:T(8,128)S(1)}) fusion(bf16[1,512,512]{2,1,0:T(8,128)(2,1)} %param.22, bf16[1,512,512]{2,1,0:T(8,128)(2,1)} %param.21, bf16[1,512,2048]{2,1,0:T(8,128)(2,1)} %param.25, bf16[1024,2048]{1,0:T(8,128)(2,1)} %all-gather.4.cloned.1.call-done), kind=kOutput, calls=%fused_computation.69 | convolution fusion | flops 1077411840 | bytes 6815744 | tf_op jit(solution)/shard_map/rd,fd->rf/dot_general | solution.py:18
  73.6 1.7 fusion.4
  75.3 0.4 copy-done.3
  75.7 1.3 add_convert_fusion
  77.2 5.4 %all_to_all.45 = bf16[2,512,1024]{2,1,0:T(8,128)(2,1)S(1)} all-to-all(bf16[2,512,1024]{2,1,0:T(8,128)(2,1)S(1)} %bitcast.233), channel_id=1, replica_groups=mesh['sp_0'=4,'sp_1'=4,'sp_2'=4,'tp'=2] {'tp'}, dimensions={0} | all-to-all | bytes 4194304 | tf_op jit(solution)/shard_map/all_to_all | solution.py:137
  82.6 1.4 fusion.38
  84.0 10.7 %all-to-all-start.2 = ((bf16[64,8,1024]{2,1,0:T(8,128)(2,1)}), bf16[64,8,1024]{2,1,0:T(8,128)(2,1)}, u32[]{:S(2)}, u32[]{:S(2)}) async-start(bf16[64,8,1024]{2,1,0:T(8,128)(2,1)} %fusion.38), calls=%async_computation.2 | async-start | bytes 2097152 | tf_op jit(solution)/shard_map/all_to_all | solution.py:112
  94.8 0.5 fusion.14
  96.3 0.6 copy-done.19
  97.1 0.9 copy.154
  98.0 15.7 %all-to-all-done.2 = bf16[64,8,1024]{2,1,0:T(8,128)(2,1)} async-done(((bf16[64,8,1024]{2,1,0:T(8,128)(2,1)}), bf16[64,8,1024]{2,1,0:T(8,128)(2,1)}, u32[]{:S(2)}, u32[]{:S(2)}) %all-to-all-start.2) | async-done | bytes 1048608 | tf_op jit(solution)/shard_map/all_to_all | solution.py:112
  113.7 1.6 fusion.16
  115.3 2.4 all_gather.13
  117.7 3.7 fusion.119
  121.4 1.0 reshape.235
  122.4 1.5 multiply_reduce_fusion.2
  124.3 1.2 fusion.51
  125.6 16.2 %all_to_all.46 = bf16[128,4,512]{2,0,1:T(8,128)(2,1)S(1)} all-to-all(bf16[128,4,512]{2,0,1:T(8,128)(2,1)S(1)} %bitcast.249), channel_id=1, replica_groups=mesh['sp_0'=4,'sp_1'=4,'sp_2'=4,'tp'=2] {'sp_0'}, dimensions={1} | all-to-all | bytes 1048576 | tf_op jit(solution)/shard_map/all_to_all | solution.py:181
  141.7 6.0 %all-gather.6.cloned.1.call-done = bf16[512,1024]{1,0:T(8,128)(2,1)} async-done(((bf16[128,1024]{1,0:T(8,128)(2,1)}), bf16[512,1024]{1,0:T(8,128)(2,1)}) %all-gather.6.cloned.1.call-update) | async-done | bytes 1048592 | tf_op jit(solution)/shard_map/all_gather | solution.py:179
  147.8 3.4 fusion.118
  151.6 0.5 iota_compare_fusion.9
  152.2 0.7 subtract_exponential_fusion.1
  152.9 4.4 %fusion.1 = bf16[1,2048,512]{2,1,0:T(8,128)(2,1)} fusion(bf16[512,512]{1,0:T(8,128)(2,1)S(1)} %copy-done.21, bf16[1024,2048]{1,0:T(8,128)(2,1)} %all-gather.4.cloned.1.call-done), kind=kOutput, calls=%fused_computation.5 | convolution fusion | flops 1074790400 | bytes 4718592 | tf_op jit(solution)/shard_map/rd,rf->df/dot_general | solution.py:39
  157.2 2.9 fusion
  160.7 0.9 pad_maximum_fusion.2
  161.6 7.1 %all-to-all-start.4 = ((f32[64,24,128]{2,1,0:T(8,128)}), f32[64,24,128]{2,1,0:T(8,128)S(1)}, u32[]{:S(2)}, u32[]{:S(2)}) async-start(f32[64,24,128]{2,1,0:T(8,128)} %pad_maximum_fusion.2), calls=%async_computation.6 | async-start | bytes 1572864 | tf_op jit(solution)/shard_map/all_to_all | solution.py:212
  168.8 4.9 %fusion.2 = bf16[1,512,2048]{2,1,0:T(8,128)(2,1)} fusion(bf16[1024,2048]{1,0:T(8,128)(2,1)} %all-gather.4.cloned.1.call-done, bf16[1,512,512]{2,1,0:T(8,128)(2,1)} %param.22, bf16[1,512,512]{2,1,0:T(8,128)(2,1)} %param.21), kind=kOutput, calls=%fused_computation.6 | convolution fusion | flops 1077936128 | bytes 5242880 | tf_op jit(solution)/shard_map/rf,rd->fd/dot_general | solution.py:33
  173.6 1.0 convolution_bitcast_fusion.2
  174.6 0.5 bitcast_reduce_fusion
  175.2 8.3 %all-to-all-done.4 = f32[64,24,128]{2,1,0:T(8,128)S(1)} async-done(((f32[64,24,128]{2,1,0:T(8,128)}), f32[64,24,128]{2,1,0:T(8,128)S(1)}, u32[]{:S(2)}, u32[]{:S(2)}) %all-to-all-start.4) | async-done | bytes 786464 | tf_op jit(solution)/shard_map/all_to_all | solution.py:212
  183.7 0.5 copy-done.24
  184.2 0.9 slice_reduce_fusion
  185.2 0.7 fusion.53
  186.0 0.9 copy.128
  186.8 7.1 %all-to-all-start.5 = ((bf16[64,16,128]{2,1,0:T(8,128)(2,1)}), bf16[64,16,128]{2,1,0:T(8,128)(2,1)S(1)}, u32[]{:S(2)}, u32[]{:S(2)}) async-start(bf16[64,16,128]{2,1,0:T(8,128)(2,1)} %copy.128), calls=%async_computation.7 | async-start | bytes 524288 | tf_op jit(solution)/shard_map/all_to_all | solution.py:222
  194.0 1.2 fusion.19
  195.2 0.8 copy.138
  196.1 8.5 %all-to-all-done.5 = bf16[64,16,128]{2,1,0:T(8,128)(2,1)S(1)} async-done(((bf16[64,16,128]{2,1,0:T(8,128)(2,1)}), bf16[64,16,128]{2,1,0:T(8,128)(2,1)S(1)}, u32[]{:S(2)}, u32[]{:S(2)}) %all-to-all-start.5) | async-done | bytes 262176 | tf_op jit(solution)/shard_map/all_to_all | solution.py:222
  204.6 0.7 copy-done.2
  205.5 0.9 bitcast_multiply_fusion.1
  206.4 2.2 multiply_reduce_fusion
  209.0 171.5 %all-gather = f32[64,1,16]{2,1,0:T(1,128)S(1)} all-gather(f32[1,1,16]{2,1,0:T(1,128)S(1)} %slice_bitcast_fusion.2), channel_id=1, replica_groups=mesh['sp_0'=4,'sp_1'=4,'sp_2'=4,'tp'=2] {'sp_0','sp_1','sp_2'}, dimensions={0}, use_global_device_ids=true | all-gather | bytes 4160 | tf_op jit(solution)/shard_map/all_gather | solution.py:247
  380.5 0.7 select_reduce_fusion
  381.2 0.7 copy.139
  381.9 1.2 convolution_bitcast_fusion.3
  383.1 1.1 fusion.18
  384.2 0.8 copy.137
  385.0 0.8 copy.136
  (154 shorter events, 6.3 us)
Async XLA Ops:
  7.2 66.4 %copy-start = (bf16[1,2048,512]{2,1,0:T(8,128)(2,1)S(1)}, bf16[1,2048,512]{2,1,0:T(8,128)(2,1)}, u32[]{:S(2)}) copy-start(bf16[1,2048,512]{2,1,0:T(8,128)(2,1)} %param.23) | copy-start | bytes 6291460
  7.2 62.2 %all-gather.4.cloned.1.call-start = ((), (), s32[]{:S(2)}) async-start(), calls=%async_computation.8 | async-start | bytes 6291456 | tf_op jit(solution)/shard_map/all_gather | solution.py:131
  9.8 3.0 copy-start.34
  9.8 3.0 copy-start.36
  56.0 0.7 copy-start.39
  56.0 1.9 copy-start.38
  56.0 3.4 copy-start.27
  56.0 3.6 copy-start.28
  56.0 4.4 %copy-start.26 = (bf16[128,1024]{1,0:T(8,128)(2,1)S(1)}, bf16[128,1024]{1,0:T(8,128)(2,1)}, u32[]{:S(2)}) copy-start(bf16[128,1024]{1,0:T(8,128)(2,1)} %param.28) | copy-start | bytes 786436
  56.7 4.6 %copy-start.4 = (f32[1,16,64,128]{3,2,1,0:T(8,128)S(1)}, f32[1,16,64,128]{3,2,1,0:T(8,128)}, u32[]{:S(2)}) copy-start(f32[1,16,64,128]{3,2,1,0:T(8,128)} %param.33) | copy-start | bytes 1572868
  58.2 1.7 copy-start.14
  58.7 0.8 copy-start.40
  59.7 1.0 copy-start.10
  59.7 0.7 copy-start.8
  59.9 0.8 copy-start.12
  60.7 0.6 copy-start.29
  62.3 11.2 %copy-start.44 = (bf16[1,512,512]{2,1,0:T(8,128)(2,1)S(1)}, bf16[1,512,512]{2,1,0:T(8,128)(2,1)}, u32[]{:S(2)}) copy-start(bf16[1,512,512]{2,1,0:T(8,128)(2,1)} %param.21) | copy-start | bytes 1572868
  69.4 4.2 %copy-start.46 = (bf16[1,512,512]{2,1,0:T(8,128)(2,1)S(1)}, bf16[1,512,512]{2,1,0:T(8,128)(2,1)}, u32[]{:S(2)}) copy-start(bf16[1,512,512]{2,1,0:T(8,128)(2,1)} %param.22) | copy-start | bytes 1572868
  73.5 1.8 copy-start.48
  73.5 1.8 copy-start.20
  73.6 2.1 copy-start.3
  82.6 12.1 %copy-start.6 = (f32[4,4,64,128]{3,2,1,0:T(8,128)S(1)}, f32[4,4,64,128]{3,2,1,0:T(8,128)}, u32[]{:S(2)}) copy-start(f32[4,4,64,128]{3,2,1,0:T(8,128)} %fusion.82) | copy-start | bytes 1572868
  84.0 29.7 %all-to-all-start.2 = ((bf16[64,8,1024]{2,1,0:T(8,128)(2,1)}), bf16[64,8,1024]{2,1,0:T(8,128)(2,1)}, u32[]{:S(2)}, u32[]{:S(2)}) async-start(bf16[64,8,1024]{2,1,0:T(8,128)(2,1)} %fusion.38), calls=%async_computation.2 | async-start | bytes 2097152 | tf_op jit(solution)/shard_map/all_to_all | solution.py:112
  94.7 1.0 copy-start.16
  94.7 53.1 %all-gather.6.cloned.1.call-start = ((), (), s32[]{:S(2)}) async-start(), calls=%async_computation.9 | async-start | bytes 1310720 | tf_op jit(solution)/shard_map/all_gather | solution.py:179
  95.6 18.1 %copy-start.35 = (s32[128]{0:T(128)S(1)}, s32[128]{0:T(128)}, u32[]{:S(2)}) copy-start(s32[128]{0:T(128)} %copy-done.34) | copy-start | bytes 1540
  95.6 18.1 %copy-start.37 = (s32[128]{0:T(128)S(1)}, s32[128]{0:T(128)}, u32[]{:S(2)}) copy-start(s32[128]{0:T(128)} %copy-done.36) | copy-start | bytes 1540
  95.8 17.9 %copy-start.23 = (bf16[128,2048]{1,0:T(8,128)(2,1)S(1)}, bf16[128,2048]{1,0:T(8,128)(2,1)}, u32[]{:S(2)}) copy-start(bf16[128,2048]{1,0:T(8,128)(2,1)} %param.18) | copy-start | bytes 1572868
  96.3 0.6 copy-start.19
  117.7 4.8 %copy-start.33 = (f32[4,256]{1,0:T(4,128)S(1)}, f32[4,256]{1,0:T(4,128)}, u32[]{:S(2)}) copy-start(f32[4,256]{1,0:T(4,128)} %mul.218) | copy-start | bytes 12292
  121.4 2.9 copy-start.32
  122.4 1.8 copy-start.7
  122.4 1.8 copy-start.17
  125.5 80.9 %reduce-scatter.3.cloned.1.call-start = ((), (), s32[]{:S(2)}) async-start(), calls=%async_computation.10 | async-start | bytes 2621440 | tf_op jit(solution)/shard_map/reduce_scatter | solution.py:185
  147.8 3.4 copy-start.15
  147.8 3.5 copy-start.42
  147.8 3.6 copy-start.41
  147.8 3.8 copy-start.25
  147.8 5.0 %copy-start.21 = (bf16[512,512]{1,0:T(8,128)(2,1)S(1)}, bf16[512,512]{1,0:T(8,128)(2,1)}, u32[]{:S(2)}) copy-start(bf16[512,512]{1,0:T(8,128)(2,1)} %copy-done.20) | copy-start | bytes 1572868
  152.8 4.4 %copy-start.43 = (bf16[1024,2048]{1,0:T(8,128)(2,1)S(1)}, bf16[1024,2048]{1,0:T(8,128)(2,1)}, u32[]{:S(2)}) copy-start(bf16[1024,2048]{1,0:T(8,128)(2,1)} %all-gather.4.cloned.1.call-done) | copy-start | bytes 12582916
  152.8 4.4 %copy-start.45 = (bf16[1,512,512]{2,1,0:T(8,128)(2,1)S(1)}, bf16[1,512,512]{2,1,0:T(8,128)(2,1)}, u32[]{:S(2)}) copy-start(bf16[1,512,512]{2,1,0:T(8,128)(2,1)} %param.21) | copy-start | bytes 1572868
  152.8 4.4 %copy-start.47 = (bf16[1,512,512]{2,1,0:T(8,128)(2,1)S(1)}, bf16[1,512,512]{2,1,0:T(8,128)(2,1)}, u32[]{:S(2)}) copy-start(bf16[1,512,512]{2,1,0:T(8,128)(2,1)} %param.22) | copy-start | bytes 1572868
  152.9 4.4 %copy-start.49 = (f32[512,512]{1,0:T(8,128)S(1)}, f32[512,512]{1,0:T(8,128)}, u32[]{:S(2)}) copy-start(f32[512,512]{1,0:T(8,128)} %copy-done.48) | copy-start | bytes 3145732
  161.6 21.8 %all-to-all-start.4 = ((f32[64,24,128]{2,1,0:T(8,128)}), f32[64,24,128]{2,1,0:T(8,128)S(1)}, u32[]{:S(2)}, u32[]{:S(2)}) async-start(f32[64,24,128]{2,1,0:T(8,128)} %pad_maximum_fusion.2), calls=%async_computation.6 | async-start | bytes 1572864 | tf_op jit(solution)/shard_map/all_to_all | solution.py:212
  168.8 4.9 %copy-start.5 = (f32[1,16,64,128]{3,2,1,0:T(8,128)S(1)}, f32[1,16,64,128]{3,2,1,0:T(8,128)}, u32[]{:S(2)}) copy-start(f32[1,16,64,128]{3,2,1,0:T(8,128)} %param.33) | copy-start | bytes 1572868
  168.8 5.8 %copy-start.30 = (pred[128,128]{1,0:T(8,128)(4,1)S(1)}, pred[128,128]{1,0:T(8,128)(4,1)}, u32[]{:S(2)}) copy-start(pred[128,128]{1,0:T(8,128)(4,1)} %copy-done.29) | copy-start | bytes 49156
  174.6 19.4 %copy-start.13 = (bf16[128,4,128]{0,2,1:T(8,128)(2,1)S(1)}, bf16[128,4,128]{0,2,1:T(8,128)(2,1)}, u32[]{:S(2)}) copy-start(bf16[128,4,128]{0,2,1:T(8,128)(2,1)} %copy-done.12) | copy-start | bytes 393220
  175.2 20.9 %copy-start.22 = (bf16[4,128,128]{2,1,0:T(8,128)(2,1)}, bf16[4,128,128]{2,1,0:T(8,128)(2,1)S(1)}, u32[]{:S(2)}) copy-start(bf16[4,128,128]{2,1,0:T(8,128)(2,1)S(1)} %bitcast_reduce_fusion) | copy-start | bytes 393220
  183.6 0.6 copy-start.24
  184.2 21.1 %copy-start.9 = (bf16[128,4,128]{2,1,0:T(4,128)(2,1)S(1)}, bf16[128,4,128]{2,1,0:T(4,128)(2,1)}, u32[]{:S(2)}) copy-start(bf16[128,4,128]{2,1,0:T(4,128)(2,1)} %copy-done.8) | copy-start | bytes 393220
  186.8 17.8 %all-to-all-start.5 = ((bf16[64,16,128]{2,1,0:T(8,128)(2,1)}), bf16[64,16,128]{2,1,0:T(8,128)(2,1)S(1)}, u32[]{:S(2)}, u32[]{:S(2)}) async-start(bf16[64,16,128]{2,1,0:T(8,128)(2,1)} %copy.128), calls=%async_computation.7 | async-start | bytes 524288 | tf_op jit(solution)/shard_map/all_to_all | solution.py:222
  194.0 191.9 %reduce-scatter.5.cloned.1.call-start = ((), (), s32[]{:S(2)}) async-start(), calls=%async_computation.11 | async-start | bytes 655360 | tf_op jit(solution)/shard_map/reduce_scatter | solution.py:186
  204.6 0.7 copy-start.2
  206.4 175.5 %copy-start.31 = (f32[128,4,4]{0,2,1:T(4,128)S(1)}, f32[128,4,4]{0,2,1:T(4,128)}, u32[]{:S(2)}) copy-start(f32[128,4,4]{0,2,1:T(4,128)} %get-tuple-element.60) | copy-start | bytes 24580
  206.4 176.7 %copy-start.11 = (bf16[128,4,128]{0,2,1:T(8,128)(2,1)S(1)}, bf16[128,4,128]{0,2,1:T(8,128)(2,1)}, u32[]{:S(2)}) copy-start(bf16[128,4,128]{0,2,1:T(8,128)(2,1)} %copy-done.10) | copy-start | bytes 393220
  206.4 179.4 %copy-start.1 = (bf16[1,2048,512]{2,1,0:T(8,128)(2,1)S(1)}, bf16[1,2048,512]{2,1,0:T(8,128)(2,1)}, u32[]{:S(2)}) copy-start(bf16[1,2048,512]{2,1,0:T(8,128)(2,1)} %param.23) | copy-start | bytes 6291460
  208.6 176.4 %copy-start.18 = (bf16[128,16,64]{0,2,1:T(8,128)(2,1)S(1)}, bf16[128,16,64]{0,2,1:T(8,128)(2,1)}, u32[]{:S(2)}) copy-start(bf16[128,16,64]{0,2,1:T(8,128)(2,1)} %get-tuple-element.53) | copy-start | bytes 786436
Sparse Core Ops, SparseCore 0:
  56.2 13.1 all-gather.3
  125.6 22.1 all-gather.5
  151.3 36.1 reduce-scatter.2
  206.5 17.3 reduce-scatter.4

commit v2 on v1

--- a/solution.py
+++ b/solution.py
@@ -1,6 +1,8 @@
 import jax
 import jax.numpy as jnp
 from jax import lax
+from jax.experimental import pallas as pl
+from jax.experimental.pallas import tpu as pltpu
 from jax.sharding import Mesh
 from jax.sharding import PartitionSpec as P
 
@@ -14,58 +16,292 @@
 swish_alpha = 1.702
 
 
-def expert_side(hidden_rows, grad_rows, gate_value, up_value, gate_weight, up_weight, down_weight):
-    act_grad = jnp.einsum("rd,fd->rf", grad_rows, down_weight, preferred_element_type=jnp.float32)
-    gate_full = gate_value.astype(jnp.float32)
-    up_full = up_value.astype(jnp.float32)
-    gate_clip = jnp.minimum(gate_full, clamp_limit)
-    up_clip = jnp.clip(up_full, -clamp_limit, clamp_limit)
-    sigmoid_gate = jax.nn.sigmoid(swish_alpha * gate_clip)
-    swish_gate = gate_clip * sigmoid_gate
-    active = ((up_clip + 1.0) * swish_gate).astype(jnp.bfloat16)
-    up_grad = jnp.where(
-        (up_full > -clamp_limit) & (up_full < clamp_limit), act_grad * swish_gate, 0.0
-    ).astype(jnp.bfloat16)
-    slope = sigmoid_gate + swish_alpha * gate_clip * sigmoid_gate * (1.0 - sigmoid_gate)
-    gate_grad = jnp.where(gate_full < clamp_limit, act_grad * (up_clip + 1.0) * slope, 0.0).astype(
-        jnp.bfloat16
-    )
-    down_wgrad = jnp.einsum(
-        "rf,rd->fd", active, grad_rows, preferred_element_type=jnp.float32
-    ).astype(jnp.bfloat16)
-    gate_wgrad = jnp.einsum(
-        "rd,rf->df", hidden_rows, gate_grad, preferred_element_type=jnp.float32
-    ).astype(jnp.bfloat16)
-    up_wgrad = jnp.einsum(
-        "rd,rf->df", hidden_rows, up_grad, preferred_element_type=jnp.float32
-    ).astype(jnp.bfloat16)
-    partial_rows = jnp.einsum(
-        "rf,df->rd", gate_grad, gate_weight, preferred_element_type=jnp.float32
-    )
-    partial_rows = partial_rows + jnp.einsum(
-        "rf,df->rd", up_grad, up_weight, preferred_element_type=jnp.float32
-    )
-    return (gate_wgrad, up_wgrad, down_wgrad, partial_rows)
-
-
-def slot_rows(expert_choice, expert_count, capacity):
-    choice = expert_choice.T
-    tokens = choice.shape[1]
-    experts = lax.broadcasted_iota(jnp.int32, (expert_count, tokens), 0)
-    hots = [(experts == choice[k][None, :]) for k in range(choice.shape[0])]
-    named = sum(h.astype(jnp.bfloat16) for h in hots)
-    before = (
+f32, bf16 = jnp.float32, jnp.bfloat16
+MESH_ID = pl.DeviceIdType.MESH
+NT = (((1,), (1,)), ((), ()))
+NN = (((1,), (0,)), ((), ()))
+TN = (((0,), (0,)), ((), ()))
+
+
+def dotf(a, b, dims=NN):
+    return lax.dot_general(a, b, dims, preferred_element_type=f32)
+
+
+def place():
+    z, y, x = (lax.axis_index(a) for a in SP)
+    return z, y, x, z * 16 + y * 4 + x
+
+
+def peer_of(k):
+    z, y, x, _ = place()
+    pz = lax.rem(z + k // 16, 4)
+    py = lax.rem(y + lax.rem(k // 4, 4), 4)
+    px = lax.rem(x + lax.rem(k, 4), 4)
+    return {SP[0]: pz, SP[1]: py, SP[2]: px}, pz * 16 + py * 4 + px
+
+
+def greet(others):
+    barrier = pltpu.get_barrier_semaphore()
+
+    def one(k, _):
+        device, _i = peer_of(k)
+        pl.semaphore_signal(barrier, inc=1, device_id=device, device_id_type=MESH_ID)
+        return 0
+
+    lax.fori_loop(1, others, one, 0)
+    partner = {"tp": 1 - lax.axis_index("tp")}
+    pl.semaphore_signal(barrier, inc=1, device_id=partner, device_id_type=MESH_ID)
+
+
+def greeted(others):
+    pl.semaphore_wait(pltpu.get_barrier_semaphore(), others)
+
+
+def push(src, dst, send, recv, device):
+    pltpu.make_async_remote_copy(
+        src_ref=src, dst_ref=dst, send_sem=send, recv_sem=recv,
+        device_id=device, device_id_type=MESH_ID,
+    ).start()
+
+
+def took(ref, sem):
+    pltpu.make_async_copy(ref, ref, sem).wait()
+
+
+def moe_kernel(
+    mixer, cot, choice, weight, gate, up, wg_h, wu_h, wd_h,
+    gwg_o, gwu_o, gwd_o, gh_o,
+    wg, wu, wd, send_g, send_h, recv_g, recv_h, oth_g, oth_h, grads, hidden,
+    fu, fg, act, acc, gg, ug, psend, precv, pown, rsend, rrecv, hot, gwg, gwu, gwd,
+    wsem, lsem, sg, rg, sh, rh, dsg, drg, dsh, drh, dsp, drp, sr, rr, lr, dso, drout, osem,
+):
+    n = recv_g.shape[0]
+    cap = recv_g.shape[1]
+    half = recv_g.shape[2]
+    tokens = mixer.shape[0]
+    z, y, x, me = place()
+    tp = lax.axis_index("tp")
+    partner = {"tp": 1 - tp}
+    mine = pl.ds(pl.multiple_of(tp * half, half), half)
+    theirs = pl.ds(pl.multiple_of((1 - tp) * half, half), half)
+    greet(n)
+    loads = [
+        pltpu.make_async_copy(a, b, wsem.at[i])
+        for i, (a, b) in enumerate(((wd_h, wd), (wg_h, wg), (wu_h, wu)))
+    ]
+    for c in loads:
+        c.start()
+    experts = lax.broadcasted_iota(jnp.int32, (n, tokens), 0)
+    hits = [experts == choice[k : k + 1, :] for k in range(2)]
+    named = jnp.where(hits[0] | hits[1], 1.0, 0.0).astype(bf16)
+    before = jnp.where(
         lax.broadcasted_iota(jnp.int32, (tokens, tokens), 0)
-        < lax.broadcasted_iota(jnp.int32, (tokens, tokens), 1)
-    ).astype(jnp.bfloat16)
-    earlier = jnp.dot(named, before, preferred_element_type=jnp.float32)
-    places = lax.broadcasted_iota(jnp.int32, (expert_count * capacity, tokens), 0)
-    out = []
-    for k, hot in enumerate(hots):
-        rank = jnp.sum(jnp.where(hot, earlier, 0.0), axis=0).astype(jnp.int32)
-        slot = choice[k] * capacity + rank
-        out.append((places == slot[None, :]).astype(jnp.bfloat16))
-    return out
+        < lax.broadcasted_iota(jnp.int32, (tokens, tokens), 1),
+        1.0, 0.0,
+    ).astype(bf16)
+    earlier = dotf(named, before)
+    places = lax.broadcasted_iota(jnp.int32, (n * cap, tokens), 0)
+    hots = []
+    for k in range(2):
+        rank = jnp.sum(jnp.where(hits[k], earlier, 0.0), axis=0, keepdims=True)
+        slot = choice[k : k + 1, :] * cap + rank.astype(jnp.int32)
+        hots.append(jnp.where(places == slot, 1.0, 0.0).astype(bf16))
+    hot[...] = hots[0] + hots[1]
+    cot_half = cot[:, mine].astype(f32)
+    rows0 = (weight[:, 0:1] * cot_half).astype(bf16)
+    rows1 = (weight[:, 1:2] * cot_half).astype(bf16)
+    packed = dotf(hots[0], rows0) + dotf(hots[1], rows1)
+    send_g[...] = packed.reshape(n, cap, half).astype(bf16)
+    packed = dotf(hot[...], mixer[:, mine])
+    send_h[...] = packed.reshape(n, cap, half).astype(bf16)
+    greeted(n)
+
+    own = []
+    for src, dst, sem in ((send_g, recv_g, rg), (send_h, recv_h, rh)):
+        own.append(pltpu.make_async_copy(src.at[me], dst.at[me], sem.at[z]))
+
+    def sends(src, dst, send, recv):
+        def one(k, _):
+            device, i = peer_of(k)
+            push(src.at[i], dst.at[me], send, recv.at[z], device)
+            return 0
+
+        lax.fori_loop(1, n, one, 0)
+
+    own[0].start()
+    sends(send_g, recv_g, sg, rg)
+    own[1].start()
+    sends(send_h, recv_h, sh, rh)
+
+    def prepare(i, _):
+        rows = pl.ds(pl.multiple_of(i * 64, 64), 64)
+        gate_full = gate[rows, :].astype(f32)
+        up_full = up[rows, :].astype(f32)
+        gate_clip = jnp.minimum(gate_full, clamp_limit)
+        up_clip = jnp.clip(up_full, -clamp_limit, clamp_limit)
+        sig = jax.nn.sigmoid(swish_alpha * gate_clip)
+        swish = gate_clip * sig
+        act[rows, :] = ((up_clip + 1.0) * swish).astype(bf16)
+        inside = (up_full > -clamp_limit) & (up_full < clamp_limit)
+        fu[rows, :] = jnp.where(inside, swish, 0.0)
+        slope = sig + swish_alpha * gate_clip * sig * (1.0 - sig)
+        fg[rows, :] = jnp.where(gate_full < clamp_limit, (up_clip + 1.0) * slope, 0.0)
+        return 0
+
+    lax.fori_loop(0, gate.shape[0] // 64, prepare, 0)
+    for c in loads:
+        c.wait()
+
+    per = n // 4
+    rowsof = per * cap
+
+    def plane(i):
+        q = lax.rem(z - i + 4, 4)
+        blocks = pl.ds(pl.multiple_of(q * per, per), per)
+        return q, blocks, pl.ds(pl.multiple_of(q * rowsof, rowsof), rowsof)
+
+    def flat(ref, blocks):
+        return ref[blocks].astype(f32).reshape(rowsof, half).astype(bf16)
+
+    def arrive(i, _):
+        q, blocks, rows = plane(i)
+        took(recv_g.at[blocks], rg.at[q])
+        push(recv_g.at[blocks], oth_g.at[blocks], dsg, drg.at[q], partner)
+        g = flat(recv_g, blocks)
+        grads[rows, mine] = g
+        acc[rows, :] = dotf(g, wd[:, mine], NT)
+        return 0
+
+    lax.fori_loop(0, 4, arrive, 0)
+
+    def expert(i, _):
+        q, blocks, rows = plane(i)
+        took(oth_g.at[blocks], drg.at[q])
+        g = flat(oth_g, blocks)
+        grads[rows, theirs] = g
+        act_grad = acc[rows, :] + dotf(g, wd[:, theirs], NT)
+        up_grad = (act_grad * fu[rows, :]).astype(bf16)
+        gate_grad = (act_grad * fg[rows, :]).astype(bf16)
+        ug[rows, :] = up_grad
+        gg[rows, :] = gate_grad
+        part = dotf(gate_grad, wg[theirs, :], NT) + dotf(up_grad, wu[theirs, :], NT)
+        psend[rows, :] = part.astype(bf16)
+        push(psend.at[rows], precv.at[rows], dsp, drp.at[q], partner)
+        part = dotf(gate_grad, wg[mine, :], NT) + dotf(up_grad, wu[mine, :], NT)
+        pown[rows, :] = part.astype(bf16)
+        return 0
+
+    lax.fori_loop(0, 4, expert, 0)
+
+    def give_back(i, _):
+        q, blocks, rows = plane(i)
+        took(precv.at[rows], drp.at[q])
+        total = pown[rows, :].astype(f32) + precv[rows, :].astype(f32)
+        rsend[blocks] = total.reshape(per, cap, half).astype(bf16)
+
+        def one(k, _):
+            device, j = peer_of(lax.rem(4 - i, 4) * per + k)
+            push(rsend.at[j], rrecv.at[me], sr, rr, device)
+            return 0
+
+        lax.fori_loop(jnp.where(i == 0, 1, 0), per, one, 0)
+        return 0
+
+    lax.fori_loop(0, 4, give_back, 0)
+    back = pltpu.make_async_copy(rsend.at[me], rrecv.at[me], rr)
+    back.start()
+
+    def down(i, _):
+        cols = pl.ds(pl.multiple_of(i * 512, 512), 512)
+        gwd[:, cols] = dotf(act[...], grads[:, cols], TN).astype(bf16)
+        pltpu.make_async_copy(gwd.at[:, cols], gwd_o.at[:, cols], osem.at[0]).start()
+        return 0
+
+    lax.fori_loop(0, grads.shape[1] // 512, down, 0)
+
+    def arrive_h(i, _):
+        q, blocks, rows = plane(i)
+        took(recv_h.at[blocks], rh.at[q])
+        push(recv_h.at[blocks], oth_h.at[blocks], dsh, drh.at[q], partner)
+        hidden[rows, mine] = flat(recv_h, blocks)
+        return 0
+
+    lax.fori_loop(0, 4, arrive_h, 0)
+
+    def other_h(i, _):
+        q, blocks, rows = plane(i)
+        took(oth_h.at[blocks], drh.at[q])
+        hidden[rows, theirs] = flat(oth_h, blocks)
+        return 0
+
+    lax.fori_loop(0, 4, other_h, 0)
+
+    def wide(i, _):
+        cols = pl.ds(pl.multiple_of(i * 512, 512), 512)
+        h = hidden[:, cols]
+        gwg[cols, :] = dotf(h, gg[...], TN).astype(bf16)
+        pltpu.make_async_copy(gwg.at[cols], gwg_o.at[cols], osem.at[1]).start()
+        gwu[cols, :] = dotf(h, ug[...], TN).astype(bf16)
+        pltpu.make_async_copy(gwu.at[cols], gwu_o.at[cols], osem.at[2]).start()
+        return 0
+
+    lax.fori_loop(0, hidden.shape[1] // 512, wide, 0)
+
+    took(rrecv, rr)
+    r = rrecv[...].astype(f32).reshape(n * cap, half).astype(bf16)
+    moe = dotf(hot[...], r, TN)
+    gh_o[:, mine] = (cot[:, mine].astype(f32) + moe).astype(bf16)
+    push(gh_o.at[:, mine], gh_o.at[:, mine], dso, drout, partner)
+    took(gh_o.at[:, theirs], drout)
+    took(gh_o.at[:, mine], dso)
+    most = pl.ds(0, n - 1)
+    took(send_g.at[most], sg)
+    took(send_h.at[most], sh)
+    took(rsend.at[most], sr)
+    took(recv_g, dsg)
+    took(recv_h, dsh)
+    took(psend, dsp)
+    took(gwd, osem.at[0])
+    took(gwg, osem.at[1])
+    took(gwu, osem.at[2])
+
+
+def moe_side(mixer, cot, choice, weight, gate, up, wg, wu, wd):
+    n = lax.axis_size(SP)
+    tokens, width = mixer.shape
+    slots, hid = gate.shape
+    cap, half = slots // n, width // 2
+    dma = pltpu.SemaphoreType.DMA
+    vm = lambda *s: pltpu.VMEM(s, bf16)
+    vf = lambda *s: pltpu.VMEM(s, f32)
+    inv = pl.BlockSpec(memory_space=pltpu.VMEM)
+    anyv = pl.BlockSpec(memory_space=pl.ANY)
+    return pl.pallas_call(
+        moe_kernel,
+        out_shape=(
+            jax.ShapeDtypeStruct((width, hid), bf16),
+            jax.ShapeDtypeStruct((width, hid), bf16),
+            jax.ShapeDtypeStruct((hid, width), bf16),
+            jax.ShapeDtypeStruct((tokens, width), bf16),
+        ),
+        in_specs=[inv] * 6 + [anyv] * 3,
+        out_specs=(anyv, anyv, anyv, inv),
+        scratch_shapes=[
+            vm(width, hid), vm(width, hid), vm(hid, width),
+            vm(n, cap, half), vm(n, cap, half), vm(n, cap, half), vm(n, cap, half),
+            vm(n, cap, half), vm(n, cap, half), vm(slots, width), vm(slots, width),
+            vf(slots, hid), vf(slots, hid), vm(slots, hid), vf(slots, hid),
+            vm(slots, hid), vm(slots, hid), vm(slots, half), vm(slots, half), vm(slots, half),
+            vm(n, cap, half), vm(n, cap, half), vm(slots, tokens),
+            vm(width, hid), vm(width, hid), vm(hid, width),
+            dma((3,)), dma, dma, dma((4,)), dma, dma((4,)), dma, dma((4,)), dma, dma((4,)),
+            dma, dma((4,)), dma, dma, dma, dma, dma, dma((3,)),
+        ],
+        compiler_params=pltpu.CompilerParams(
+            collective_id=1, has_side_effects=True, vmem_limit_bytes=60 * 1024 * 1024
+        ),
+        name="experts",
+    )(mixer, cot, choice.T, weight, gate, up, wg, wu, wd)
 
 
 def body(
@@ -91,57 +327,10 @@
     expert_count = lax.axis_size(SP)
     sp = lax.axis_index(SP)
     tokens_here, model_width = mixer_output.shape
-    capacity = gate_pre.shape[1] // expert_count
-    half_width = model_width // lax.axis_size("tp")
-    half_start = lax.axis_index("tp") * half_width
-    mixer_half = lax.dynamic_slice_in_dim(mixer_output, half_start, half_width, 1)
-    cotangent_half = lax.dynamic_slice_in_dim(layer_cotangent, half_start, half_width, 1)
-    hot0, hot1 = slot_rows(expert_choice, expert_count, capacity)
-    hot_any = hot0 + hot1
-    cot_f = cotangent_half.astype(f32)
-    rows0 = (route_weight[:, 0:1] * cot_f).astype(bf16)
-    rows1 = (route_weight[:, 1:2] * cot_f).astype(bf16)
-    send_grads = jnp.dot(
-        jnp.concatenate([hot0, hot1], axis=1),
-        jnp.concatenate([rows0, rows1], axis=0),
-        preferred_element_type=f32,
-    ).astype(bf16)
-    send_hidden = jnp.dot(hot_any, mixer_half, preferred_element_type=f32).astype(bf16)
-
-    def exchanged(rows):
-        return lax.all_to_all(
-            rows.reshape(expert_count, capacity, -1), SP, 0, 0, tiled=True
-        ).reshape(expert_count * capacity, -1)
-
-    both = jnp.concatenate(
-        [
-            send_grads.reshape(expert_count, capacity, -1),
-            send_hidden.reshape(expert_count, capacity, -1),
-        ],
-        axis=1,
-    )
-    came = lax.all_to_all(both, SP, 0, 0, tiled=True)
-    came = jnp.concatenate(
-        [
-            came[:, :capacity].reshape(-1, half_width),
-            came[:, capacity:].reshape(-1, half_width),
-        ],
-        axis=0,
-    )
-    came = lax.all_gather(came, "tp", axis=1, tiled=True)
-    recv_grads, recv_hidden = jnp.split(came, 2, axis=0)
-    gate_wgrad, up_wgrad, down_wgrad, partial_rows = expert_side(
-        recv_hidden, recv_grads, gate_pre[0], up_pre[0], w_gate[0], w_up[0], w_down[0]
-    )
-    pieces = partial_rows.astype(bf16).reshape(-1, 2, half_width)
-    pieces = lax.all_to_all(pieces.transpose(1, 0, 2), "tp", 0, 0, tiled=True)
-    summed = (pieces[0].astype(f32) + pieces[1].astype(f32)).astype(bf16)
-    returned = exchanged(summed)
-    moe_half = lax.dot_general(
-        hot_any, returned, (((0,), (0,)), ((), ())), preferred_element_type=f32
-    )
-    hidden_half = (cot_f + moe_half).astype(bf16)
-    grad_hidden = lax.all_gather(hidden_half, "tp", axis=1, tiled=True)
+    gate_wgrad, up_wgrad, down_wgrad, grad_hidden = moe_side(
+        mixer_output, layer_cotangent, expert_choice, route_weight,
+        gate_pre[0], up_pre[0], w_gate[0], w_up[0], w_down[0],
+    )
 
     head_count = log_decay.shape[1]
     group_count = b_proj.shape[1] // STATE
@@ -244,7 +433,10 @@
     grad_b_carry = jnp.einsum("sgrp,grpn->sgn", x_tail, later_groups)
     grad_a = jnp.sum(grad_y * scan_out, axis=2) - jnp.sum(x_float * grad_x, axis=2)
     suffix = jnp.flip(jnp.cumsum(jnp.flip(grad_a, 0), axis=0), 0)
-    totals = lax.all_gather(suffix[0], SP)
+    totals = suffix[0]
+    for axis in reversed(SP):
+        totals = lax.all_gather(totals, axis)
+    totals = totals.reshape(expert_count, head_count)
     later_grad = jnp.sum(jnp.where(blocks[:, None] > sp, totals, 0.0), axis=0)
     grad_log_decay = suffix + later_grad[None, :]
     grad_scan_in = grad_x.reshape(tokens_here, -1).astype(bf16)

time: 393 us -> 209 us (0.53)
  blocking collectives: 237 us -> 42.9 us
  Pallas kernels: 0 us -> 56.9 us
  matrix products: 39.9 us -> 11.1 us
  waiting for transfers between devices: 45.7 us -> 36.4 us
  starting transfers between devices: 25.1 us -> 16.7 us
  other arithmetic: 14.2 us -> 7.94 us
  local copies, waits for them, and re-layouts: 16.3 us -> 21.8 us
    all_gather x2 -> x3, blocking collectives: 174 us -> 30.2 us  [body(): totals = lax.all_gather(totals, axis)]
    pallas_call x0 -> x1, Pallas kernels: none -> 56.9 us  [moe_side(): pl.pallas_call(moe_kernel, out_shape=(jax.ShapeDtypeStruct((width, hid),...]
    all_to_all x2 -> x0, blocking collectives: 46.7 us -> none  [the longest x1 41.3 us: body(): came = lax.all_to_all(both, SP, 0, 0, tiled=True)]
    dot_general x10 -> x0, matrix products: 22.8 us -> none  [the longest x1 4.86 us: expert_side(): jnp.einsum('rf,rd->fd', active, grad_rows, preferred_element_type=jnp.flo...]
    all_to_all x1 -> x0, waiting for transfers between devices: 15.7 us -> none  [exchanged(): lax.all_to_all(rows.reshape(expert_count, capacity, -1), SP, 0, 0, tiled=...]
    all_to_all x1 -> x0, starting transfers between devices: 10.7 us -> none  [exchanged(): lax.all_to_all(rows.reshape(expert_count, capacity, -1), SP, 0, 0, tiled=...]
    all_gather x1 -> x0, waiting for transfers between devices: 7.05 us -> none  [body(): came = lax.all_gather(came, 'tp', axis=1, tiled=True)]
    all_gather x1, waiting for transfers between devices: 6.05 us -> 12.6 us  [body(): mixed_line = lax.all_gather(mixed, SP[0], axis=0, tiled=True)]
  transfers between devices with their start and end apart: 7 -> 5, of which waited for: 5 -> 3; matrix products, arithmetic and copies ran while one was open for 10% -> 5% of each run, Pallas kernels for 0% -> 0%
where the time goes in v2:
time: 209 us; the launch traced here: 208 us
  Pallas kernels  56.9 us (27%)
  blocking collectives  42.9 us (21%)
  waiting for transfers between devices  36.4 us (17%)
  local copies, waits for them, and re-layouts  21.8 us (10%)
  starting transfers between devices  16.7 us (8%)
  between operations  14.3 us (7%)
  matrix products  11.1 us (5%)
  other arithmetic  7.94 us (4%)
    pallas_call x1, Pallas kernels, moe_side(): pl.pallas_call(moe_kernel, out_shape=(jax.ShapeDtypeStruct((width, hid),...  56.9 us
    all_gather x3, blocking collectives, body(): totals = lax.all_gather(totals, axis)  30.2 us
    unnamed x59, local copies, waits for them, and re-layouts  14.4 us
    all_to_all x1, waiting for transfers between devices, body(): came_state = lax.all_to_all(sent, SP, 0, 0, tiled=True)  13.3 us
    all_to_all x1, blocking collectives, body(): columns_line = lax.all_to_all(grad_hidden, SP[0], 1, 0, tiled=True)  12.7 us
    all_gather x1, waiting for transfers between devices, body(): mixed_line = lax.all_gather(mixed, SP[0], axis=0, tiled=True)  12.6 us
    all_to_all x1, waiting for transfers between devices, body(): later_state = lax.all_to_all(later_all, SP, 0, 0, tiled=True)  10.5 us
    all_to_all x1, starting transfers between devices, body(): came_state = lax.all_to_all(sent, SP, 0, 0, tiled=True)  9.6 us
  transfers between devices with their start and end apart: 5, of which 3 were waited for; matrix products, arithmetic and copies ran while one was open for 5% of the time, Pallas kernels for 0%

profile of v2, /device:TPU:0, one launch (start us, length us, event | category | flops | bytes accessed | tf_op | source)
XLA Modules:
  0.0 208.0 jit_solution(9169311099696695087)
XLA Ops:
  7.3 0.8 mul.145
  8.0 0.7 convert_element_type.55
  8.7 0.8 copy.116
  9.5 0.2 reduce_window_sum.26
  9.7 0.5 slice_reduce_fusion.1
  10.2 0.7 subtract_exponential_fusion
  10.9 1.0 reshape.170
  11.9 0.1 copy.133
  12.0 1.0 reshape.171
  13.0 0.1 copy.135
  13.2 0.5 copy-done.5
  13.7 1.1 copy.119
  14.9 0.2 fusion.28
  15.2 0.2 fusion.40
  15.5 0.3 fusion.5
  15.8 0.5 fusion
  16.3 0.2 copy.122
  16.5 0.1 fusion.22
  16.7 0.2 reshape.177
  16.9 0.2 multiply_reduce_fusion.3
  17.1 0.6 add_rsqrt_fusion
  17.8 1.4 copy.112.weight
  19.2 56.9 %experts.1 = (bf16[2048,512]{1,0:T(8,128)(2,1)}, bf16[2048,512]{1,0:T(8,128)(2,1)}, bf16[512,2048]{1,0:T(8,128)(2,1)}, bf16[128,2048]{1,0:T(8,128)(2,1)}) custom-call(bf16[128,2048]{1,0:T(8,128)(2,1)} %mixer.1, bf16[128,2048]{1,0:T(8,128)(2,1)} %cot.1, s32[2,128]{1,0:T(2,128)} %bitcast.158, f32[128,2]{1,0:T(8,128)} %copy.112.weight, ...), custom_call_target="tpu_custom_call" | custom-call | tf_op jit(solution)/shard_map/experts/pallas_call | solution.py:279
  76.1 3.9 %fusion.42 = f32[128,1024]{1,0:T(8,128)S(1)} fusion(bf16[128,2048]{1,0:T(8,128)(2,1)} %get-tuple-element.16, bf16[1024,2048]{1,0:T(8,128)(2,1)} %param.26), kind=kOutput, calls=%fused_computation.81 | convolution fusion | flops 536870912 | bytes 5242880 | tf_op jit(solution)/shard_map/td,id->ti/dot_general | solution.py:377
  80.0 1.0 reshape.178
  81.0 1.5 multiply_reduce_fusion.2
  82.5 0.2 mul.150
  82.8 0.2 mul.139
  83.1 1.2 fusion.11
  84.5 12.7 %all_to_all.29 = bf16[128,4,512]{2,0,1:T(8,128)(2,1)S(1)} all-to-all(bf16[128,4,512]{2,0,1:T(8,128)(2,1)S(1)} %bitcast.144), channel_id=1, replica_groups=mesh['sp_0'=4,'sp_1'=4,'sp_2'=4,'tp'=2] {'sp_0'}, dimensions={1} | all-to-all | bytes 1048576 | tf_op jit(solution)/shard_map/all_to_all | solution.py:370
  97.2 12.6 %all-gather.6.cloned.1.call-done = bf16[512,1024]{1,0:T(8,128)(2,1)} async-done(((bf16[128,1024]{1,0:T(8,128)(2,1)}), bf16[512,1024]{1,0:T(8,128)(2,1)}) %all-gather.6.cloned.1.call-update) | async-done | bytes 1048592 | tf_op jit(solution)/shard_map/all_gather | solution.py:368
  109.8 3.3 %fusion.41 = f32[512,1024]{1,0:T(8,128)} fusion(bf16[512,512]{1,0:T(8,128)(2,1)S(1)} %bitcast.135, bf16[512,1024]{1,0:T(8,128)(2,1)} %all-gather.6.cloned.1.call-done), kind=kOutput, calls=%fused_computation.80 | convolution fusion | flops 536870912 | bytes 3670016 | tf_op jit(solution)/shard_map/dot_general | solution.py:371
  113.2 0.2 copy.123
  113.4 0.3 copy-done.22
  114.0 0.7 subtract_exponential_fusion.1
  114.7 0.2 fusion.16
  114.9 0.1 broadcast_in_dim.79
  115.0 0.9 pad_maximum_fusion
  116.0 9.6 %all-to-all-start.1 = ((f32[64,24,128]{2,1,0:T(8,128)}), f32[64,24,128]{2,1,0:T(8,128)S(1)}, u32[]{:S(2)}, u32[]{:S(2)}) async-start(f32[64,24,128]{2,1,0:T(8,128)} %pad_maximum_fusion), calls=%async_computation.3 | async-start | bytes 1572864 | tf_op jit(solution)/shard_map/all_to_all | solution.py:401
  125.7 0.3 convolution_bitcast_fusion.2
  126.0 0.5 bitcast_reduce_fusion
  126.5 0.2 fusion.4
  126.7 0.8 copy.139
  127.5 13.3 %all-to-all-done.1 = f32[64,24,128]{2,1,0:T(8,128)S(1)} async-done(((f32[64,24,128]{2,1,0:T(8,128)}), f32[64,24,128]{2,1,0:T(8,128)S(1)}, u32[]{:S(2)}, u32[]{:S(2)}) %all-to-all-start.1) | async-done | bytes 786464 | tf_op jit(solution)/shard_map/all_to_all | solution.py:401
  140.9 0.1 reduce.2
  141.2 0.7 fusion.12
  142.0 0.9 copy.129
  142.8 7.0 %all-to-all-start.2 = ((bf16[64,16,128]{2,1,0:T(8,128)(2,1)}), bf16[64,16,128]{2,1,0:T(8,128)(2,1)S(1)}, u32[]{:S(2)}, u32[]{:S(2)}) async-start(bf16[64,16,128]{2,1,0:T(8,128)(2,1)} %copy.129), calls=%async_computation.4 | async-start | bytes 524288 | tf_op jit(solution)/shard_map/all_to_all | solution.py:411
  150.0 10.5 %all-to-all-done.2 = bf16[64,16,128]{2,1,0:T(8,128)(2,1)S(1)} async-done(((bf16[64,16,128]{2,1,0:T(8,128)(2,1)}), bf16[64,16,128]{2,1,0:T(8,128)(2,1)S(1)}, u32[]{:S(2)}, u32[]{:S(2)}) %all-to-all-start.2) | async-done | bytes 262176 | tf_op jit(solution)/shard_map/all_to_all | solution.py:411
  160.4 0.2 fusion.23
  160.8 0.3 multiply_reduce_fusion
  161.3 0.2 reduce_window_sum.28
  161.5 7.9 %all-gather.2 = f32[4,1,16]{2,1,0:T(1,128)S(1)} all-gather(f32[1,1,16]{2,1,0:T(1,128)S(1)} %slice_bitcast_fusion), channel_id=1, replica_groups=mesh['sp_0'=4,'sp_1'=4,'sp_2'=4,'tp'=2] {'sp_2'}, dimensions={0}, use_global_device_ids=true | all-gather | bytes 320 | tf_op jit(solution)/shard_map/all_gather | solution.py:438
  169.4 10.4 %all-gather.3 = f32[4,4,16]{2,1,0:T(4,128)S(1)} all-gather(f32[1,4,16]{2,1,0:T(4,128)S(1)} %bitcast.157), channel_id=2, replica_groups=mesh['sp_0'=4,'sp_1'=4,'sp_2'=4,'tp'=2] {'sp_1'}, dimensions={0}, use_global_device_ids=true | all-gather | bytes 1280 | tf_op jit(solution)/shard_map/all_gather | solution.py:438
  179.8 11.9 %all-gather.1 = f32[16,4,16]{2,1,0:T(4,128)S(1)} all-gather(f32[4,4,16]{2,1,0:T(4,128)S(1)} %all-gather.3), channel_id=3, replica_groups=mesh['sp_0'=4,'sp_1'=4,'sp_2'=4,'tp'=2] {'sp_0'}, dimensions={0}, use_global_device_ids=true | all-gather | bytes 5120 | tf_op jit(solution)/shard_map/all_gather | solution.py:438
  191.8 0.7 copy.140
  192.5 0.3 convolution_bitcast_fusion.3
  192.8 0.2 fusion.3
  193.0 0.8 copy.138
  193.7 0.8 copy.137
  194.6 3.2 %copy.175 = bf16[1,2048,512]{2,1,0:T(8,128)(2,1)} copy(bf16[1,2048,512]{2,1,0:T(8,128)(2,1)} %bitcast.140) | data formatting | bytes 4194304
  197.8 1.3 copy.176
  199.1 1.0 copy-done.2
  200.1 1.3 copy.177
  (79 shorter events, 1.8 us)
Async XLA Ops:
  7.2 7.7 %copy-start = (f32[1,16,64,128]{3,2,1,0:T(8,128)S(1)}, f32[1,16,64,128]{3,2,1,0:T(8,128)}, u32[]{:S(2)}) copy-start(f32[1,16,64,128]{3,2,1,0:T(8,128)} %param.33) | copy-start | bytes 1572868
  7.2 102.6 %all-gather.6.cloned.1.call-start = ((), (), s32[]{:S(2)}) async-start(), calls=%async_computation.5 | async-start | bytes 1310720 | tf_op jit(solution)/shard_map/all_gather | solution.py:368
  7.3 8.2 %copy-start.17 = (pred[128,128]{1,0:T(8,128)(4,1)}, pred[128,128]{1,0:T(8,128)(4,1)S(1)}, u32[]{:S(2)}) copy-start(pred[128,128]{1,0:T(8,128)(4,1)S(1)} %iota_compare_fusion) | copy-start | bytes 49156
  9.7 5.5 %copy-start.11 = (f32[128,16]{1,0:T(8,128)}, f32[128,16]{1,0:T(8,128)S(1)}, u32[]{:S(2)}) copy-start(f32[128,16]{1,0:T(8,128)S(1)} %reduce_window_sum.26) | copy-start | bytes 24580
  10.2 0.7 copy-start.20
  12.0 3.8 %copy-start.7 = (bf16[128,4,128]{0,2,1:T(8,128)(2,1)}, bf16[128,4,128]{0,2,1:T(8,128)(2,1)S(1)}, u32[]{:S(2)}) copy-start(bf16[128,4,128]{0,2,1:T(8,128)(2,1)S(1)} %copy.133) | copy-start | bytes 393220
  13.0 0.7 copy-start.5
  13.2 2.6 %copy-start.9 = (bf16[128,4,128]{0,2,1:T(8,128)(2,1)}, bf16[128,4,128]{0,2,1:T(8,128)(2,1)S(1)}, u32[]{:S(2)}) copy-start(bf16[128,4,128]{0,2,1:T(8,128)(2,1)S(1)} %copy.135) | copy-start | bytes 393220
  15.2 1.3 copy-start.13
  81.0 1.8 copy-start.15
  81.0 2.1 %copy-start.14 = (bf16[128,1024]{1,0:T(8,128)(2,1)S(1)}, bf16[128,1024]{1,0:T(8,128)(2,1)}, u32[]{:S(2)}) copy-start(bf16[128,1024]{1,0:T(8,128)(2,1)} %param.29) | copy-start | bytes 786436
  83.1 1.3 copy-start.1
  84.4 76.4 %reduce-scatter.3.cloned.1.call-start = ((), (), s32[]{:S(2)}) async-start(), calls=%async_computation.6 | async-start | bytes 2621440 | tf_op jit(solution)/shard_map/reduce_scatter | solution.py:374
  109.8 3.4 %copy-start.12 = (f32[128,16]{1,0:T(8,128)S(1)}, f32[128,16]{1,0:T(8,128)}, u32[]{:S(2)}) copy-start(f32[128,16]{1,0:T(8,128)} %copy-done.11) | copy-start | bytes 24580
  109.8 3.4 %copy-start.4 = (f32[128,1024]{1,0:T(8,128)S(1)}, f32[128,1024]{1,0:T(8,128)}, u32[]{:S(2)}) copy-start(f32[128,1024]{1,0:T(8,128)} %get-tuple-element.54) | copy-start | bytes 1572868
  113.1 0.7 copy-start.22
  113.1 0.7 copy-start.21
  114.7 10.9 %copy-start.16 = (f32[128,16]{1,0:T(8,128)S(1)}, f32[128,16]{1,0:T(8,128)}, u32[]{:S(2)}) copy-start(f32[128,16]{1,0:T(8,128)} %get-tuple-element.60) | copy-start | bytes 24580
  115.0 10.9 %copy-start.18 = (pred[128,128]{1,0:T(8,128)(4,1)S(1)}, pred[128,128]{1,0:T(8,128)(4,1)}, u32[]{:S(2)}) copy-start(pred[128,128]{1,0:T(8,128)(4,1)} %copy-done.17) | copy-start | bytes 49156
  116.0 10.5 %copy-start.10 = (bf16[128,4,128]{0,2,1:T(8,128)(2,1)S(1)}, bf16[128,4,128]{0,2,1:T(8,128)(2,1)}, u32[]{:S(2)}) copy-start(bf16[128,4,128]{0,2,1:T(8,128)(2,1)} %copy-done.9) | copy-start | bytes 393220
  116.0 24.8 %all-to-all-start.1 = ((f32[64,24,128]{2,1,0:T(8,128)}), f32[64,24,128]{2,1,0:T(8,128)S(1)}, u32[]{:S(2)}, u32[]{:S(2)}) async-start(f32[64,24,128]{2,1,0:T(8,128)} %pad_maximum_fusion), calls=%async_computation.3 | async-start | bytes 1572864 | tf_op jit(solution)/shard_map/all_to_all | solution.py:401
  127.5 32.9 %copy-start.6 = (bf16[128,4,128]{2,1,0:T(4,128)(2,1)S(1)}, bf16[128,4,128]{2,1,0:T(4,128)(2,1)}, u32[]{:S(2)}) copy-start(bf16[128,4,128]{2,1,0:T(4,128)(2,1)} %copy-done.5) | copy-start | bytes 393220
  142.8 17.6 %all-to-all-start.2 = ((bf16[64,16,128]{2,1,0:T(8,128)(2,1)}), bf16[64,16,128]{2,1,0:T(8,128)(2,1)S(1)}, u32[]{:S(2)}, u32[]{:S(2)}) async-start(bf16[64,16,128]{2,1,0:T(8,128)(2,1)} %copy.129), calls=%async_computation.4 | async-start | bytes 524288 | tf_op jit(solution)/shard_map/all_to_all | solution.py:411
  149.8 44.8 %reduce-scatter.5.cloned.1.call-start = ((), (), s32[]{:S(2)}) async-start(), calls=%async_computation.7 | async-start | bytes 655360 | tf_op jit(solution)/shard_map/reduce_scatter | solution.py:375
  160.7 31.8 %copy-start.19 = (f32[128,4,4]{0,2,1:T(4,128)S(1)}, f32[128,4,4]{0,2,1:T(4,128)}, u32[]{:S(2)}) copy-start(f32[128,4,4]{0,2,1:T(4,128)} %get-tuple-element.62) | copy-start | bytes 24580
  160.7 32.1 %copy-start.8 = (bf16[128,4,128]{0,2,1:T(8,128)(2,1)S(1)}, bf16[128,4,128]{0,2,1:T(8,128)(2,1)}, u32[]{:S(2)}) copy-start(bf16[128,4,128]{0,2,1:T(8,128)(2,1)} %copy-done.7) | copy-start | bytes 393220
  194.6 3.2 %copy-start.3 = (bf16[2048,512]{1,0:T(8,128)(2,1)S(1)}, bf16[2048,512]{1,0:T(8,128)(2,1)}, u32[]{:S(2)}) copy-start(bf16[2048,512]{1,0:T(8,128)(2,1)} %get-tuple-element.14) | copy-start | bytes 6291460
  197.8 2.3 %copy-start.2 = (bf16[512,2048]{1,0:T(8,128)(2,1)S(1)}, bf16[512,2048]{1,0:T(8,128)(2,1)}, u32[]{:S(2)}) copy-start(bf16[512,2048]{1,0:T(8,128)(2,1)} %get-tuple-element.15) | copy-start | bytes 6291460
Sparse Core Ops, SparseCore 0:
  84.5 25.2 all-gather.5
  113.3 38.3 reduce-scatter.2
  160.9 17.4 reduce-scatter.4

commit v3 on v2

--- a/solution.py
+++ b/solution.py
@@ -304,6 +304,271 @@
     )(mixer, cot, choice.T, weight, gate, up, wg, wu, wd)
 
 
+HIGH = lax.Precision.HIGHEST
+
+
+def exact(a, b, dims=NN):
+    return lax.dot_general(a, b, dims, precision=HIGH, preferred_element_type=f32)
+
+
+def scan_kernel(
+    gh, wout_h, gain, xin, gate, bp, cp, logd, state,
+    gop_o, gsi_o, ggi_o, gb_o, gc_o, gld_o,
+    wout, mixl, coll, dsend, drecv, bsend, brecv, lsend, lrecv, osend, orecv, tsend, trecv,
+    stb, so, unit, gy, gxi, gbi, dec, mw, mwt, xm, gym, grown,
+    wsem, msn, mrv, csn, crv, dsn, drv, bsn, brv, lsn, lrv, osn, orv, tsn, trv,
+):
+    n, slab = bsend.shape[0], bsend.shape[1]
+    tokens, width = xin.shape
+    heads = logd.shape[1]
+    groups = bp.shape[1] // STATE
+    per = heads // groups
+    gw_cols = width // groups
+    z, y, x, me = place()
+    plane = y * 4 + x
+    greet(n)
+    load = pltpu.make_async_copy(wout_h, wout, wsem)
+    load.start()
+
+    ti = lax.broadcasted_iota(jnp.int32, (tokens, tokens), 0)
+    si = lax.broadcasted_iota(jnp.int32, (tokens, tokens), 1)
+    lower = ti >= si
+    upper = ti <= si
+    ones_low = jnp.where(lower, 1.0, 0.0)
+    ones_up = jnp.where(upper, 1.0, 0.0)
+    cum = exact(ones_low, logd[...])
+    cum_t = exact(logd[...], ones_up, TN)
+    growth = jnp.exp(cum)
+    tail = jnp.exp(cum[tokens - 1 : tokens, :] - cum)
+    lane_head = lax.broadcasted_iota(jnp.int32, (tokens, gw_cols), 1) // HEAD_DIM
+    masks = [lane_head == r for r in range(per)]
+    for h in range(heads):
+        dsend[h] = jnp.broadcast_to(growth[tokens - 1 : tokens, h : h + 1], dsend.shape[1:])
+
+    def spread(v, g):
+        w = jnp.broadcast_to(v[:, g * per : g * per + 1], (tokens, gw_cols))
+        for r in range(1, per):
+            w = jnp.where(masks[r], v[:, g * per + r : g * per + r + 1], w)
+        return w
+
+    def cols(g):
+        return slice(g * gw_cols, (g + 1) * gw_cols)
+
+    def states(g):
+        return slice(g * STATE, (g + 1) * STATE)
+
+    invs = []
+    for g in range(groups):
+        c, b = cp[:, states(g)], bp[:, states(g)]
+        inner, inner_t = dotf(c, b, NT), dotf(b, c, NT)
+        xg = xin[:, cols(g)]
+        for r in range(per):
+            h = g * per + r
+            col, row = cum[:, h : h + 1], cum_t[h : h + 1, :]
+            d = jnp.exp(jnp.where(lower, col - row, -1e30))
+            dt = jnp.exp(jnp.where(upper, row - col, -1e30))
+            span = slice(r * tokens, (r + 1) * tokens)
+            dec[g, span, :] = d
+            mw[:, span] = (inner * d).astype(bf16)
+            mwt[g, :, span] = (inner_t * dt).astype(bf16)
+            xm[span, :] = jnp.where(masks[r], xg.astype(f32), 0.0).astype(bf16)
+        stb[cols(g), :] = state[cols(g), :].astype(bf16)
+        carry = dotf(c, stb[cols(g), :], NT)
+        out = dotf(mw[...], xm[...]) + carry * spread(growth, g)
+        so[:, cols(g)] = out
+        gf = gate[:, cols(g)].astype(f32)
+        gated = out * (gf * jax.nn.sigmoid(gf))
+        inv = lax.rsqrt(jnp.mean(gated * gated, axis=1, keepdims=True) + rms_epsilon)
+        invs.append(inv)
+        u = gated * inv
+        unit[:, cols(g)] = u
+        mixl[z, :, cols(g)] = (u * gain[:, cols(g)].astype(f32)).astype(bf16)
+
+    quarter = gh.shape[1] // 4
+    coll[z] = gh[:, pl.ds(pl.multiple_of(z * quarter, quarter), quarter)]
+    greeted(n)
+    for k in range(1, 4):
+        pz = lax.rem(z + k, 4)
+        part = pl.ds(pl.multiple_of(pz * quarter, quarter), quarter)
+        push(gh.at[:, part], coll.at[z], csn, crv, {SP[0]: pz})
+
+    def send_decay(k, _):
+        device, j = peer_of(k)
+        push(dsend.at[j // (n // heads)], drecv.at[me], dsn, drv, device)
+        return 0
+
+    lax.fori_loop(1, n, send_decay, 0)
+    own_decay = pltpu.make_async_copy(dsend.at[me // (n // heads)], drecv.at[me], drv)
+    own_decay.start()
+    for k in range(1, 4):
+        push(mixl.at[z], mixl.at[z], msn, mrv, {SP[0]: lax.rem(z + k, 4)})
+    load.wait()
+
+    slabs = gw_cols // slab
+    for g in range(groups):
+        c = cp[:, states(g)]
+        gain_f = gain[:, cols(g)].astype(f32)
+        gu = dotf(gh[...], wout[cols(g), :], NT) * gain_f
+        u = unit[:, cols(g)]
+        out = so[:, cols(g)]
+        gg = invs[g] * (gu - u * jnp.mean(gu * u, axis=1, keepdims=True))
+        gf = gate[:, cols(g)].astype(f32)
+        sig = jax.nn.sigmoid(gf)
+        ggi_o[:, cols(g)] = (gg * out * sig * (1.0 + gf * (1.0 - sig))).astype(bf16)
+        gyg = gg * (gf * sig)
+        gy[:, cols(g)] = gyg
+        gr = (gyg * spread(growth, g)).astype(bf16)
+        grown[:, cols(g)] = gr
+        bs = dotf(gr, c, TN)
+        bsend[g * slabs : (g + 1) * slabs] = bs.reshape(slabs, slab, STATE).astype(bf16)
+
+    def sends(src, dst, send, recv):
+        def one(k, _):
+            device, j = peer_of(k)
+            push(src.at[j], dst.at[me], send, recv, device)
+            return 0
+
+        lax.fori_loop(1, n, one, 0)
+        pltpu.make_async_copy(src.at[me], dst.at[me], recv).start()
+
+    sends(bsend, brecv, bsn, brv)
+
+    for g in range(groups):
+        c, b = cp[:, states(g)], bp[:, states(g)]
+        xg = xin[:, cols(g)]
+        gyg = gy[:, cols(g)]
+        for r in range(per):
+            gym[r * tokens : (r + 1) * tokens, :] = jnp.where(masks[r], gyg, 0.0).astype(bf16)
+        pairs = dotf(gym[...], xg, NT) * dec[g]
+        gw = pairs[:tokens]
+        for r in range(1, per):
+            gw = gw + pairs[r * tokens : (r + 1) * tokens]
+        gw = gw.astype(bf16)
+        gxi[:, cols(g)] = dotf(mwt[g], gym[...])
+        gc = dotf(gw, b) + dotf(grown[:, cols(g)], stb[cols(g), :])
+        gc_o[:, states(g)] = gc.astype(bf16)
+        gbi[:, states(g)] = dotf(gw, c, TN)
+
+    took(coll.at[pl.ds(0, 3)], crv)
+    took(mixl.at[pl.ds(0, 3)], mrv)
+    rows = osend.shape[1]
+    left = coll[...].reshape(4 * tokens, quarter)
+    right = mixl[...].reshape(4 * tokens, width)
+    osend[...] = dotf(left, right, TN).astype(bf16).reshape(n // 4, rows, width)
+
+    took(brecv, brv)
+    took(drecv, drv)
+
+    def step(i, acc):
+        j = n - 1 - i
+        lsend[j] = acc.reshape(slab, STATE).astype(bf16)
+        block = brecv[j].astype(f32).reshape(slab // 8, 8, STATE)
+        return acc * drecv[j][None] + block
+
+    lax.fori_loop(0, n, step, jnp.zeros((slab // 8, 8, STATE), f32), unroll=4)
+    sends(lsend, lrecv, lsn, lrv)
+
+    def send_outer(k, _):
+        py, px = lax.rem(y + k // 4, 4), lax.rem(x + lax.rem(k, 4), 4)
+        push(osend.at[py * 4 + px], orecv.at[plane], osn, orv, {SP[1]: py, SP[2]: px})
+        return 0
+
+    lax.fori_loop(1, n // 4, send_outer, 0)
+    pltpu.make_async_copy(osend.at[plane], orecv.at[plane], orv).start()
+
+    took(lrecv, lrv)
+    ga = jnp.zeros((tokens, STATE), f32)
+    for g in range(groups):
+        b = bp[:, states(g)]
+        xf = xin[:, cols(g)].astype(f32)
+        later = lrecv[g * slabs : (g + 1) * slabs].reshape(gw_cols, STATE)
+        tails = spread(tail, g)
+        gx = gxi[:, cols(g)] + dotf(b, later, NT) * tails
+        gsi_o[:, cols(g)] = gx.astype(bf16)
+        gb = gbi[:, states(g)] + dotf((xf * tails).astype(bf16), later)
+        gb_o[:, states(g)] = gb.astype(bf16)
+        sel = jnp.where(
+            lax.broadcasted_iota(jnp.int32, (gw_cols, STATE), 0) // HEAD_DIM + g * per
+            == lax.broadcasted_iota(jnp.int32, (gw_cols, STATE), 1),
+            1.0, 0.0,
+        )
+        ga = ga + exact(gy[:, cols(g)] * so[:, cols(g)] - xf * gx, sel)
+    suffix = exact(ones_up, ga)
+    tsend[...] = jnp.broadcast_to(suffix[0:1, :], tsend.shape)
+
+    def send_total(k, _):
+        device, _j = peer_of(k)
+        push(tsend, trecv.at[me], tsn, trv, device)
+        return 0
+
+    lax.fori_loop(1, n, send_total, 0)
+    took(orecv, orv)
+    total = orecv[0].astype(f32)
+    for k in range(1, n // 4):
+        total = total + orecv[k].astype(f32)
+    gop_o[...] = total
+    most = pl.ds(0, n - 1)
+    took(trecv.at[most], trv)
+    after = lax.fori_loop(
+        me + 1, n, lambda j, t: t + trecv[j], jnp.zeros(tsend.shape, f32)
+    )
+    gld_o[...] = (suffix + after[0:1, :])[:, :heads]
+
+    took(coll.at[pl.ds(0, 3)], csn)
+    took(mixl.at[pl.ds(0, 3)], msn)
+    took(drecv.at[most], dsn)
+    took(bsend.at[most], bsn)
+    took(lsend.at[most], lsn)
+    took(osend.at[pl.ds(0, n // 4 - 1)], osn)
+    took(trecv.at[most], tsn)
+
+
+def mixer_side(gh, wout, gain, xin, gate, bp, cp, logd, state):
+    n = lax.axis_size(SP)
+    tokens, width = xin.shape
+    heads = logd.shape[1]
+    groups = bp.shape[1] // STATE
+    per = heads // groups
+    slab = heads * HEAD_DIM // n
+    dwidth = gh.shape[1]
+    rows = dwidth // n
+    dma = pltpu.SemaphoreType.DMA
+    vm = lambda *s: pltpu.VMEM(s, bf16)
+    vf = lambda *s: pltpu.VMEM(s, f32)
+    inv = pl.BlockSpec(memory_space=pltpu.VMEM)
+    anyv = pl.BlockSpec(memory_space=pl.ANY)
+    return pl.pallas_call(
+        scan_kernel,
+        out_shape=(
+            jax.ShapeDtypeStruct((rows, width), f32),
+            jax.ShapeDtypeStruct((tokens, width), bf16),
+            jax.ShapeDtypeStruct((tokens, width), bf16),
+            jax.ShapeDtypeStruct(bp.shape, bf16),
+            jax.ShapeDtypeStruct(cp.shape, bf16),
+            jax.ShapeDtypeStruct((tokens, heads), f32),
+        ),
+        in_specs=[inv, anyv] + [inv] * 7,
+        out_specs=(inv,) * 6,
+        scratch_shapes=[
+            vm(*wout.shape), vm(4, tokens, width), vm(4, tokens, dwidth // 4),
+            vf(heads, 8, STATE), vf(n, 8, STATE),
+            vm(n, slab, STATE), vm(n, slab, STATE), vm(n, slab, STATE), vm(n, slab, STATE),
+            vm(n // 4, rows, width), vm(n // 4, rows, width),
+            vf(8, STATE), vf(n, 8, STATE),
+            vm(width, STATE), vf(tokens, width), vf(tokens, width), vf(tokens, width),
+            vf(tokens, width), vf(tokens, groups * STATE),
+            vf(groups, per * tokens, tokens), vm(tokens, per * tokens),
+            vm(groups, tokens, per * tokens), vm(per * tokens, width // groups),
+            vm(per * tokens, width // groups), vm(tokens, width),
+        ]
+        + [dma] * 15,
+        compiler_params=pltpu.CompilerParams(
+            collective_id=2, has_side_effects=True, vmem_limit_bytes=60 * 1024 * 1024
+        ),
+        name="mixer",
+    )(gh, wout, gain, xin, gate, bp, cp, logd, state)
+
+
 def body(
     mixer_output,
     layer_cotangent,
@@ -323,136 +588,15 @@
     log_decay,
     entry_state,
 ):
-    f32, bf16 = jnp.float32, jnp.bfloat16
-    expert_count = lax.axis_size(SP)
-    sp = lax.axis_index(SP)
-    tokens_here, model_width = mixer_output.shape
+    state = entry_state.reshape(-1, STATE)
     gate_wgrad, up_wgrad, down_wgrad, grad_hidden = moe_side(
         mixer_output, layer_cotangent, expert_choice, route_weight,
         gate_pre[0], up_pre[0], w_gate[0], w_up[0], w_down[0],
     )
-
-    head_count = log_decay.shape[1]
-    group_count = b_proj.shape[1] // STATE
-    per_group = head_count // group_count
-    scan_heads = scan_in.reshape(tokens_here, head_count, HEAD_DIM)
-    b_groups = b_proj.reshape(tokens_here, group_count, STATE)
-    c_groups = c_proj.reshape(tokens_here, group_count, STATE)
-    x_float = scan_heads.astype(f32)
-    b_float = b_groups.astype(f32)
-    c_float = c_groups.astype(f32)
-    cumulative = jnp.cumsum(log_decay, axis=0)
-    growth = jnp.exp(cumulative)
-    tail_decay = jnp.exp(cumulative[-1][None, :] - cumulative)
-    token_locations = jnp.arange(tokens_here)
-    causal = token_locations[:, None] >= token_locations[None, :]
-    log_gaps = cumulative.T[:, :, None] - cumulative.T[:, None, :]
-    decay_mat = jnp.exp(jnp.where(causal[None], log_gaps, -jnp.inf))
-    inner_prod = jnp.einsum("tgn,sgn->gts", c_groups, b_groups, preferred_element_type=f32)
-    mix_weights = (jnp.repeat(inner_prod, per_group, axis=0) * decay_mat).astype(bf16)
-    state_groups = entry_state.reshape(group_count, per_group, HEAD_DIM, STATE)
-    y_inner = jnp.einsum("hts,shp->thp", mix_weights, scan_heads, preferred_element_type=f32)
-    y_carry = jnp.einsum("tgn,grpn->tgrp", c_float, state_groups).reshape(
-        tokens_here, head_count, HEAD_DIM
+    rest = mixer_side(
+        grad_hidden, w_out, norm_gain[None], scan_in, gate_in, b_proj, c_proj, log_decay, state
     )
-    scan_out = y_inner + y_carry * growth[:, :, None]
-    gate_float = gate_in.astype(f32)
-    gate_sig = jax.nn.sigmoid(gate_float)
-    gate_silu = gate_float * gate_sig
-    gated = scan_out.reshape(tokens_here, -1) * gate_silu
-    grouped = gated.reshape(tokens_here, group_count, -1)
-    inv_rms = lax.rsqrt(jnp.mean(grouped * grouped, axis=-1, keepdims=True) + rms_epsilon)
-    unit = grouped * inv_rms
-    gain_groups = norm_gain.astype(f32).reshape(group_count, -1)
-    mixed = (unit * gain_groups).reshape(tokens_here, -1).astype(bf16)
-    mixed_line = lax.all_gather(mixed, SP[0], axis=0, tiled=True)
-
-    columns_line = lax.all_to_all(grad_hidden, SP[0], 1, 0, tiled=True)
-    outer = lax.dot_general(
-        columns_line, mixed_line, (((0,), (0,)), ((), ())), preferred_element_type=f32
-    )
-    outer = lax.psum_scatter(outer, SP[1], scatter_dimension=0, tiled=True)
-    grad_out_proj = lax.psum_scatter(outer, SP[2], scatter_dimension=0, tiled=True)
-
-    grad_mixed = jnp.einsum("td,id->ti", grad_hidden, w_out, preferred_element_type=f32)
-    grad_unit = grad_mixed.reshape(tokens_here, group_count, -1) * gain_groups
-    grad_grouped = inv_rms * (grad_unit - unit * jnp.mean(grad_unit * unit, axis=-1, keepdims=True))
-    grad_gated = grad_grouped.reshape(tokens_here, -1)
-    grad_gate_in = (
-        grad_gated
-        * scan_out.reshape(tokens_here, -1)
-        * gate_sig
-        * (1.0 + gate_float * (1.0 - gate_sig))
-    ).astype(bf16)
-    grad_y = (grad_gated * gate_silu).reshape(tokens_here, head_count, HEAD_DIM)
-    grad_y_b = grad_y.astype(bf16)
-    grown_grads = (grad_y * growth[:, :, None]).reshape(
-        tokens_here, group_count, per_group, HEAD_DIM
-    )
-    block_state = jnp.einsum("tgrp,tgn->grpn", grown_grads, c_float).reshape(
-        expert_count, -1, STATE
-    )
-    rows = block_state.shape[1]
-    each = expert_count // head_count
-    last = jnp.repeat(cumulative[-1], each)
-    sent = jnp.concatenate(
-        [block_state, jnp.broadcast_to(last[:, None, None], (expert_count, 8, STATE))], axis=1
-    )
-    came_state = lax.all_to_all(sent, SP, 0, 0, tiled=True)
-    states, lasts = came_state[:, :rows], came_state[:, rows, 0]
-    through = jnp.cumsum(lasts)
-    upto = jnp.concatenate([jnp.zeros((1,), f32), through[:-1]])
-    blocks = jnp.arange(expert_count)
-    gaps = upto[None, :] - through[:, None]
-    carry = jnp.exp(jnp.where(blocks[None, :] > blocks[:, None], gaps, -jnp.inf))
-    later_all = jnp.dot(
-        carry, states.reshape(expert_count, -1), precision=lax.Precision.HIGHEST
-    ).reshape(expert_count, rows, STATE)
-    later_state = lax.all_to_all(later_all, SP, 0, 0, tiled=True)
-
-    grad_x_inner = jnp.einsum("hts,thp->shp", mix_weights, grad_y_b, preferred_element_type=f32)
-    grad_weights = (
-        jnp.einsum("thp,shp->hts", grad_y_b, scan_heads, preferred_element_type=f32) * decay_mat
-    )
-    grad_weights = (
-        grad_weights.reshape(group_count, per_group, tokens_here, tokens_here)
-        .sum(axis=1)
-        .astype(bf16)
-    )
-    grad_c_inner = jnp.einsum("gts,sgn->tgn", grad_weights, b_groups, preferred_element_type=f32)
-    grad_b_inner = jnp.einsum("gts,tgn->sgn", grad_weights, c_groups, preferred_element_type=f32)
-    grad_c_carry = jnp.einsum("tgrp,grpn->tgn", grown_grads, state_groups)
-    x_tail = (x_float * tail_decay[:, :, None]).reshape(
-        tokens_here, group_count, per_group, HEAD_DIM
-    )
-    later_groups = later_state.reshape(group_count, per_group, HEAD_DIM, STATE)
-    grad_x_carry = jnp.einsum("sgn,grpn->sgrp", b_float, later_groups).reshape(
-        tokens_here, head_count, HEAD_DIM
-    )
-    grad_x = grad_x_inner + grad_x_carry * tail_decay[:, :, None]
-    grad_b_carry = jnp.einsum("sgrp,grpn->sgn", x_tail, later_groups)
-    grad_a = jnp.sum(grad_y * scan_out, axis=2) - jnp.sum(x_float * grad_x, axis=2)
-    suffix = jnp.flip(jnp.cumsum(jnp.flip(grad_a, 0), axis=0), 0)
-    totals = suffix[0]
-    for axis in reversed(SP):
-        totals = lax.all_gather(totals, axis)
-    totals = totals.reshape(expert_count, head_count)
-    later_grad = jnp.sum(jnp.where(blocks[:, None] > sp, totals, 0.0), axis=0)
-    grad_log_decay = suffix + later_grad[None, :]
-    grad_scan_in = grad_x.reshape(tokens_here, -1).astype(bf16)
-    grad_b_proj = (grad_b_inner + grad_b_carry).reshape(tokens_here, -1).astype(bf16)
-    grad_c_proj = (grad_c_inner + grad_c_carry).reshape(tokens_here, -1).astype(bf16)
-    return (
-        gate_wgrad[None],
-        up_wgrad[None],
-        down_wgrad[None],
-        grad_out_proj,
-        grad_scan_in,
-        grad_gate_in,
-        grad_b_proj,
-        grad_c_proj,
-        grad_log_decay,
-    )
+    return (gate_wgrad[None], up_wgrad[None], down_wgrad[None], *rest)
 
 
 def solution(mesh):

time: 209 us -> 132 us (0.63)
  Pallas kernels: 56.9 us -> 117 us
  blocking collectives: 42.9 us -> 0 us
  waiting for transfers between devices: 36.4 us -> 0 us
  starting transfers between devices: 16.7 us -> 0 us
  between operations: 14.3 us -> 0.69 us
  matrix products: 11.1 us -> 0 us
  local copies, waits for them, and re-layouts: 21.8 us -> 13.7 us
  other arithmetic: 7.94 us -> 0 us
    pallas_call x0 -> x1, Pallas kernels: none -> 60.6 us  [mixer_side(): pl.pallas_call(scan_kernel, out_shape=(jax.ShapeDtypeStruct((rows, width)...]
    all_gather x3 -> x0, blocking collectives: 30.2 us -> none  [body(): totals = lax.all_gather(totals, axis)]
    all_to_all x2 -> x0, waiting for transfers between devices: 23.7 us -> none  [the longest x1 13.3 us: body(): came_state = lax.all_to_all(sent, SP, 0, 0, tiled=True)]
    all_to_all x2 -> x0, starting transfers between devices: 16.6 us -> none  [the longest x1 9.6 us: body(): came_state = lax.all_to_all(sent, SP, 0, 0, tiled=True)]
    all_to_all x1 -> x0, blocking collectives: 12.7 us -> none  [body(): columns_line = lax.all_to_all(grad_hidden, SP[0], 1, 0, tiled=True)]
    all_gather x1 -> x0, waiting for transfers between devices: 12.6 us -> none  [body(): mixed_line = lax.all_gather(mixed, SP[0], axis=0, tiled=True)]
    dot_general x14 -> x0, matrix products: 11.1 us -> none  [the longest x1 3.88 us: body(): jnp.einsum('td,id->ti', grad_hidden, w_out, preferred_element_type=f32)]
    reshape x7 -> x0, local copies, waits for them, and re-layouts: 3.71 us -> none  [the longest x2 1.13 us: body(): b_groups = b_proj.reshape(tokens_here, group_count, STATE)]
  transfers between devices with their start and end apart: 5 -> 0, of which waited for: 3 -> 0; matrix products, arithmetic and copies ran while one was open for 5% -> 0% of each run, Pallas kernels for 0% -> 0%
where the time goes in v3:
time: 132 us
  Pallas kernels  117 us (89%)
  local copies, waits for them, and re-layouts  13.7 us (10%)
    pallas_call x1, Pallas kernels, mixer_side(): pl.pallas_call(scan_kernel, out_shape=(jax.ShapeDtypeStruct((rows, width)...  60.6 us
    pallas_call x1, Pallas kernels, moe_side(): pl.pallas_call(moe_kernel, out_shape=(jax.ShapeDtypeStruct((width, hid),...  56.9 us
    unnamed x31, local copies, waits for them, and re-layouts  13.1 us

profile of v3, /device:TPU:0, one launch (start us, length us, event | category | flops | bytes accessed | tf_op | source)
XLA Modules:
  0.0 131.9 jit_solution(13876170220869441565)
XLA Ops:
  0.6 1.4 %copy.26.weight = f32[128,2]{1,0:T(8,128)} copy(f32[128,2]{0,1:T(2,128)} %param.20) | data formatting | bytes 2048 | tf_op args[3]
  2.1 0.0 copy-start.9
  2.1 0.0 copy-start.8
  2.1 56.9 %experts.1 = (bf16[2048,512]{1,0:T(8,128)(2,1)}, bf16[2048,512]{1,0:T(8,128)(2,1)}, bf16[512,2048]{1,0:T(8,128)(2,1)}, bf16[128,2048]{1,0:T(8,128)(2,1)}) custom-call(bf16[128,2048]{1,0:T(8,128)(2,1)} %mixer.2, bf16[128,2048]{1,0:T(8,128)(2,1)} %cot.1, s32[2,128]{1,0:T(2,128)} %bitcast.19, f32[128,2]{1,0:T(8,128)} %copy.26.weight, ...), custom_call_target="tpu_custom_call" | custom-call | tf_op jit(solution)/shard_map/experts/pallas_call | solution.py:279
  59.0 0.0 copy-done.9
  59.0 0.6 broadcast_in_dim.15.gain
  59.6 0.0 copy-done.8
  59.6 0.7 copy.27.logd
  60.3 0.0 copy-start.2
  60.3 60.6 %mixer.3 = (f32[32,1024]{1,0:T(8,128)}, bf16[128,1024]{1,0:T(8,128)(2,1)}, bf16[128,1024]{1,0:T(8,128)(2,1)}, bf16[128,512]{1,0:T(8,128)(2,1)}, bf16[128,512]{1,0:T(8,128)(2,1)}, /*index=5*/f32[128,16]{1,0:T(8,128)}) custom-call(bf16[128,2048]{1,0:T(8,128)(2,1)} %get-tuple-element.22.gh, bf16[1024,2048]{1,0:T(8,128)(2,1)} %wout_h.1, ...), custom_call_target="tpu_custom_call" | custom-call | tf_op jit(solution)/shard_map/mixer/pallas_call | solution.py:540
  120.9 1.5 %copy.28 = f32[128,16]{0,1:T(8,128)} copy(f32[128,16]{1,0:T(8,128)} %get-tuple-element.37) | data formatting | bytes 16384
  122.4 0.0 copy-done.2
  122.4 0.0 copy-start.1
  122.4 1.3 %copy.37 = bf16[1,2048,512]{2,1,0:T(8,128)(2,1)} copy(bf16[1,2048,512]{2,1,0:T(8,128)(2,1)S(1)} %bitcast.15) | data formatting | bytes 4194304
  123.7 1.0 copy-done.1
  124.8 0.0 copy-start
  124.8 1.3 copy.38
  126.1 1.0 copy-done
  127.1 0.0 copy-start.7
  127.1 0.0 copy-start.4
  127.1 0.0 copy-start.3
  127.1 0.0 copy-start.6
  127.1 0.0 copy-start.5
  127.1 1.3 %copy.39 = bf16[1,512,2048]{2,1,0:T(8,128)(2,1)} copy(bf16[1,512,2048]{2,1,0:T(8,128)(2,1)S(1)} %bitcast.13) | data formatting | bytes 4194304
  128.5 0.0 copy-done.7
  128.5 0.7 copy.40
  129.1 0.0 copy-done.4
  129.1 0.7 copy.41
  129.8 0.0 copy-done.3
  129.8 0.7 copy.42
  130.5 0.0 copy-done.6
  130.5 0.7 copy.43
  131.2 0.0 copy-done.5
  131.2 0.7 copy.44
Async XLA Ops:
  2.1 56.9 %copy-start.9 = (bf16[1024]{0:T(1024)(128)(2,1)S(1)}, bf16[1024]{0:T(1024)(128)(2,1)}, u32[]{:S(2)}) copy-start(bf16[1024]{0:T(1024)(128)(2,1)} %param.27) | copy-start | bytes 6148
  2.1 57.5 %copy-start.8 = (f32[128,16]{0,1:T(8,128)S(1)}, f32[128,16]{0,1:T(8,128)}, u32[]{:S(2)}) copy-start(f32[128,16]{0,1:T(8,128)} %param.32) | copy-start | bytes 24580
  60.3 62.1 %copy-start.2 = (bf16[2048,512]{1,0:T(8,128)(2,1)S(1)}, bf16[2048,512]{1,0:T(8,128)(2,1)}, u32[]{:S(2)}) copy-start(bf16[2048,512]{1,0:T(8,128)(2,1)} %get-tuple-element.19) | copy-start | bytes 6291460
  122.4 2.3 %copy-start.1 = (bf16[2048,512]{1,0:T(8,128)(2,1)S(1)}, bf16[2048,512]{1,0:T(8,128)(2,1)}, u32[]{:S(2)}) copy-start(bf16[2048,512]{1,0:T(8,128)(2,1)} %get-tuple-element.20) | copy-start | bytes 6291460
  124.8 2.3 %copy-start = (bf16[512,2048]{1,0:T(8,128)(2,1)S(1)}, bf16[512,2048]{1,0:T(8,128)(2,1)}, u32[]{:S(2)}) copy-start(bf16[512,2048]{1,0:T(8,128)(2,1)} %get-tuple-element.21) | copy-start | bytes 6291460
  127.1 1.3 %copy-start.7 = (f32[32,1024]{1,0:T(8,128)S(1)}, f32[32,1024]{1,0:T(8,128)}, u32[]{:S(2)}) copy-start(f32[32,1024]{1,0:T(8,128)} %get-tuple-element.50) | copy-start | bytes 393220
  127.1 2.0 %copy-start.4 = (bf16[128,1024]{1,0:T(8,128)(2,1)S(1)}, bf16[128,1024]{1,0:T(8,128)(2,1)}, u32[]{:S(2)}) copy-start(bf16[128,1024]{1,0:T(8,128)(2,1)} %get-tuple-element.51) | copy-start | bytes 786436
  127.1 2.7 %copy-start.3 = (bf16[128,1024]{1,0:T(8,128)(2,1)S(1)}, bf16[128,1024]{1,0:T(8,128)(2,1)}, u32[]{:S(2)}) copy-start(bf16[128,1024]{1,0:T(8,128)(2,1)} %get-tuple-element.52) | copy-start | bytes 786436
  127.1 3.4 %copy-start.6 = (bf16[128,512]{1,0:T(8,128)(2,1)S(1)}, bf16[128,512]{1,0:T(8,128)(2,1)}, u32[]{:S(2)}) copy-start(bf16[128,512]{1,0:T(8,128)(2,1)} %get-tuple-element.53) | copy-start | bytes 393220
  127.1 4.1 %copy-start.5 = (bf16[128,512]{1,0:T(8,128)(2,1)S(1)}, bf16[128,512]{1,0:T(8,128)(2,1)}, u32[]{:S(2)}) copy-start(bf16[128,512]{1,0:T(8,128)(2,1)} %get-tuple-element.54) | copy-start | bytes 393220

commit v4 on v2

v4 whole, which is shorter than its diff:
```python
import jax
import jax.numpy as jnp
from jax import lax
from jax.experimental import pallas as pl
from jax.experimental.pallas import tpu as pltpu
from jax.sharding import Mesh
from jax.sharding import PartitionSpec as P

HEAD_DIM = 64
STATE = 128
SP = ("sp_0", "sp_1", "sp_2")


rms_epsilon = 1e-05
clamp_limit = 7.0
swish_alpha = 1.702


f32, bf16 = jnp.float32, jnp.bfloat16
MESH_ID = pl.DeviceIdType.MESH
NT = (((1,), (1,)), ((), ()))
NN = (((1,), (0,)), ((), ()))
TN = (((0,), (0,)), ((), ()))


def dotf(a, b, dims=NN):
    return lax.dot_general(a, b, dims, preferred_element_type=f32)


def place():
    z, y, x = (lax.axis_index(a) for a in SP)
    return z, y, x, z * 16 + y * 4 + x


def peer_of(k):
    z, y, x, _ = place()
    pz = lax.rem(z + k // 16, 4)
    py = lax.rem(y + lax.rem(k // 4, 4), 4)
    px = lax.rem(x + lax.rem(k, 4), 4)
    return {SP[0]: pz, SP[1]: py, SP[2]: px}, pz * 16 + py * 4 + px


def greet(others):
    barrier = pltpu.get_barrier_semaphore()

    def one(k, _):
        device, _i = peer_of(k)
        pl.semaphore_signal(barrier, inc=1, device_id=device, device_id_type=MESH_ID)
        return 0

    lax.fori_loop(1, others, one, 0)
    partner = {"tp": 1 - lax.axis_index("tp")}
    pl.semaphore_signal(barrier, inc=1, device_id=partner, device_id_type=MESH_ID)


def greeted(others):
    pl.semaphore_wait(pltpu.get_barrier_semaphore(), others)


def push(src, dst, send, recv, device):
    pltpu.make_async_remote_copy(
        src_ref=src, dst_ref=dst, send_sem=send, recv_sem=recv,
        device_id=device, device_id_type=MESH_ID,
    ).start()


def took(ref, sem):
    pltpu.make_async_copy(ref, ref, sem).wait()


HIGH = lax.Precision.HIGHEST
EARLY = 2
MIX = 0
REST = 3
COLL = 1


def exact(a, b, dims=NN):
    return lax.dot_general(a, b, dims, precision=HIGH, preferred_element_type=f32)


def whole_kernel(
    cot, choice, weight, logd, gain,
    mixer_h, gate_h, up_h, wd_h, wg_h, wu_h, wout_h, xin_h, gin_h, bp_h, cp_h, state_h,
    gwg, gwu, gwd, gop_o, gsi_o, ggi_o, gb_o, gc_o, gld_o,
    mixer, gate, up, wd, wg, wu, wout, xin, gin, bp, cp, state,
    send_g, send_h, recv_g, recv_h, oth_g, oth_h, grads, hidden,
    fu, fg, act, acc, gg, ug, psend, precv, pown, rsend, rrecv, hot,
    gh, mixl, coll, dsend, drecv, bsend, brecv, lsend, lrecv, osend, orecv, tsend, trecv,
    stb, so, unit, gy, gxi, gbi, dec, mw, mwt, xm, gym, grown,
    wsem, sg, rg, sh, rh, dsg, drg, dsh, drh, dsp, drp, sr, rr, dso, drout,
    msn, mrv, csn, crv, dsn, drv, bsn, brv, lsn, lrv, osn, orv, tsn, trv,
):
    n, cap, half = recv_g.shape
    tokens = cot.shape[0]
    z, y, x, me = place()
    plane_at = y * 4 + x
    tp = lax.axis_index("tp")
    partner = {"tp": 1 - tp}
    mine = pl.ds(pl.multiple_of(tp * half, half), half)
    theirs = pl.ds(pl.multiple_of((1 - tp) * half, half), half)
    most = pl.ds(0, n - 1)
    greet(n)
    order = (
        (xin_h, xin), (gin_h, gin), (bp_h, bp), (cp_h, cp), (state_h, state), (mixer_h, mixer),
        (gate_h, gate), (up_h, up), (wd_h, wd), (wg_h, wg), (wu_h, wu), (wout_h, wout),
    )
    loads = [pltpu.make_async_copy(a, b, wsem.at[i]) for i, (a, b) in enumerate(order)]
    for c in loads:
        c.start()

    ti = lax.broadcasted_iota(jnp.int32, (tokens, tokens), 0)
    si = lax.broadcasted_iota(jnp.int32, (tokens, tokens), 1)
    lower = ti >= si
    upper = ti <= si
    experts = lax.broadcasted_iota(jnp.int32, (n, tokens), 0)
    hits = [experts == choice[k : k + 1, :] for k in range(2)]
    named = jnp.where(hits[0] | hits[1], 1.0, 0.0).astype(bf16)
    before = jnp.where(ti < si, 1.0, 0.0).astype(bf16)
    earlier = dotf(named, before)
    places = lax.broadcasted_iota(jnp.int32, (n * cap, tokens), 0)
    hots = []
    for k in range(2):
        rank = jnp.sum(jnp.where(hits[k], earlier, 0.0), axis=0, keepdims=True)
        slot = choice[k : k + 1, :] * cap + rank.astype(jnp.int32)
        hots.append(jnp.where(places == slot, 1.0, 0.0).astype(bf16))
    hot[...] = hots[0] + hots[1]
    weights = exact(jnp.where(ti == si, 1.0, 0.0), weight[...], NT)
    cot_half = cot[:, mine].astype(f32)
    rows0 = (weights[:, 0:1] * cot_half).astype(bf16)
    rows1 = (weights[:, 1:2] * cot_half).astype(bf16)
    packed = dotf(hots[0], rows0) + dotf(hots[1], rows1)
    send_g[...] = packed.reshape(n, cap, half).astype(bf16)
    greeted(n)

    def sends(src, dst, send, recv, first, last):
        def one(k, _):
            device, i = peer_of(k)
            push(src.at[i], dst.at[me], send, recv, device)
            return 0

        lax.fori_loop(first, last, one, 0)

    pltpu.make_async_copy(send_g.at[me], recv_g.at[me], rg.at[z]).start()
    sends(send_g, recv_g, sg, rg.at[z], 1, n)

    heads = logd.shape[0]
    groups = bp.shape[1] // STATE
    width = xin.shape[1]
    per = heads // groups
    gw_cols = width // groups
    ones_low = jnp.where(lower, 1.0, 0.0)
    ones_up = jnp.where(upper, 1.0, 0.0)
    cum = exact(ones_low, logd[...], NT)
    cum_t = exact(logd[...], ones_up)
    growth = jnp.exp(cum)
    tail = jnp.exp(cum[tokens - 1 : tokens, :] - cum)
    lane_head = lax.broadcasted_iota(jnp.int32, (tokens, gw_cols), 1) // HEAD_DIM
    masks = [lane_head == r for r in range(per)]
    for h in range(heads):
        dsend[h] = jnp.broadcast_to(growth[tokens - 1 : tokens, h : h + 1], dsend.shape[1:])
    each = n // heads
    pltpu.make_async_copy(dsend.at[me // each], drecv.at[me], drv).start()

    def send_decay(k, _):
        device, j = peer_of(k)
        push(dsend.at[j // each], drecv.at[me], dsn, drv, device)
        return 0

    lax.fori_loop(1, n, send_decay, 0)

    def spread(v, g):
        w = jnp.broadcast_to(v[:, g * per : g * per + 1], (tokens, gw_cols))
        for r in range(1, per):
            w = jnp.where(masks[r], v[:, g * per + r : g * per + r + 1], w)
        return w

    def cols(g):
        return slice(g * gw_cols, (g + 1) * gw_cols)

    def states(g):
        return slice(g * STATE, (g + 1) * STATE)

    for c in loads[:5]:
        c.wait()
    invs = []
    for g in range(groups):
        c, b = cp[:, states(g)], bp[:, states(g)]
        inner, inner_t = dotf(c, b, NT), dotf(b, c, NT)
        xg = xin[:, cols(g)]
        for r in range(per):
            h = g * per + r
            col, row = cum[:, h : h + 1], cum_t[h : h + 1, :]
            d = jnp.exp(jnp.where(lower, col - row, -1e30))
            dt = jnp.exp(jnp.where(upper, row - col, -1e30))
            span = slice(r * tokens, (r + 1) * tokens)
            dec[g, span, :] = d
            mw[:, span] = (inner * d).astype(bf16)
            mwt[g, :, span] = (inner_t * dt).astype(bf16)
            xm[span, :] = jnp.where(masks[r], xg.astype(f32), 0.0).astype(bf16)
        stb[cols(g), :] = state[cols(g), :].astype(bf16)
        carry = dotf(c, stb[cols(g), :], NT)
        out = dotf(mw[...], xm[...]) + carry * spread(growth, g)
        so[:, cols(g)] = out
        gf = gin[:, cols(g)].astype(f32)
        gated = out * (gf * jax.nn.sigmoid(gf))
        inv = lax.rsqrt(jnp.mean(gated * gated, axis=1, keepdims=True) + rms_epsilon)
        invs.append(inv)
        u = gated * inv
        unit[:, cols(g)] = u
        mixl[z, :, cols(g)] = (u * gain[:, cols(g)].astype(f32)).astype(bf16)

    def send_mixed():
        for k in range(1, 4):
            push(mixl.at[z], mixl.at[z], msn, mrv, {SP[0]: lax.rem(z + k, 4)})

    if MIX == 0:
        send_mixed()

    loads[5].wait()
    packed = dotf(hot[...], mixer[:, mine])
    send_h[...] = packed.reshape(n, cap, half).astype(bf16)
    pltpu.make_async_copy(send_h.at[me], recv_h.at[me], rh.at[z]).start()

    loads[6].wait()
    loads[7].wait()

    def prepare(i, _):
        rows = pl.ds(pl.multiple_of(i * 64, 64), 64)
        gate_full = gate[rows, :].astype(f32)
        up_full = up[rows, :].astype(f32)
        gate_clip = jnp.minimum(gate_full, clamp_limit)
        up_clip = jnp.clip(up_full, -clamp_limit, clamp_limit)
        sig = jax.nn.sigmoid(swish_alpha * gate_clip)
        swish = gate_clip * sig
        act[rows, :] = ((up_clip + 1.0) * swish).astype(bf16)
        inside = (up_full > -clamp_limit) & (up_full < clamp_limit)
        fu[rows, :] = jnp.where(inside, swish, 0.0)
        slope = sig + swish_alpha * gate_clip * sig * (1.0 - sig)
        fg[rows, :] = jnp.where(gate_full < clamp_limit, (up_clip + 1.0) * slope, 0.0)
        return 0

    lax.fori_loop(0, gate.shape[0] // 64, prepare, 0)
    for c in loads[8:11]:
        c.wait()

    quart = n // 4
    rowsof = quart * cap

    def plane(i):
        q = lax.rem(z - i + 4, 4)
        blocks = pl.ds(pl.multiple_of(q * quart, quart), quart)
        return q, blocks, pl.ds(pl.multiple_of(q * rowsof, rowsof), rowsof)

    def flat(ref, blocks):
        return ref[blocks].astype(f32).reshape(rowsof, half).astype(bf16)

    def arrive(i, _):
        q, blocks, rows = plane(i)
        took(recv_g.at[blocks], rg.at[q])
        push(recv_g.at[blocks], oth_g.at[blocks], dsg, drg.at[q], partner)
        g = flat(recv_g, blocks)
        grads[rows, mine] = g
        acc[rows, :] = dotf(g, wd[:, mine], NT)
        return 0


    def expert(i, _):
        q, blocks, rows = plane(i)
        took(oth_g.at[blocks], drg.at[q])
        g = flat(oth_g, blocks)
        grads[rows, theirs] = g
        act_grad = acc[rows, :] + dotf(g, wd[:, theirs], NT)
        up_grad = (act_grad * fu[rows, :]).astype(bf16)
        gate_grad = (act_grad * fg[rows, :]).astype(bf16)
        ug[rows, :] = up_grad
        gg[rows, :] = gate_grad
        part = dotf(gate_grad, wg[theirs, :], NT) + dotf(up_grad, wu[theirs, :], NT)
        psend[rows, :] = part.astype(bf16)
        push(psend.at[rows], precv.at[rows], dsp, drp.at[q], partner)
        part = dotf(gate_grad, wg[mine, :], NT) + dotf(up_grad, wu[mine, :], NT)
        pown[rows, :] = part.astype(bf16)
        return 0


    def give_back(i, _):
        q, blocks, rows = plane(i)
        took(precv.at[rows], drp.at[q])
        total = pown[rows, :].astype(f32) + precv[rows, :].astype(f32)
        rsend[blocks] = total.reshape(quart, cap, half).astype(bf16)

        def one(k, _):
            device, j = peer_of((4 - i) % 4 * quart + k)
            push(rsend.at[j], rrecv.at[me], sr, rr, device)
            return 0

        lax.fori_loop(1 if i == 0 else 0, quart, one, 0)
        return 0

    arrive(0, 0)
    expert(0, 0)
    give_back(0, 0)
    arrive(1, 0)
    arrive(2, 0)
    expert(1, 0)
    arrive(3, 0)
    sends(send_h, recv_h, sh, rh.at[z], 1, max(1, EARLY * n // 4))
    expert(2, 0)
    give_back(1, 0)
    expert(3, 0)
    give_back(2, 0)
    give_back(3, 0)
    def send_rest(at):
        if REST == at:
            sends(send_h, recv_h, sh, rh.at[z], max(1, EARLY * n // 4), n)

    send_rest(0)
    pltpu.make_async_copy(rsend.at[me], rrecv.at[me], rr).start()

    def down(i, _):
        cols = pl.ds(pl.multiple_of(i * 512, 512), 512)
        gwd[:, cols] = dotf(act[...], grads[:, cols], TN).astype(bf16)
        return 0

    lax.fori_loop(0, grads.shape[1] // 512, down, 0)

    loads[11].wait()
    took(rrecv, rr)
    r = rrecv[...].astype(f32).reshape(n * cap, half).astype(bf16)
    gh[:, mine] = (cot[:, mine].astype(f32) + dotf(hot[...], r, TN)).astype(bf16)
    push(gh.at[:, mine], gh.at[:, mine], dso, drout, partner)
    took(gh.at[:, theirs], drout)
    quarter = gh.shape[1] // 4

    def send_columns():
        for k in range(1, 4):
            pz = lax.rem(z + k, 4)
            part = pl.ds(pl.multiple_of(pz * quarter, quarter), quarter)
            push(gh.at[:, part], coll.at[z], csn, crv, {SP[0]: pz})

    if COLL == 0:
        send_columns()
    coll[z] = gh[:, pl.ds(pl.multiple_of(z * quarter, quarter), quarter)]
    send_rest(1)
    slab = bsend.shape[1]
    slabs = gw_cols // slab
    for g in range(groups):
        c = cp[:, states(g)]
        gain_f = gain[:, cols(g)].astype(f32)
        gu = dotf(gh[...], wout[cols(g), :], NT) * gain_f
        u = unit[:, cols(g)]
        out = so[:, cols(g)]
        dgated = invs[g] * (gu - u * jnp.mean(gu * u, axis=1, keepdims=True))
        gf = gin[:, cols(g)].astype(f32)
        sig = jax.nn.sigmoid(gf)
        ggi_o[:, cols(g)] = (dgated * out * sig * (1.0 + gf * (1.0 - sig))).astype(bf16)
        gyg = dgated * (gf * sig)
        gy[:, cols(g)] = gyg
        gr = (gyg * spread(growth, g)).astype(bf16)
        grown[:, cols(g)] = gr
        bs = dotf(gr, c, TN)
        bsend[g * slabs : (g + 1) * slabs] = bs.reshape(slabs, slab, STATE).astype(bf16)

    def exchange(src, dst, send, recv):
        sends(src, dst, send, recv, 1, n)
        pltpu.make_async_copy(src.at[me], dst.at[me], recv).start()

    exchange(bsend, brecv, bsn, brv)
    if COLL == 1:
        send_columns()
    send_rest(2)
    if MIX == 1:
        send_mixed()

    for g in range(groups):
        c, b = cp[:, states(g)], bp[:, states(g)]
        xg = xin[:, cols(g)]
        gyg = gy[:, cols(g)]
        for r in range(per):
            gym[r * tokens : (r + 1) * tokens, :] = jnp.where(masks[r], gyg, 0.0).astype(bf16)
        pairs = dotf(gym[...], xg, NT) * dec[g]
        gw = pairs[:tokens]
        for r in range(1, per):
            gw = gw + pairs[r * tokens : (r + 1) * tokens]
        gw = gw.astype(bf16)
        gxi[:, cols(g)] = dotf(mwt[g], gym[...])
        gc = dotf(gw, b) + dotf(grown[:, cols(g)], stb[cols(g), :])
        gc_o[:, states(g)] = gc.astype(bf16)
        gbi[:, states(g)] = dotf(gw, c, TN)

    took(brecv, brv)
    took(drecv, drv)

    def step(i, acc):
        j = n - 1 - i
        lsend[j] = acc.reshape(slab, STATE).astype(bf16)
        block = brecv[j].astype(f32).reshape(slab // 8, 8, STATE)
        return acc * drecv[j][None] + block

    lax.fori_loop(0, n, step, jnp.zeros((slab // 8, 8, STATE), f32), unroll=4)
    exchange(lsend, lrecv, lsn, lrv)
    send_rest(3)

    took(coll.at[pl.ds(0, 3)], crv)
    took(mixl.at[pl.ds(0, 3)], mrv)
    rows = osend.shape[1]
    left = coll[...].reshape(4 * tokens, quarter)
    right = mixl[...].reshape(4 * tokens, width)
    osend[...] = dotf(left, right, TN).astype(bf16).reshape(n // 4, rows, width)

    def send_outer(k, _):
        py, px = lax.rem(y + k // 4, 4), lax.rem(x + lax.rem(k, 4), 4)
        push(osend.at[py * 4 + px], orecv.at[plane_at], osn, orv, {SP[1]: py, SP[2]: px})
        return 0

    lax.fori_loop(1, n // 4, send_outer, 0)
    pltpu.make_async_copy(osend.at[plane_at], orecv.at[plane_at], orv).start()

    send_rest(4)

    def arrive_h(i, _):
        q, blocks, rows = plane(i)
        took(recv_h.at[blocks], rh.at[q])
        push(recv_h.at[blocks], oth_h.at[blocks], dsh, drh.at[q], partner)
        hidden[rows, mine] = flat(recv_h, blocks)
        return 0

    lax.fori_loop(0, 4, arrive_h, 0)

    def other_h(i, _):
        q, blocks, rows = plane(i)
        took(oth_h.at[blocks], drh.at[q])
        hidden[rows, theirs] = flat(oth_h, blocks)
        return 0

    lax.fori_loop(0, 4, other_h, 0)

    def wide(i, _):
        cols = pl.ds(pl.multiple_of(i * 512, 512), 512)
        h = hidden[:, cols]
        gwg[cols, :] = dotf(h, gg[...], TN).astype(bf16)
        gwu[cols, :] = dotf(h, ug[...], TN).astype(bf16)
        return 0

    lax.fori_loop(0, hidden.shape[1] // 512, wide, 0)

    took(lrecv, lrv)
    ga = jnp.zeros((tokens, STATE), f32)
    for g in range(groups):
        b = bp[:, states(g)]
        xf = xin[:, cols(g)].astype(f32)
        later = lrecv[g * slabs : (g + 1) * slabs].reshape(gw_cols, STATE)
        tails = spread(tail, g)
        gx = gxi[:, cols(g)] + dotf(b, later, NT) * tails
        gsi_o[:, cols(g)] = gx.astype(bf16)
        gb = gbi[:, states(g)] + dotf((xf * tails).astype(bf16), later)
        gb_o[:, states(g)] = gb.astype(bf16)
        sel = jnp.where(
            lax.broadcasted_iota(jnp.int32, (gw_cols, STATE), 0) // HEAD_DIM + g * per
            == lax.broadcasted_iota(jnp.int32, (gw_cols, STATE), 1),
            1.0, 0.0,
        )
        ga = ga + exact(gy[:, cols(g)] * so[:, cols(g)] - xf * gx, sel)
    suffix = exact(ones_up, ga)
    tsend[...] = jnp.broadcast_to(suffix[0:1, :], tsend.shape)

    def send_total(k, _):
        device, _j = peer_of(k)
        push(tsend, trecv.at[me], tsn, trv, device)
        return 0

    lax.fori_loop(1, n, send_total, 0)
    took(orecv, orv)
    total = orecv[0].astype(f32)
    for k in range(1, n // 4):
        total = total + orecv[k].astype(f32)
    gop_o[...] = total
    took(trecv.at[most], trv)
    after = lax.fori_loop(
        me + 1, n, lambda j, t: t + trecv[j], jnp.zeros(tsend.shape, f32)
    )
    total = suffix + after[0:1, :]
    gld_o[...] = exact(total, jnp.where(ti == si, 1.0, 0.0), TN)[:heads, :]

    took(coll.at[pl.ds(0, 3)], csn)
    took(mixl.at[pl.ds(0, 3)], msn)
    took(drecv.at[most], dsn)
    took(bsend.at[most], bsn)
    took(lsend.at[most], lsn)
    took(osend.at[pl.ds(0, n // 4 - 1)], osn)
    took(trecv.at[most], tsn)
    took(gh.at[:, mine], dso)
    took(send_g.at[most], sg)
    took(send_h.at[most], sh)
    took(rsend.at[most], sr)
    took(recv_g, dsg)
    took(recv_h, dsh)
    took(psend, dsp)


def whole(cot, choice, weight, logd, gain, mixer, gate, up, wd, wg, wu, wout, xin, gin, bp, cp, state):
    n = lax.axis_size(SP)
    tokens, dwidth = cot.shape
    slots, hid = gate.shape
    cap, half = slots // n, dwidth // 2
    width = xin.shape[1]
    heads = logd.shape[0]
    groups = bp.shape[1] // STATE
    per = heads // groups
    slab = heads * HEAD_DIM // n
    rows = dwidth // n
    dma = pltpu.SemaphoreType.DMA
    vm = lambda *s: pltpu.VMEM(s, bf16)
    vf = lambda *s: pltpu.VMEM(s, f32)
    inv = pl.BlockSpec(memory_space=pltpu.VMEM)
    anyv = pl.BlockSpec(memory_space=pl.ANY)
    bulk = (mixer, gate, up, wd, wg, wu, wout, xin, gin, bp, cp, state)
    shaped = lambda s, t: pltpu.VMEM(s, t)
    return pl.pallas_call(
        whole_kernel,
        out_shape=(
            shaped((dwidth, hid), bf16), shaped((dwidth, hid), bf16), shaped((hid, dwidth), bf16),
            shaped((rows, width), f32),
            shaped((tokens, width), bf16), shaped((tokens, width), bf16),
            shaped(bp.shape, bf16), shaped(cp.shape, bf16),
            shaped((heads, tokens), f32),
        ),
        in_specs=[inv] * 5 + [anyv] * 12,
        out_specs=(inv,) * 9,
        scratch_shapes=[pltpu.VMEM(a.shape, a.dtype) for a in bulk]
        + [
            vm(n, cap, half), vm(n, cap, half), vm(n, cap, half), vm(n, cap, half),
            vm(n, cap, half), vm(n, cap, half), vm(slots, dwidth), vm(slots, dwidth),
            vf(slots, hid), vf(slots, hid), vm(slots, hid), vf(slots, hid),
            vm(slots, hid), vm(slots, hid), vm(slots, half), vm(slots, half), vm(slots, half),
            vm(n, cap, half), vm(n, cap, half), vm(slots, tokens),
            vm(tokens, dwidth), vm(4, tokens, width), vm(4, tokens, dwidth // 4),
            vf(heads, 1, STATE), vf(n, 1, STATE),
            vm(n, slab, STATE), vm(n, slab, STATE), vm(n, slab, STATE), vm(n, slab, STATE),
            vm(n // 4, rows, width), vm(n // 4, rows, width),
            vf(1, STATE), vf(n, 1, STATE),
            vm(width, STATE), vf(tokens, width), vf(tokens, width), vf(tokens, width),
            vf(tokens, width), vf(tokens, groups * STATE),
            vf(groups, per * tokens, tokens), vm(tokens, per * tokens),
            vm(groups, tokens, per * tokens), vm(per * tokens, width // groups),
            vm(per * tokens, width // groups), vm(tokens, width),
            dma((12,)), dma, dma((4,)), dma, dma((4,)), dma, dma((4,)), dma, dma((4,)),
            dma, dma((4,)), dma, dma, dma, dma,
        ]
        + [dma] * 14,
        compiler_params=pltpu.CompilerParams(
            collective_id=1, has_side_effects=True, vmem_limit_bytes=55 * 1024 * 1024
        ),
        name="backward",
    )(cot, choice, weight, logd, gain, *bulk)


def put_out_kernel(*refs):
    count = len(refs) // 2
    sems = refs[-1]
    copies = [
        pltpu.make_async_copy(refs[i], refs[count + i], sems.at[i]) for i in range(count)
    ]
    for c in copies:
        c.start()
    for c in copies:
        c.wait()


def put_out(arrays):
    anyv = pl.BlockSpec(memory_space=pl.ANY)
    return pl.pallas_call(
        put_out_kernel,
        out_shape=tuple(pltpu.HBM(a.shape, a.dtype) for a in arrays),
        in_specs=[pl.BlockSpec(memory_space=pltpu.VMEM)] * len(arrays),
        out_specs=(pl.BlockSpec(memory_space=pltpu.HBM),) * len(arrays),
        scratch_shapes=[pltpu.SemaphoreType.DMA((len(arrays),))],
        compiler_params=pltpu.CompilerParams(vmem_limit_bytes=1024 * 1024),
        name="put_out",
    )(*[pltpu.with_memory_space_constraint(a, pltpu.VMEM) for a in arrays])


def body(
    mixer_output,
    layer_cotangent,
    expert_choice,
    route_weight,
    gate_pre,
    up_pre,
    w_gate,
    w_up,
    w_down,
    w_out,
    norm_gain,
    scan_in,
    gate_in,
    b_proj,
    c_proj,
    log_decay,
    entry_state,
):
    outs = whole(
        layer_cotangent, expert_choice.T, route_weight.T, log_decay.T, norm_gain[None],
        mixer_output, gate_pre[0], up_pre[0], w_down[0], w_gate[0], w_up[0], w_out,
        scan_in, gate_in, b_proj, c_proj, entry_state.reshape(-1, STATE),
    )
    grad_w_gate, grad_w_up, grad_w_down, *rest = put_out(outs)
    *rest, grad_log_decay = rest
    return (grad_w_gate[None], grad_w_up[None], grad_w_down[None], *rest, grad_log_decay.T)


def solution(mesh):
    split = Mesh(mesh.devices.reshape(4, 4, 4, mesh.shape["tp"]), ("sp_0", "sp_1", "sp_2", "tp"))
    return jax.shard_map(
        body,
        mesh=split,
        in_specs=(
            P(SP, None),
            P(SP, None),
            P(SP, None),
            P(SP, None),
            P(SP, None, "tp"),
            P(SP, None, "tp"),
            P(SP, None, "tp"),
            P(SP, None, "tp"),
            P(SP, "tp", None),
            P("tp", None),
            P("tp"),
            P(SP, "tp"),
            P(SP, "tp"),
            P(SP, "tp"),
            P(SP, "tp"),
            P(SP, "tp"),
            P(SP, "tp", None, None),
        ),
        out_specs=(
            P(SP, None, "tp"),
            P(SP, None, "tp"),
            P(SP, "tp", None),
            P(SP, "tp"),
            P(SP, "tp"),
            P(SP, "tp"),
            P(SP, "tp"),
            P(SP, "tp"),
            P(SP, "tp"),
        ),
        check_vma=False,
    )
```

time: 209 us -> 110 us (0.53)
  Pallas kernels: 56.9 us -> 107 us
  blocking collectives: 42.9 us -> 0 us
  waiting for transfers between devices: 36.4 us -> 0 us
  local copies, waits for them, and re-layouts: 21.8 us -> 1.28 us
  starting transfers between devices: 16.7 us -> 0 us
  between operations: 14.3 us -> 0.65 us
  matrix products: 11.1 us -> 0 us
  other arithmetic: 7.94 us -> 0 us
    pallas_call x1 -> x2, Pallas kernels: 56.9 us -> 107 us  [the longest x1 104 us: whole(): pl.pallas_call(whole_kernel, out_shape=(shaped((dwidth, hid), bf16), shap...]
    all_gather x3 -> x0, blocking collectives: 30.2 us -> none  [body(): totals = lax.all_gather(totals, axis)]
    all_to_all x2 -> x0, waiting for transfers between devices: 23.7 us -> none  [the longest x1 13.3 us: body(): came_state = lax.all_to_all(sent, SP, 0, 0, tiled=True)]
    all_to_all x2 -> x0, starting transfers between devices: 16.6 us -> none  [the longest x1 9.6 us: body(): came_state = lax.all_to_all(sent, SP, 0, 0, tiled=True)]
    unnamed x59 -> x0, local copies, waits for them, and re-layouts: 14.4 us -> none
    all_to_all x1 -> x0, blocking collectives: 12.7 us -> none  [body(): columns_line = lax.all_to_all(grad_hidden, SP[0], 1, 0, tiled=True)]
    all_gather x1 -> x0, waiting for transfers between devices: 12.6 us -> none  [body(): mixed_line = lax.all_gather(mixed, SP[0], axis=0, tiled=True)]
    dot_general x14 -> x0, matrix products: 11.1 us -> none  [the longest x1 3.88 us: body(): jnp.einsum('td,id->ti', grad_hidden, w_out, preferred_element_type=f32)]
  transfers between devices with their start and end apart: 5 -> 0, of which waited for: 3 -> 0; matrix products, arithmetic and copies ran while one was open for 5% -> 0% of each run, Pallas kernels for 0% -> 0%
where the time goes in v4:
time: 110 us; the launch traced here: 109 us
  Pallas kernels  107 us (97%)
  local copies, waits for them, and re-layouts  1.28 us (1%)
    pallas_call x1, Pallas kernels, whole(): pl.pallas_call(whole_kernel, out_shape=(shaped((dwidth, hid), bf16), shap...  104 us
    pallas_call x1, Pallas kernels, put_out(): pl.pallas_call(put_out_kernel, out_shape=tuple((pltpu.HBM(a.shape, a.dtyp...  2.99 us

profile of v4, /device:TPU:0, one launch (start us, length us, event | category | flops | bytes accessed | tf_op | source)
XLA Modules:
  0.0 109.0 jit_solution(14203449515355004913)
XLA Ops:
  0.6 1.3 %broadcast_in_dim.12.gain = bf16[1,1024]{1,0:T(2,128)(2,1)} reshape(bf16[1024]{0:T(1024)(128)(2,1)} %param.27) | data formatting | bytes 4096 | tf_op jit(solution)/shard_map/broadcast_in_dim | solution.py:603
  1.9 104.0 %backward.1 = (bf16[2048,512]{1,0:T(8,128)(2,1)S(1)}, bf16[2048,512]{1,0:T(8,128)(2,1)S(1)}, bf16[512,2048]{1,0:T(8,128)(2,1)S(1)}, f32[32,1024]{1,0:T(8,128)S(1...) custom-call(bf16[128,2048]{1,0:T(8,128)(2,1)} %cot.1, ...), custom_call_target="tpu_custom_call" | custom-call | tf_op jit(solution)/shard_map/backward/pallas_call | solution.py:519
  106.0 3.0 %put_out.1 = (bf16[2048,512]{1,0:T(8,128)(2,1)}, bf16[2048,512]{1,0:T(8,128)(2,1)}, bf16[512,2048]{1,0:T(8,128)(2,1)}, f32[32,1024]{1,0:T(8,128)}, bf16[128,1024...) custom-call(bf16[2048,512]{1,0:T(8,128)(2,1)S(1)} %get-tuple-element, ...), custom_call_target="tpu_custom_call" | custom-call | tf_op jit(solution)/shard_map/put_out/pallas_call | solution.py:572

commit v5 on v4

--- a/solution.py
+++ b/solution.py
@@ -69,9 +69,9 @@
 
 
 HIGH = lax.Precision.HIGHEST
-EARLY = 2
+EARLY = 1
 MIX = 0
-REST = 3
+REST = 0
 COLL = 1
 
 
@@ -89,7 +89,7 @@
     gh, mixl, coll, dsend, drecv, bsend, brecv, lsend, lrecv, osend, orecv, tsend, trecv,
     stb, so, unit, gy, gxi, gbi, dec, mw, mwt, xm, gym, grown,
     wsem, sg, rg, sh, rh, dsg, drg, dsh, drh, dsp, drp, sr, rr, dso, drout,
-    msn, mrv, csn, crv, dsn, drv, bsn, brv, lsn, lrv, osn, orv, tsn, trv,
+    msn, mrv, csn, crv, dsn, drv, bsn, brv, lsn, lrv, osn, orv, tsn, trv, cfw,
 ):
     n, cap, half = recv_g.shape
     tokens = cot.shape[0]
@@ -167,7 +167,6 @@
         push(dsend.at[j // each], drecv.at[me], dsn, drv, device)
         return 0
 
-    lax.fori_loop(1, n, send_decay, 0)
 
     def spread(v, g):
         w = jnp.broadcast_to(v[:, g * per : g * per + 1], (tokens, gw_cols))
@@ -329,18 +328,28 @@
     r = rrecv[...].astype(f32).reshape(n * cap, half).astype(bf16)
     gh[:, mine] = (cot[:, mine].astype(f32) + dotf(hot[...], r, TN)).astype(bf16)
     push(gh.at[:, mine], gh.at[:, mine], dso, drout, partner)
+    lax.fori_loop(1, n, send_decay, 0)
     took(gh.at[:, theirs], drout)
     quarter = gh.shape[1] // 4
 
+    owner = z // 2 == tp
+
     def send_columns():
-        for k in range(1, 4):
-            pz = lax.rem(z + k, 4)
+        for k in range(2):
+            pz = 2 * tp + k
             part = pl.ds(pl.multiple_of(pz * quarter, quarter), quarter)
-            push(gh.at[:, part], coll.at[z], csn, crv, {SP[0]: pz})
+
+            @pl.when(pz != z)
+            def _():
+                push(gh.at[:, part], coll.at[z], csn, crv, {SP[0]: pz})
 
     if COLL == 0:
         send_columns()
-    coll[z] = gh[:, pl.ds(pl.multiple_of(z * quarter, quarter), quarter)]
+
+    @pl.when(owner)
+    def _():
+        coll[z] = gh[:, pl.ds(pl.multiple_of(z * quarter, quarter), quarter)]
+
     send_rest(1)
     slab = bsend.shape[1]
     slabs = gw_cols // slab
@@ -401,7 +410,15 @@
     exchange(lsend, lrecv, lsn, lrv)
     send_rest(3)
 
-    took(coll.at[pl.ds(0, 3)], crv)
+    @pl.when(owner)
+    def _():
+        took(coll.at[pl.ds(0, 3)], crv)
+        push(coll, coll, csn, cfw, partner)
+
+    @pl.when(jnp.logical_not(owner))
+    def _():
+        took(coll, cfw)
+
     took(mixl.at[pl.ds(0, 3)], mrv)
     rows = osend.shape[1]
     left = coll[...].reshape(4 * tokens, quarter)
@@ -453,8 +470,6 @@
         tails = spread(tail, g)
         gx = gxi[:, cols(g)] + dotf(b, later, NT) * tails
         gsi_o[:, cols(g)] = gx.astype(bf16)
-        gb = gbi[:, states(g)] + dotf((xf * tails).astype(bf16), later)
-        gb_o[:, states(g)] = gb.astype(bf16)
         sel = jnp.where(
             lax.broadcasted_iota(jnp.int32, (gw_cols, STATE), 0) // HEAD_DIM + g * per
             == lax.broadcasted_iota(jnp.int32, (gw_cols, STATE), 1),
@@ -470,6 +485,11 @@
         return 0
 
     lax.fori_loop(1, n, send_total, 0)
+    for g in range(groups):
+        xf = xin[:, cols(g)].astype(f32)
+        later = lrecv[g * slabs : (g + 1) * slabs].reshape(gw_cols, STATE)
+        gb = gbi[:, states(g)] + dotf((xf * spread(tail, g)).astype(bf16), later)
+        gb_o[:, states(g)] = gb.astype(bf16)
     took(orecv, orv)
     total = orecv[0].astype(f32)
     for k in range(1, n // 4):
@@ -482,7 +502,15 @@
     total = suffix + after[0:1, :]
     gld_o[...] = exact(total, jnp.where(ti == si, 1.0, 0.0), TN)[:heads, :]
 
-    took(coll.at[pl.ds(0, 3)], csn)
+    @pl.when(owner)
+    def _():
+        took(coll.at[pl.ds(0, 1)], csn)
+        took(coll, csn)
+
+    @pl.when(jnp.logical_not(owner))
+    def _():
+        took(coll.at[pl.ds(0, 2)], csn)
+
     took(mixl.at[pl.ds(0, 3)], msn)
     took(drecv.at[most], dsn)
     took(bsend.at[most], bsn)
@@ -547,7 +575,7 @@
             dma((12,)), dma, dma((4,)), dma, dma((4,)), dma, dma((4,)), dma, dma((4,)),
             dma, dma((4,)), dma, dma, dma, dma,
         ]
-        + [dma] * 14,
+        + [dma] * 15,
         compiler_params=pltpu.CompilerParams(
             collective_id=1, has_side_effects=True, vmem_limit_bytes=55 * 1024 * 1024
         ),

time: 110 us -> 99.7 us (0.906)
  Pallas kernels: 107 us -> 97 us
    pallas_call x1, Pallas kernels: 104 us -> 94 us  [whole(): pl.pallas_call(whole_kernel, out_shape=(shaped((dwidth, hid), bf16), shap...]
where the time goes in v5:
time: 99.7 us; the launch traced here: 99.1 us
  Pallas kernels  97 us (97%)
  local copies, waits for them, and re-layouts  1.28 us (1%)
    pallas_call x1, Pallas kernels, whole(): pl.pallas_call(whole_kernel, out_shape=(shaped((dwidth, hid), bf16), shap...  94 us
    pallas_call x1, Pallas kernels, put_out(): pl.pallas_call(put_out_kernel, out_shape=tuple((pltpu.HBM(a.shape, a.dtyp...  2.99 us

profile of v5, /device:TPU:0, one launch (start us, length us, event | category | flops | bytes accessed | tf_op | source)
XLA Modules:
  0.0 99.1 jit_solution(7860981091974413535)
XLA Ops:
  0.6 1.3 %broadcast_in_dim.12.gain = bf16[1,1024]{1,0:T(2,128)(2,1)} reshape(bf16[1024]{0:T(1024)(128)(2,1)} %param.27) | data formatting | bytes 4096 | tf_op jit(solution)/shard_map/broadcast_in_dim | solution.py:631
  1.9 94.0 %backward.1 = (bf16[2048,512]{1,0:T(8,128)(2,1)S(1)}, bf16[2048,512]{1,0:T(8,128)(2,1)S(1)}, bf16[512,2048]{1,0:T(8,128)(2,1)S(1)}, f32[32,1024]{1,0:T(8,128)S(1...) custom-call(bf16[128,2048]{1,0:T(8,128)(2,1)} %cot.1, ...), custom_call_target="tpu_custom_call" | custom-call | tf_op jit(solution)/shard_map/backward/pallas_call | solution.py:547
  95.9 3.0 %put_out.1 = (bf16[2048,512]{1,0:T(8,128)(2,1)}, bf16[2048,512]{1,0:T(8,128)(2,1)}, bf16[512,2048]{1,0:T(8,128)(2,1)}, f32[32,1024]{1,0:T(8,128)}, bf16[128,1024...) custom-call(bf16[2048,512]{1,0:T(8,128)(2,1)S(1)} %get-tuple-element, ...), custom_call_target="tpu_custom_call" | custom-call | tf_op jit(solution)/shard_map/put_out/pallas_call | solution.py:600

commit v6 on v5

--- a/solution.py
+++ b/solution.py
@@ -177,6 +177,13 @@
     def cols(g):
         return slice(g * gw_cols, (g + 1) * gw_cols)
 
+    gain_rows = gain[...].astype(f32)
+    lines = gw_cols // STATE
+
+    def gains(g):
+        at = range(g * lines, (g + 1) * lines)
+        return jnp.concatenate([gain_rows[i : i + 1, :] for i in at], axis=1)
+
     def states(g):
         return slice(g * STATE, (g + 1) * STATE)
 
@@ -207,7 +214,7 @@
         invs.append(inv)
         u = gated * inv
         unit[:, cols(g)] = u
-        mixl[z, :, cols(g)] = (u * gain[:, cols(g)].astype(f32)).astype(bf16)
+        mixl[z, :, cols(g)] = (u * gains(g)).astype(bf16)
 
     def send_mixed():
         for k in range(1, 4):
@@ -355,7 +362,7 @@
     slabs = gw_cols // slab
     for g in range(groups):
         c = cp[:, states(g)]
-        gain_f = gain[:, cols(g)].astype(f32)
+        gain_f = gains(g)
         gu = dotf(gh[...], wout[cols(g), :], NT) * gain_f
         u = unit[:, cols(g)]
         out = so[:, cols(g)]
@@ -628,7 +635,7 @@
     entry_state,
 ):
     outs = whole(
-        layer_cotangent, expert_choice.T, route_weight.T, log_decay.T, norm_gain[None],
+        layer_cotangent, expert_choice.T, route_weight.T, log_decay.T, norm_gain.reshape(-1, STATE),
         mixer_output, gate_pre[0], up_pre[0], w_down[0], w_gate[0], w_up[0], w_out,
         scan_in, gate_in, b_proj, c_proj, entry_state.reshape(-1, STATE),
     )

time: 99.7 us -> 98.5 us (0.988)
  local copies, waits for them, and re-layouts: 1.28 us -> 0 us
    broadcast_in_dim x1 -> x0, local copies, waits for them, and re-layouts: 1.28 us -> none  [body(): norm_gain[None]]
where the time goes in v6:
time: 98.5 us; the launch traced here: 97.8 us
  Pallas kernels  97 us (98%)
    pallas_call x1, Pallas kernels, whole(): pl.pallas_call(whole_kernel, out_shape=(shaped((dwidth, hid), bf16), shap...  94 us
    pallas_call x1, Pallas kernels, put_out(): pl.pallas_call(put_out_kernel, out_shape=tuple((pltpu.HBM(a.shape, a.dtyp...  2.99 us

profile of v6, /device:TPU:0, one launch (start us, length us, event | category | flops | bytes accessed | tf_op | source)
XLA Modules:
  0.0 97.8 jit_solution(621594279218415770)
XLA Ops:
  0.6 94.0 %backward.1 = (bf16[2048,512]{1,0:T(8,128)(2,1)S(1)}, bf16[2048,512]{1,0:T(8,128)(2,1)S(1)}, bf16[512,2048]{1,0:T(8,128)(2,1)S(1)}, f32[32,1024]{1,0:T(8,128)S(1...) custom-call(bf16[128,2048]{1,0:T(8,128)(2,1)} %cot.1, ...), custom_call_target="tpu_custom_call" | custom-call | tf_op jit(solution)/shard_map/backward/pallas_call | solution.py:554
  94.7 3.0 %put_out.1 = (bf16[2048,512]{1,0:T(8,128)(2,1)}, bf16[2048,512]{1,0:T(8,128)(2,1)}, bf16[512,2048]{1,0:T(8,128)(2,1)}, f32[32,1024]{1,0:T(8,128)}, bf16[128,1024...) custom-call(bf16[2048,512]{1,0:T(8,128)(2,1)S(1)} %get-tuple-element, ...), custom_call_target="tpu_custom_call" | custom-call | tf_op jit(solution)/shard_map/put_out/pallas_call | solution.py:607
